TPU v7x, 128 devices: a whole 4x4x4 slice. The times are simulated.
128 devices in a mesh: sp: 16 (over z, x), tp: 8 (over y, core).
Axes of the slice: x: 4, y: 4, z: 4, core: 2. Of those that a mesh axis runs over, the one named last changes fastest.
Arguments:
- resid: bfloat16 [12288, 3072], P('sp', 'tp'), may hold values from -12 to 12
- query: bfloat16 [12288, 1536], P('sp', 'tp'), may hold values from -6 to 6
- keys: bfloat16 [12288, 1536], P('sp', 'tp'), may hold values from -6 to 6
- values: bfloat16 [12288, 1536], P('sp', 'tp'), may hold values from -6 to 6
- out_gate: bfloat16 [12288, 1536], P('sp', 'tp'), may hold values from -6 to 6
- in_gate: float32 [16, 12288], P('tp', 'sp'), may hold values from -6 to 110
- forget: float32 [16, 12288], P('tp', 'sp'), may hold values from -1 to 16
- doc_ids: int32 [12288], P('sp'), may hold values from 0 to 7, never falling along the last dimension, each value on 1 to 3072 neighbouring positions
- head_gain: float32 [1536], P('tp'), may hold values from 0.1 to 1.9
- w_out: bfloat16 [1536, 3072], P('tp'), may hold values from -0.15625 to 0.15625
- ffn_gain: float32 [3072], replicated, may hold values from 0.1 to 1.9
- w_gate: bfloat16 [3072, 8448], P('sp', 'tp'), may hold values from -0.109375 to 0.109375
- w_value: bfloat16 [3072, 8448], P('sp', 'tp'), may hold values from -0.109375 to 0.109375
- conv_taps: float32 [3, 8448], P(None, 'tp'), may hold values from -3.5 to 3.5
- w_down: bfloat16 [8448, 3072], P('tp', 'sp'), may hold values from -0.0625 to 0.0625
Outputs:
- layer_out: bfloat16 [12288, 3072], P('sp', 'tp')
Inputs may be any that keep to these rules, and one draw needn't show every extreme that they name: `doc_ids`: document numbers never fall along the positions; each document is 1 to 3072 positions long.
All inputs are finite; a program needn't handle non-finite values.
Results may differ from a plain program's by a relative error of at most 0.02.
Values may be sent and summed in bfloat16 or wider, within the bound.
No kernel may reach another device: no remote copies, remote signals or barrier semaphores. Data moves between devices by JAX's collectives and lax.ppermute only.
A program may use at most 128 MiB of HBM per device.

v0:
```python
import jax
import jax.numpy as jnp
from jax import lax
from jax.sharding import Mesh
from jax.sharding import PartitionSpec as P

DH = 96
BLOCK = 64
SP = ("sp_0", "sp_1")


ABSENT = -1e30
epsilon = 1e-06
head_floor = 1.0


def nothing_yet(value, identity):
    return jax.tree.map(
        lambda part, zero: jnp.zeros_like(part) + jnp.asarray(zero, part.dtype), value, identity
    )


def collected_together(value, axis):
    leaves = jax.tree.leaves(value)
    order = sorted(range(len(leaves)), key=lambda k: -leaves[k].size)
    width = (1, *leaves[order[0]].shape)[-1]
    lines = [
        jnp.pad(leaves[k].reshape(-1), (0, -leaves[k].size % width)).reshape(-1, width)
        for k in order
    ]
    both, at, found = (lax.all_gather(jnp.concatenate(lines), axis), 0, {})
    for k, line in zip(order, lines):
        share = both[:, at : at + len(line)].reshape(len(both), -1)
        found[k] = share[:, : leaves[k].size].reshape(-1, *leaves[k].shape)
        at += len(line)
    numbers = iter(range(len(leaves)))
    return jax.tree.map(lambda _: found[next(numbers)], value)


def prefix_by_axis(value, axes, combine, identity):
    before = start = nothing_yet(value, identity)
    subtotal = value
    for axis in reversed(axes):
        length, index = (lax.axis_size(axis), lax.axis_index(axis))
        pieces = collected_together(subtotal, axis)
        inside, subtotal = (start, start)
        for k in range(length):
            passed = k < index
            subtotal = combine(subtotal, jax.tree.map(lambda part: part[k], pieces))
            inside = jax.tree.map(lambda new, old: jnp.where(passed, new, old), subtotal, inside)
        before = combine(inside, before)
    return before


def in_one_piece(arrays, axis, dim, along):
    widths = [a.shape[along] for a in arrays]
    both = jnp.concatenate(arrays, axis=along)
    result = lax.all_gather(both, axis, axis=dim, tiled=True)
    return tuple(jnp.split(result, [sum(widths[:k]) for k in range(1, len(widths))], axis=along))


def passed_along(value, axis, steps):
    count = lax.axis_size(axis)
    initial, last = (max(0, -steps), min(count, count - steps))
    return lax.ppermute(value, axis, [(source, source + steps) for source in range(initial, last)])


def combine(early, late):
    state_early, peak_early, decay_early, first_early, last_early, second_early = early
    state_late, peak_late, decay_late, first_late, last_late, second_late = late
    early_empty = last_early < 0.0
    late_empty = first_late < 0.0
    cut = (first_late != last_early) & jnp.logical_not(early_empty) & jnp.logical_not(late_empty)
    passed = jnp.where(cut, ABSENT, decay_late)
    peak = jnp.maximum(passed + peak_early, peak_late)
    keep = jnp.exp(passed + peak_early - peak)
    fresh = jnp.exp(peak_late - peak)
    state = keep[..., None, None] * state_early + fresh[..., None, None] * state_late
    return (
        state,
        peak,
        decay_early + passed,
        jnp.where(early_empty, first_late, first_early),
        jnp.where(late_empty, last_early, last_late),
        jnp.where(late_empty, second_early, second_late),
    )


def empty_state(heads, width):
    return (
        jnp.zeros((heads, width, width), jnp.float32),
        jnp.full((heads,), ABSENT, jnp.float32),
        jnp.zeros((heads,), jnp.float32),
        jnp.full((1,), -1.0, jnp.float32),
        jnp.full((1,), -1.0, jnp.float32),
        jnp.full((1,), -1.0, jnp.float32),
    )


def advance(carry, item):
    return (combine(carry, item), carry)


def block_parts(query, keys, values, in_gate, forget, seg):
    length, heads, width = query.shape
    count = length // BLOCK
    query_blocks = query.reshape(count, BLOCK, heads, width)
    key_blocks = (keys * width ** (-0.5)).reshape(count, BLOCK, heads, width)
    value_blocks = values.reshape(count, BLOCK, heads, width)
    gate_in = in_gate.T.reshape(count, BLOCK, heads)
    cumul = jnp.cumsum(jax.nn.log_sigmoid(forget.T).reshape(count, BLOCK, heads), axis=1)
    seg_blocks = seg.reshape(count, BLOCK)
    total = cumul[:, -1]
    in_last = (seg_blocks == seg_blocks[:, -1:])[:, :, None]
    weight_log = jnp.where(in_last, total[:, None] - cumul + gate_in, ABSENT)
    local_peak = jnp.max(weight_log, axis=1)
    weights = jnp.exp(weight_log - local_peak[:, None])
    update = jnp.einsum("nchk,nchv->nhkv", weights[..., None] * key_blocks, value_blocks)
    whole = jnp.all(seg_blocks == seg_blocks[:, :1], axis=1)[:, None]
    decay = jnp.where(whole, total, ABSENT)
    elements = (
        update,
        local_peak,
        decay,
        seg_blocks[:, :1],
        seg_blocks[:, -1:],
        seg_blocks[:, -2:-1],
    )
    return (elements, (query_blocks, key_blocks, value_blocks, gate_in, cumul, seg_blocks))


def block_outputs(before, parts):
    state, peak_prev, _, _, last_prev, _ = before
    query_blocks, key_blocks, value_blocks, gate_in, cumul, seg_blocks = parts
    count, span, heads, width = query_blocks.shape
    carried = (seg_blocks == last_prev)[:, :, None]
    inter = jnp.where(carried, cumul + peak_prev[:, None], ABSENT)
    places = jnp.arange(span)
    causal = (places[:, None] >= places[None, :])[None, :, :, None]
    same = (seg_blocks[:, :, None] == seg_blocks[:, None, :])[..., None]
    diff_log = jnp.where(
        causal & same, cumul[:, :, None] - cumul[:, None] + gate_in[:, None], ABSENT
    )
    top = jnp.maximum(inter, jnp.max(diff_log, axis=2))
    scores = jnp.einsum("nthd,nshd->ntsh", query_blocks, key_blocks) * jnp.exp(
        diff_log - top[:, :, None]
    )
    result = jnp.einsum("ntsh,nshd->nthd", scores, value_blocks)
    result = result + jnp.exp(inter - top)[..., None] * jnp.einsum(
        "nthk,nhkv->nthv", query_blocks, state
    )
    return result.reshape(count * span, heads, width)


def body(
    resid,
    query,
    keys,
    values,
    out_gate,
    in_gate,
    forget,
    doc_ids,
    head_gain,
    w_out,
    ffn_gain,
    w_gate,
    w_value,
    conv_taps,
    w_down,
):
    tokens = query.shape[0]
    heads = query.shape[1] // DH
    seg = doc_ids.astype(jnp.float32)
    query_f = query.astype(jnp.float32).reshape(tokens, heads, DH)
    keys_f = keys.astype(jnp.float32).reshape(tokens, heads, DH)
    values_f = values.astype(jnp.float32).reshape(tokens, heads, DH)
    elements, parts = block_parts(query_f, keys_f, values_f, in_gate, forget, seg)
    local_end, before = lax.scan(advance, empty_state(heads, DH), elements)
    incoming = prefix_by_axis(local_end, SP, combine, empty_state(heads, DH))
    starts = combine(incoming, before)
    memory_out = block_outputs(starts, parts)
    normed = memory_out * lax.rsqrt(
        jnp.mean(memory_out * memory_out, axis=-1, keepdims=True) + head_floor
    )
    normed = (
        normed.reshape(tokens, heads * DH)
        * head_gain
        * jax.nn.sigmoid(out_gate.astype(jnp.float32))
    )
    mix = normed.astype(jnp.bfloat16)
    share = jnp.dot(mix, w_out, preferred_element_type=jnp.float32).astype(jnp.bfloat16)
    term = lax.optimization_barrier(share).astype(jnp.float32)
    local_cols = resid.shape[1]
    offset = lax.axis_index("tp") * local_cols
    placed = lax.dynamic_update_slice_in_dim(
        jnp.zeros_like(term), resid.astype(jnp.float32), offset, 1
    )
    full_rows = lax.psum(term + placed, "tp")
    scale = lax.rsqrt(jnp.mean(full_rows * full_rows, axis=1, keepdims=True) + epsilon)
    normed_rows = (full_rows * scale * ffn_gain).astype(jnp.bfloat16)
    residual_own = lax.dynamic_slice_in_dim(full_rows, offset, local_cols, 1)
    pieces = in_one_piece((w_gate, w_value), SP, 0, 1)
    gate = jnp.dot(normed_rows, pieces[0], preferred_element_type=jnp.float32)
    value = jnp.dot(normed_rows, pieces[1], preferred_element_type=jnp.float32)
    gate = gate.astype(jnp.bfloat16)
    value = value.astype(jnp.bfloat16)
    edge = passed_along(gate[tokens - 2 :], SP, 1)
    extended = jnp.concatenate([edge, gate], axis=0).astype(jnp.float32)
    ids = jnp.concatenate([incoming[5], incoming[4], seg])
    near = (ids[1:-1] == seg)[:, None]
    far = (ids[:-2] == seg)[:, None]
    conv = (
        conv_taps[2] * extended[2:]
        + conv_taps[1] * jnp.where(near, extended[1:-1], 0.0)
        + conv_taps[0] * jnp.where(far, extended[:-2], 0.0)
    )
    hidden = (jax.nn.silu(conv) * value.astype(jnp.float32)).astype(jnp.bfloat16)
    terms = jnp.dot(
        hidden, lax.all_gather(w_down, SP, axis=1, tiled=True), preferred_element_type=jnp.float32
    )
    down = lax.psum_scatter(
        terms.astype(jnp.bfloat16), "tp", scatter_dimension=1, tiled=True
    ).astype(jnp.float32)
    return (residual_own + down).astype(jnp.bfloat16)


def solution(mesh):
    torus = Mesh(mesh.devices.reshape(4, 4, mesh.shape["tp"]), ("sp_0", "sp_1", "tp"))
    placed = (
        P(SP, "tp"),
        P(SP, "tp"),
        P(SP, "tp"),
        P(SP, "tp"),
        P(SP, "tp"),
        P("tp", SP),
        P("tp", SP),
        P(SP),
        P("tp"),
        P("tp", None),
        P(),
        P(SP, "tp"),
        P(SP, "tp"),
        P(None, "tp"),
        P("tp", SP),
    )
    return jax.shard_map(body, mesh=torus, in_specs=placed, out_specs=P(SP, "tp"), check_vma=False)
```

profile of v0, /device:TPU:0, one launch (start us, length us, event | category | flops | bytes accessed | tf_op | source)
XLA Modules:
  0.0 438.6 jit_solution(1473426285927869053)
XLA Ops:
  8.6 6.3 %fusion.104 = f32[12,64,2]{2,0,1:T(8,128)S(1)} fusion(f32[12,64,2]{2,0,1:T(8,128)S(1)} %copy.338), kind=kOutput, calls=%fused_computation.244 | output fusion | flops 96768 | bytes 12288 | tf_op jit(solution)/shard_map/jit(cumsum)/reduce_window_sum | solution.py:111
  19.5 1.4 reshape.907
  20.9 1.3 copy.349
  22.3 1.6 broadcast_multiply_fusion.1
  23.9 1.3 fusion.37
  25.3 94.5 %while.32 = (s32[]{:T(128)}, f32[2,96,96]{2,1,0:T(8,128)S(1)}, f32[2]{0:T(128)S(1)}, f32[2]{0:T(128)S(1)}, f32[1]{0:T(128)}, /*index=5*/f32[1]{0:T(128)}, f32[1]...) while((s32[]{:T(128)}, f32[2,96,96]{2,1,0:T(8,128)S(1)}, ...), condition=%wide.region_4.5_spmd.clone.clone, body=%wide.region_3.4_spmd.clone.sunk.clone | while | flops 92189 | bytes 394247 | solution.py:179
  27.9 1.3 dynamic_update_slice.40
  29.2 1.3 dynamic_update_slice.41
  36.9 1.3 dynamic_update_slice.41
  43.5 1.3 dynamic_update_slice.40
  44.8 1.3 dynamic_update_slice.41
  51.4 1.3 dynamic_update_slice.40
  52.7 1.3 dynamic_update_slice.41
  59.3 1.3 dynamic_update_slice.40
  60.6 1.3 dynamic_update_slice.41
  68.4 1.3 dynamic_update_slice.41
  75.0 1.3 dynamic_update_slice.40
  76.3 1.3 dynamic_update_slice.41
  84.2 1.3 dynamic_update_slice.41
  90.8 1.3 dynamic_update_slice.40
  92.1 1.3 dynamic_update_slice.41
  98.7 1.3 dynamic_update_slice.40
  100.0 1.3 dynamic_update_slice.41
  106.6 1.3 dynamic_update_slice.40
  107.9 1.3 dynamic_update_slice.41
  114.5 1.3 dynamic_update_slice.40
  115.7 1.3 dynamic_update_slice.41
  120.7 13.0 %all-gather.2 = f32[4,197,96]{1,2,0:T(8,128)S(1)} all-gather(f32[1,197,96]{1,2,0:T(8,128)S(1)} %bitcast.367), channel_id=2, replica_groups=mesh['sp_0'=4,'sp_1'=4,'tp'=8] {'sp_1'}, dimensions={0}, use_global_device_ids=true | all-gather | bytes 378240 | tf_op jit(solution)/shard_map/all_gather | solution.py:31
  151.3 14.3 %all-gather.3 = f32[4,197,96]{1,2,0:T(8,128)S(1)} all-gather(f32[1,197,96]{1,2,0:T(8,128)S(1)} %bitcast.368), channel_id=3, replica_groups=mesh['sp_0'=4,'sp_1'=4,'tp'=8] {'sp_0'}, dimensions={0}, use_global_device_ids=true | all-gather | bytes 378240 | tf_op jit(solution)/shard_map/all_gather | solution.py:31
  184.1 1.3 multiply_add_fusion
  185.4 1.7 fusion.33
  187.1 2.6 multiply_reduce_fusion.1
  193.0 1.4 convolution_convert_fusion.1
  194.5 4.9 %convert_element_type.66 = f32[768,3072]{1,0:T(8,128)} convert(bf16[768,3072]{1,0:T(8,128)(2,1)S(1)} %convolution_convert_fusion.1) | non-fusion elementwise | flops 2359296 | bytes 14155776 | tf_op jit(solution)/shard_map/convert_element_type | solution.py:193
  199.4 2.5 add_dynamic-update-slice_fusion
  208.3 108.6 %all-reduce.12.cloned.1.call-done = f32[768,3072]{1,0:T(8,128)} async-done(((f32[768,3072]{1,0:T(8,128)}), f32[768,3072]{1,0:T(8,128)}) %all-reduce.12.cloned.1.call-update) | async-done | bytes 9437200 | tf_op jit(solution)/shard_map/psum | solution.py:199
  316.9 4.5 %multiply_reduce_fusion = f32[768]{0:T(1024)S(1)} fusion(f32[768,3072]{1,0:T(8,128)} %all-reduce.12.cloned.1.call-done), kind=kLoop, calls=%fused_computation.21 | loop fusion | flops 4717824 | bytes 9440256 | tf_op jit(solution)/shard_map/reduce_sum | solution.py:200
  321.5 11.5 %fusion.12 = bf16[768,1056]{0,1:T(8,128)(2,1)S(1)} fusion(bf16[3072,2112]{1,0:T(8,128)(2,1)} %all-gather.7.cloned.1.call-done, f32[768,3072]{1,0:T(8,128)} %all-reduce.12.cloned.1.call-done, f32[3072]{0:T(1024)S(1)} %copy-done.33, f32[768]{0:T(1024)S(1)} %add_rsqrt_fusion.1), kind=kOutput, calls=%fused_computation.28 | convolution fusion | flops 4990722048 | bytes 18152448 | tf_op jit(solution)/shard_map/dot_general | solution.py:204
  333.1 3.6 collective-permute-start
  336.8 11.9 %collective-permute-done = bf16[2,1056]{0,1:T(8,128)(2,1)S(1)} collective-permute-done((bf16[2,1056]{0,1:T(8,128)(2,1)S(1)}, bf16[2,1056]{0,1:T(8,128)(2,1)S(1)}, u32[]{:S(2)}, u32[]{:S(2)}) %collective-permute-start) | collective-permute-done | bytes 4256 | tf_op jit(solution)/shard_map/ppermute | solution.py:65
  348.6 2.6 maximum_convert_fusion
  351.3 18.2 %fusion.24 = bf16[768,1056]{0,1:T(8,128)(2,1)S(1)} fusion(bf16[3072,2112]{1,0:T(8,128)(2,1)} %all-gather.7.cloned.1.call-done, f32[770,1056]{0,1:T(8,128)} %maximum_convert_fusion, f32[1056]{0:T(1024)S(1)} %get-tuple-element.330, f32[1056]{0:T(1024)S(1)} %get-tuple-element.331, f32[1056]{0:T(1024)S(1)} %get-tuple-element.329, ...), kind=kOutput, calls=%fused_computation.32 | convolution fusion | flops 5002076160 | bytes 27898752 | tf_op jit(solution)/shard_map/dot_general | solution.py:205
  369.5 1.5 all-gather.9.cloned.1.call-done
  371.0 11.1 %convolution_convert_fusion = bf16[768,3072]{1,0:T(8,128)(2,1)} fusion(bf16[768,1056]{0,1:T(8,128)(2,1)S(1)} %fusion.24, bf16[1056,3072]{0,1:T(8,128)(2,1)} %all-gather.9.cloned.1.call-done), kind=kOutput, calls=%fused_computation.26 | convolution fusion | flops 4985192448 | bytes 12828672 | tf_op jit(solution)/shard_map/dot_general | solution.py:219
  382.1 6.6 %copy.389 = bf16[768,3072]{0,1:T(8,128)(2,1)} copy(bf16[768,3072]{1,0:T(8,128)(2,1)} %convolution_convert_fusion) | data formatting | bytes 9437184
  388.8 38.8 %reduce-scatter.4.cloned.1.call-done = bf16[384,768]{1,0:T(8,128)(2,1)} async-done(((bf16[3072,768]{1,0:T(8,128)(2,1)}), bf16[384,768]{1,0:T(8,128)(2,1)}) %reduce-scatter.4.cloned.1.call-update) | async-done | bytes 589840
  427.6 1.4 copy.390
  429.0 2.2 add_convert_fusion
  (311 shorter events, 59.8 us)
Async XLA Ops:
  7.4 185.6 %copy-start = (bf16[192,3072]{1,0:T(8,128)(2,1)S(1)}, bf16[192,3072]{1,0:T(8,128)(2,1)}, u32[]{:S(2)}) copy-start(bf16[192,3072]{1,0:T(8,128)(2,1)} %param.26) | copy-start | bytes 3538948
  7.4 309.5 %all-reduce.12.cloned.1.call-start = ((), (), s32[]{:S(2)}) async-start(), calls=%async_computation.1 | async-start | bytes 18874368 | tf_op jit(solution)/shard_map/psum | solution.py:199
  17.5 158.7 %copy-start.11 = (f32[12,64,2]{1,2,0:T(2,128)}, f32[12,64,2]{1,2,0:T(2,128)S(1)}, u32[]{:S(2)}) copy-start(f32[12,64,2]{1,2,0:T(2,128)S(1)} %get-tuple-element.393) | copy-start | bytes 18436
  119.7 0.6 copy-start.29
  119.8 0.6 copy-start.31
  120.6 54.9 %copy-start.15 = (f32[12,2]{1,0:T(8,128)S(1)}, f32[12,2]{1,0:T(8,128)}, u32[]{:S(2)}) copy-start(f32[12,2]{1,0:T(8,128)} %get-tuple-element.116) | copy-start | bytes 292
  120.6 55.0 %copy-start.16 = (f32[12,2]{1,0:T(8,128)S(1)}, f32[12,2]{1,0:T(8,128)}, u32[]{:S(2)}) copy-start(f32[12,2]{1,0:T(8,128)} %get-tuple-element.115) | copy-start | bytes 292
  120.6 55.1 %copy-start.30 = (f32[12,1]{0,1:T(1,128)S(1)}, f32[12,1]{0,1:T(1,128)}, u32[]{:S(2)}) copy-start(f32[12,1]{0,1:T(1,128)} %copy-done.29) | copy-start | bytes 148
  120.6 55.3 %copy-start.32 = (f32[12,1]{0,1:T(1,128)S(1)}, f32[12,1]{0,1:T(1,128)}, u32[]{:S(2)}) copy-start(f32[12,1]{0,1:T(1,128)} %copy-done.31) | copy-start | bytes 148
  147.0 34.6 %copy-start.10 = (bf16[768,192]{0,1:T(8,128)(2,1)S(1)}, bf16[768,192]{0,1:T(8,128)(2,1)}, u32[]{:S(2)}) copy-start(bf16[768,192]{0,1:T(8,128)(2,1)} %param.18) | copy-start | bytes 884740
  149.2 1.9 copy-start.26
  149.2 0.6 copy-start.23
  149.2 0.7 copy-start.24
  149.2 0.9 copy-start.17
  149.3 1.0 copy-start.20
  149.3 1.2 copy-start.21
  149.3 1.3 copy-start.19
  149.3 1.4 copy-start.22
  166.7 17.4 %copy-start.18 = (f32[2]{0:T(128)S(1)}, f32[2]{0:T(128)}, u32[]{:S(2)}) copy-start(f32[2]{0:T(128)} %copy-done.17) | copy-start | bytes 28
  175.9 6.7 %copy-start.27 = (f32[2]{0:T(128)S(1)}, f32[2]{0:T(128)}, u32[]{:S(2)}) copy-start(f32[2]{0:T(128)} %get-tuple-element.377) | copy-start | bytes 28
  176.2 5.3 %copy-start.9 = (pred[12,64,64]{1,2,0:T(8,128)(4,1)}, pred[12,64,64]{1,2,0:T(8,128)(4,1)S(1)}, u32[]{:S(2)}) copy-start(pred[12,64,64]{1,2,0:T(8,128)(4,1)S(1)} %compare_and_fusion) | copy-start | bytes 147460
  176.2 6.4 %copy-start.28 = (f32[2]{0:T(128)S(1)}, f32[2]{0:T(128)}, u32[]{:S(2)}) copy-start(f32[2]{0:T(128)} %get-tuple-element.381) | copy-start | bytes 28
  176.2 7.9 %copy-start.25 = (f32[2]{0:T(128)S(1)}, f32[2]{0:T(128)}, u32[]{:S(2)}) copy-start(f32[2]{0:T(128)} %get-tuple-element.376) | copy-start | bytes 28
  178.2 5.9 %copy-start.6 = (f32[1,192,96]{2,1,0:T(8,128)S(1)}, f32[1,192,96]{2,1,0:T(8,128)}, u32[]{:S(2)}) copy-start(f32[1,192,96]{2,1,0:T(8,128)} %copy.372) | copy-start | bytes 221188
  179.0 5.1 %copy-start.7 = (f32[1,192,96]{2,1,0:T(8,128)S(1)}, f32[1,192,96]{2,1,0:T(8,128)}, u32[]{:S(2)}) copy-start(f32[1,192,96]{2,1,0:T(8,128)} %copy.373) | copy-start | bytes 221188
  179.7 4.4 %copy-start.8 = (f32[1,192,96]{2,1,0:T(8,128)S(1)}, f32[1,192,96]{2,1,0:T(8,128)}, u32[]{:S(2)}) copy-start(f32[1,192,96]{2,1,0:T(8,128)} %copy.374) | copy-start | bytes 221188
  180.5 6.6 %copy-start.2 = (bf16[12,64,2,96]{3,1,2,0:T(8,128)(2,1)S(1)}, bf16[12,64,2,96]{3,1,2,0:T(8,128)(2,1)}, u32[]{:S(2)}) copy-start(bf16[12,64,2,96]{3,1,2,0:T(8,128)(2,1)} %copy.349) | copy-start | bytes 884740
  189.7 3.4 copy-start.34
  194.5 5.0 %copy-start.3 = (bf16[768,384]{1,0:T(8,128)(2,1)S(1)}, bf16[768,384]{1,0:T(8,128)(2,1)}, u32[]{:S(2)}) copy-start(bf16[768,384]{1,0:T(8,128)(2,1)} %param.17) | copy-start | bytes 1769476
  201.9 1.0 copy-start.4
  201.9 1.1 copy-start.5
  201.9 3.2 copy-start.14
  201.9 6.4 %copy-start.12 = (s32[768]{0:T(1024)S(1)}, s32[768]{0:T(1024)}, u32[]{:S(2)}) copy-start(s32[768]{0:T(1024)} %param.24) | copy-start | bytes 9220
  202.0 119.5 %all-gather.7.cloned.1.call-start = ((), (), s32[]{:S(2)}) async-start(), calls=%async_computation.2 | async-start | bytes 14204928 | tf_op jit(solution)/shard_map/all_gather | solution.py:58
  204.2 166.8 %all-gather.9.cloned.1.call-start = ((), (), s32[]{:S(2)}) async-start(), calls=%async_computation.3 | async-start | bytes 7520256 | tf_op jit(solution)/shard_map/all_gather | solution.py:220
  204.8 222.8 %reduce-scatter.4.cloned.1.call-start = ((), (), s32[]{:S(2)}) async-start(), calls=%async_computation.4 | async-start | bytes 5308416
  208.3 113.1 %copy-start.33 = (f32[3072]{0:T(1024)S(1)}, f32[3072]{0:T(1024)}, u32[]{:S(2)}) copy-start(f32[3072]{0:T(1024)} %param.27) | copy-start | bytes 36868
  321.4 15.3 %copy-start.13 = (f32[3,1056]{1,0:T(4,128)S(1)}, f32[3,1056]{1,0:T(4,128)}, u32[]{:S(2)}) copy-start(f32[3,1056]{1,0:T(4,128)} %param.30) | copy-start | bytes 38020
  333.1 15.5 %collective-permute-start = (bf16[2,1056]{0,1:T(8,128)(2,1)S(1)}, bf16[2,1056]{0,1:T(8,128)(2,1)S(1)}, u32[]{:S(2)}, u32[]{:S(2)}) collective-permute-start(bf16[2,1056]{0,1:T(8,128)(2,1)S(1)} %slice.379), channel_id=1, source_target_pairs={{0,8},{8,16},{16,24},{24,32},{32,40},{40,48},{48,56},{56,64},{64,7... | collective-permute-start | bytes 12680 | tf_op jit(solution)/shard_map/ppermute | solution.py:65
  388.8 42.4 %copy-start.1 = (bf16[192,3072]{1,0:T(8,128)(2,1)S(1)}, bf16[192,3072]{1,0:T(8,128)(2,1)}, u32[]{:S(2)}) copy-start(bf16[192,3072]{1,0:T(8,128)(2,1)} %param.26) | copy-start | bytes 3538948
Sparse Core Ops, SparseCore 0:
  202.1 114.7 all-reduce.11
  388.9 38.6 reduce-scatter.3
Sparse Core Ops, SparseCore 1:
  204.6 94.4 all-gather.6
  301.0 70.0 all-gather.8
where the time goes:
time: 441 us; the launch traced here: 439 us
  waiting for transfers between devices  161 us (37%)
  local copies, waits for them, and re-layouts  80 us (18%)
  matrix products  47.9 us (11%)
  other arithmetic  42.4 us (10%)
  loops' own time  38.2 us (9%)
  between operations  37.6 us (9%)
  blocking collectives  27.3 us (6%)
    psum x1, waiting for transfers between devices, body(): full_rows = lax.psum(term + placed, 'tp')  109 us
    unnamed x5, waiting for transfers between devices  39.4 us
    another operation x1, loops' own time, body(): local_end, before = lax.scan(advance, empty_state(heads, DH), elements)  38.2 us
    dynamic_update_slice x48, local copies, waits for them, and re-layouts, body(): local_end, before = lax.scan(advance, empty_state(heads, DH), elements)  33.1 us
    all_gather x2, blocking collectives, collected_together(): both, at, found = (lax.all_gather(jnp.concatenate(lines), axis), 0, {})  27.3 us
    dot_general x1, matrix products, body(): value = jnp.dot(normed_rows, pieces[1], preferred_element_type=jnp.float32)  18.2 us
    dynamic_slice x24, local copies, waits for them, and re-layouts, body(): local_end, before = lax.scan(advance, empty_state(heads, DH), elements)  13.8 us
    ppermute x1, waiting for transfers between devices, passed_along(): lax.ppermute(value, axis, [(source, source + steps) for source in range(i...  11.9 us
  transfers between devices with their start and end apart: 5, of which 4 were waited for; matrix products, arithmetic and copies ran while one was open for 9% of the time, Pallas kernels for 0%

commit v1 on v0

v1 whole, which is shorter than its diff:
```python
import jax
import jax.numpy as jnp
from jax import lax
from jax.experimental import pallas as pl
from jax.experimental.pallas import tpu as pltpu
from jax.sharding import Mesh
from jax.sharding import PartitionSpec as P

DH = 96
DOC_MAX = 3072
SP = ("z", "x")
ABSENT = -1e30
EPS = 1e-06
HEAD_FLOOR = 1.0
F32 = jnp.float32
BF16 = jnp.bfloat16


def in_first_head(shape):
    return lax.broadcasted_iota(jnp.int32, shape, len(shape) - 1) < DH


def state_kernel(k_ref, v_ref, in_ref, forget_ref, doc_ref, pay_ref, row_ref, col_ref, scr):
    tokens, width = k_ref.shape
    lane = lax.broadcasted_iota(jnp.int32, (8, tokens), 1)
    doc = jnp.broadcast_to(doc_ref[...].astype(F32), (8, tokens))
    scr[...] = jnp.zeros_like(scr)
    scr[0:2, :] = forget_ref[...]
    raw = scr[...]
    total = jnp.minimum(raw, 0.0) - jnp.log1p(jnp.exp(-jnp.abs(raw)))
    step = 1
    while step < tokens:
        total = total + jnp.where(lane >= step, pltpu.roll(total, step, 1), 0.0)
        step *= 2
    scr[0:2, :] = in_ref[...]
    rest = scr[...] - total
    peak = rest
    step = 1
    while step < tokens:
        near = (lane >= step) & (pltpu.roll(doc, step, 1) == doc)
        peak = jnp.maximum(peak, jnp.where(near, pltpu.roll(peak, step, 1), ABSENT))
        step *= 2
    end_doc = doc[:, tokens - 1 : tokens]
    end_peak = peak[:, tokens - 1 : tokens]
    end_total = total[:, tokens - 1 : tokens]
    weight = jnp.where(doc == end_doc, jnp.exp(jnp.minimum(rest - end_peak, 0.0)), 0.0)
    row_ref[...] = jnp.zeros_like(row_ref)
    row_ref[0:2, :] = total[0:2, :]
    row_ref[2:4, :] = peak[0:2, :]
    row_ref[4:6, :] = weight[0:2, :]
    row_ref[6:7, :] = doc[0:1, :]
    scr[...] = row_ref[...]
    cols = scr[...].T
    col_ref[...] = cols
    row_ref[4:6, :] = rest[0:2, :]
    first = in_first_head((tokens, width))
    spread = jnp.where(first, cols[:, 4:5], cols[:, 5:6])
    weighted = (k_ref[...].astype(F32) * (spread * DH**-0.5)).astype(BF16)
    state = lax.dot_general(
        weighted, v_ref[...], (((0,), (0,)), ((), ())), preferred_element_type=F32
    )
    small = in_first_head((DH, width))
    pay_ref[0:DH, :] = jnp.where(small, state[0:DH, :], state[DH:, :]).astype(BF16)

    line = in_first_head((1, width))

    def spread_heads(x):
        return jnp.where(line, x[0:1, :], x[1:2, :])

    def split(x):
        high = x.astype(BF16).astype(F32)
        mid = (x - high).astype(BF16).astype(F32)
        return high, mid, x - high - mid

    lines = [
        *split(spread_heads(end_total + end_peak)),
        *split(spread_heads(end_total)),
        jnp.broadcast_to(end_doc[0:1, :] + 1.0, (1, width)),
        jnp.broadcast_to(doc[0:1, tokens - 2 : tokens - 1] + 1.0, (1, width)),
    ]
    place = lax.broadcasted_iota(jnp.int32, (16, width), 0)
    table = jnp.zeros((16, width), F32)
    for k, value in enumerate(lines):
        table = jnp.where(place == k, value, table)
    pay_ref[DH:, :] = table.astype(BF16)


def local_kernel(q_ref, k_ref, v_ref, row_ref, col_ref, out_ref):
    tokens, width = q_ref.shape
    block = 256
    for start in range(0, tokens, block):
        stop = start + block
        keys = k_ref[0:stop, :]
        vals = v_ref[0:stop, :]
        q = q_ref[start:stop, :]
        first = in_first_head((block, width))
        at = lax.broadcasted_iota(jnp.int32, (block, stop), 0) + start
        source = lax.broadcasted_iota(jnp.int32, (block, stop), 1)
        seen = (at >= source) & (row_ref[6:7, 0:stop] == col_ref[start:stop, 6:7])
        found = []
        for h in range(2):
            mine = jnp.where(first if h == 0 else jnp.logical_not(first), q, jnp.zeros_like(q))
            scores = lax.dot_general(
                mine, keys, (((1,), (1,)), ((), ())), preferred_element_type=F32
            )
            gap = row_ref[4 + h : 5 + h, 0:stop] - col_ref[start:stop, 2 + h : 3 + h]
            part = (scores * jnp.exp(jnp.where(seen, gap, ABSENT))).astype(BF16)
            found.append(jnp.dot(part, vals, preferred_element_type=F32))
        out_ref[start:stop, :] = jnp.where(first, found[0], found[1])


def mix_kernel(
    q_ref, gate_ref, local_ref, row_ref, col_ref, gain_ref, w_ref, *refs
):
    pays, (out_ref, ids_ref, mix_ref) = refs[:-3], refs[-3:]
    tokens, width = q_ref.shape

    @pl.when(pl.program_id(0) == 0)
    def _():
        own = row_ref[6:7, 0:1] + 1.0
        behind = jnp.zeros((1, width), F32)
        peaks, goods = [], []
        for ref in pays:
            table = ref[DH:, :].astype(F32)
            good = table[6:7, :] == own
            peaks.append(
                jnp.where(good, table[0:1, :] + table[1:2, :] + table[2:3, :] + behind, ABSENT)
            )
            goods.append(good)
            behind = behind + (table[3:4, :] + table[4:5, :] + table[5:6, :])
        best = peaks[0]
        for value in peaks[1:]:
            best = jnp.maximum(best, value)
        state = jnp.zeros((DH, width), F32)
        for ref, value, good in zip(pays, peaks, goods):
            state = state + jnp.where(good, jnp.exp(value - best), 0.0) * ref[0:DH, :].astype(F32)
        small = in_first_head((DH, width))
        whole = jnp.concatenate(
            [jnp.where(small, state, 0.0), jnp.where(small, 0.0, state)], axis=0
        ).astype(BF16)
        carried = jnp.dot(q_ref[...], whole, preferred_element_type=F32)
        first = in_first_head((tokens, width))
        total = jnp.where(first, col_ref[:, 0:1], col_ref[:, 1:2])
        peak = total + jnp.where(first, col_ref[:, 2:3], col_ref[:, 3:4])
        inter = jnp.where(col_ref[:, 6:7] + 1.0 == own, total + best, ABSENT)
        top = jnp.maximum(peak, inter)
        memory = (
            jnp.exp(peak - top) * (local_ref[...] * DH**-0.5) + jnp.exp(inter - top) * carried
        )
        square = memory * memory
        mean_0 = jnp.sum(jnp.where(first, square, 0.0), axis=1, keepdims=True) / DH
        mean_1 = jnp.sum(jnp.where(first, 0.0, square), axis=1, keepdims=True) / DH
        norm = jnp.where(first, lax.rsqrt(mean_0 + HEAD_FLOOR), lax.rsqrt(mean_1 + HEAD_FLOOR))
        gate = gate_ref[...].astype(F32)
        mix_ref[...] = (memory * norm * gain_ref[...] * (1.0 / (1.0 + jnp.exp(-gate)))).astype(BF16)
        ids_ref[...] = pays[0][DH : DH + 16, 0:128].astype(F32)[0:16, :]

    out_ref[0] = jnp.dot(mix_ref[...], w_ref[...], preferred_element_type=F32).astype(BF16)


def proj_kernel(x_ref, gain_ref, wg_ref, wv_ref, wt_ref, gate_ref, value_ref, tail_ref, x_scr):
    parts, tokens, cols = x_ref.shape
    j = pl.program_id(0)

    @pl.when(j == 0)
    def _():
        def block(i, _):
            at = pl.multiple_of(i * 64, 64)
            rows = pl.ds(at, 64)
            square = jnp.zeros((64, cols), F32)
            for p in range(parts):
                r = x_ref[p, rows, :].astype(F32)
                square = square + r * r
            mean = jnp.sum(square, axis=1, keepdims=True) / (parts * cols)
            scale = lax.rsqrt(mean + EPS)
            for p in range(parts):
                r = x_ref[p, rows, :].astype(F32)
                x_scr[rows, p * cols : (p + 1) * cols] = (
                    r * scale * gain_ref[0:1, p * cols : (p + 1) * cols]
                ).astype(BF16)
            return 0

        lax.fori_loop(0, tokens // 64, block, 0)

    x = x_scr[...]
    gate = jnp.dot(x, wg_ref[...], preferred_element_type=F32).astype(BF16)
    gate_ref[...] = gate
    value_ref[...] = jnp.dot(x, wv_ref[...], preferred_element_type=F32).astype(BF16)

    @pl.when(j == pl.num_programs(0) - 1)
    def _():
        tail_ref[...] = jnp.dot(x_scr[...], wt_ref[...], preferred_element_type=F32).astype(BF16)


def down_kernel(
    gate_ref, value_ref, tail_ref, edge_ref, ids_ref, doc_ref, taps_ref, w_ref, wt_ref, out_ref, h_scr
):
    tokens, main = gate_ref.shape

    @pl.when(pl.program_id(0) == 0)
    def _():
        row = lax.broadcasted_iota(jnp.int32, (tokens, 1), 0)
        doc = doc_ref[:, 6:7] + 1.0
        last = ids_ref[6:7, 0:1]
        second = ids_ref[7:8, 0:1]
        one = jnp.where(row == 0, last, pltpu.roll(jnp.broadcast_to(doc, (tokens, 128)), 1, 0)[:, 0:1])
        two = jnp.where(
            row == 0,
            second,
            jnp.where(row == 1, last, pltpu.roll(jnp.broadcast_to(doc, (tokens, 128)), 2, 0)[:, 0:1]),
        )
        near = (one == doc).astype(F32)
        far = (two == doc).astype(F32)

        def finish(gate, value, edge, taps):
            prev_1 = jnp.where(row == 0, edge[7:8, :], pltpu.roll(gate, 1, 0))
            prev_2 = jnp.where(
                row == 0, edge[6:7, :], jnp.where(row == 1, edge[7:8, :], pltpu.roll(gate, 2, 0))
            )
            conv = taps[2:3, :] * gate + taps[1:2, :] * (near * prev_1) + taps[0:1, :] * (far * prev_2)
            return conv / (1.0 + jnp.exp(-conv)) * value

        for at in range(0, main, 128):
            cut = slice(at, at + 128)
            h_scr[:, cut] = finish(
                gate_ref[:, cut].astype(F32),
                value_ref[:, cut].astype(F32),
                edge_ref[:, cut].astype(F32),
                taps_ref[:, cut],
            ).astype(BF16)
        tail = tail_ref[...].astype(F32)
        lane = lax.broadcasted_iota(jnp.int32, (tokens, 128), 1)
        mine = (lane >= 64) & (lane < 96)
        gate = jnp.where(mine, pltpu.roll(tail, 64, 1), 0.0)
        value = jnp.where(mine, pltpu.roll(tail, 32, 1), 0.0)
        edge = pltpu.roll(edge_ref[:, main : main + 128].astype(F32), 64, 1)
        done = finish(gate, value, edge, taps_ref[:, main : main + 128])
        h_scr[:, main : main + 128] = jnp.where(mine, done, 0.0).astype(BF16)

    contract = (((1,), (1,)), ((), ()))
    for p in range(out_ref.shape[0]):
        cols = out_ref.shape[2]
        rows = slice(p * cols, (p + 1) * cols)
        out_ref[p] = (
            lax.dot_general(h_scr[:, 0:main], w_ref[rows, :], contract, preferred_element_type=F32)
            + lax.dot_general(h_scr[:, main:], wt_ref[rows, :], contract, preferred_element_type=F32)
        ).astype(BF16)


def shape(dims, dtype):
    return jax.ShapeDtypeStruct(dims, dtype)


def whole(dims):
    return pl.BlockSpec(dims, lambda *_: (0,) * len(dims))


def body(
    resid,
    query,
    keys,
    values,
    out_gate,
    in_gate,
    forget,
    doc_ids,
    head_gain,
    w_out,
    ffn_gain,
    w_gate,
    w_value,
    conv_taps,
    w_down,
):
    tokens, width = query.shape
    cols = resid.shape[1]
    parts = w_out.shape[1] // cols
    model = w_out.shape[1]
    hidden = w_gate.shape[1]
    main = hidden // 128 * 128
    spare = hidden - main
    down_t = w_down.T
    packed = jnp.concatenate(
        [
            w_gate[:, :main],
            w_value[:, :main],
            down_t[:, :main],
            w_gate[:, main:],
            w_value[:, main:],
            down_t[:, main:],
            jnp.zeros((w_gate.shape[0], 128 - 3 * spare), BF16),
        ],
        axis=1,
    )
    weights = lax.all_gather(packed, SP, axis=0, tiled=True)
    taps = jnp.concatenate(
        [
            conv_taps[:, :main],
            jnp.zeros((3, 2 * spare), F32),
            conv_taps[:, main:],
            jnp.zeros((3, 128 - 3 * spare), F32),
        ],
        axis=1,
    )

    pay, rows, cols_aux = pl.pallas_call(
        state_kernel,
        out_shape=(
            shape((DH + 16, width), BF16),
            shape((8, tokens), F32),
            shape((tokens, 8), F32),
        ),
        scratch_shapes=[pltpu.VMEM((8, tokens), F32)],
        name="state",
    )(keys, values, in_gate, forget, doc_ids.reshape(1, tokens))
    count = lax.axis_size(SP)
    reach = -(-(DOC_MAX - 1) // tokens)
    pays = [
        lax.ppermute(pay, SP, [(i, i + k) for i in range(count - k)]) for k in range(1, reach + 1)
    ]
    local = pl.pallas_call(
        local_kernel,
        out_shape=shape((tokens, width), F32),
        name="local",
    )(query, keys, values, rows, cols_aux)
    share, ids = pl.pallas_call(
        mix_kernel,
        grid=(parts,),
        in_specs=[
            whole((tokens, width)),
            whole((tokens, width)),
            whole((tokens, width)),
            whole((8, tokens)),
            whole((tokens, 8)),
            whole((1, width)),
            pl.BlockSpec((width, cols), lambda j: (0, j)),
            *[whole((DH + 16, width)) for _ in pays],
        ],
        out_specs=(
            pl.BlockSpec((1, tokens, cols), lambda j: (j, 0, 0)),
            whole((16, 128)),
        ),
        out_shape=(shape((parts, tokens, cols), BF16), shape((16, 128), F32)),
        scratch_shapes=[pltpu.VMEM((tokens, width), BF16)],
        name="mix",
    )(query, out_gate, local, rows, cols_aux, head_gain.reshape(1, width), w_out, *pays)
    attended = lax.psum_scatter(share, "tp", scatter_dimension=0, tiled=False)
    residual_own = resid.astype(F32) + attended.astype(F32)
    full = lax.all_gather(residual_own.astype(BF16), "tp", axis=0, tiled=False)

    step = 512
    lanes = main // step
    gate, value, tail = pl.pallas_call(
        proj_kernel,
        grid=(lanes,),
        in_specs=[
            whole((parts, tokens, cols)),
            whole((1, model)),
            pl.BlockSpec((model, step), lambda j: (0, j)),
            pl.BlockSpec((model, step), lambda j: (0, lanes + j)),
            pl.BlockSpec((model, 128), lambda j: (0, 3 * main // 128)),
        ],
        out_specs=(
            pl.BlockSpec((tokens, step), lambda j: (0, j)),
            pl.BlockSpec((tokens, step), lambda j: (0, j)),
            whole((tokens, 128)),
        ),
        out_shape=(
            shape((tokens, main), BF16),
            shape((tokens, main), BF16),
            shape((tokens, 128), BF16),
        ),
        scratch_shapes=[pltpu.VMEM((tokens, model), BF16)],
        compiler_params=pltpu.CompilerParams(vmem_limit_bytes=56 * 2**20),
        name="proj",
    )(full, ffn_gain.reshape(1, model), weights, weights, weights)
    edge = lax.ppermute(
        jnp.concatenate([gate[tokens - 8 :], tail[tokens - 8 :]], axis=1),
        SP,
        [(i, i + 1) for i in range(count - 1)],
    )
    pieces = 2
    terms = pl.pallas_call(
        down_kernel,
        grid=(parts // pieces,),
        in_specs=[
            whole((tokens, main)),
            whole((tokens, main)),
            whole((tokens, 128)),
            whole((8, main + 128)),
            whole((16, 128)),
            whole((tokens, 8)),
            whole((3, main + 128)),
            pl.BlockSpec((pieces * cols, main), lambda j: (j, 2)),
            pl.BlockSpec((pieces * cols, 128), lambda j: (j, 3 * main // 128)),
        ],
        out_specs=pl.BlockSpec((pieces, tokens, cols), lambda j: (j, 0, 0)),
        out_shape=shape((parts, tokens, cols), BF16),
        scratch_shapes=[pltpu.VMEM((tokens, main + 128), BF16)],
        compiler_params=pltpu.CompilerParams(vmem_limit_bytes=56 * 2**20),
        name="down",
    )(gate, value, tail, edge, ids, cols_aux, taps, weights, weights)
    down = lax.psum_scatter(terms, "tp", scatter_dimension=0, tiled=False)
    return (residual_own + down.astype(F32)).astype(BF16)


def solution(mesh):
    torus = Mesh(mesh.devices.reshape(4, 4, mesh.shape["tp"]), ("z", "x", "tp"))
    placed = (
        P(SP, "tp"),
        P(SP, "tp"),
        P(SP, "tp"),
        P(SP, "tp"),
        P(SP, "tp"),
        P("tp", SP),
        P("tp", SP),
        P(SP),
        P("tp"),
        P("tp", None),
        P(),
        P(SP, "tp"),
        P(SP, "tp"),
        P(None, "tp"),
        P("tp", SP),
    )
    return jax.shard_map(body, mesh=torus, in_specs=placed, out_specs=P(SP, "tp"), check_vma=False)
```

time: 441 us -> 340 us (0.77)
  waiting for transfers between devices: 161 us -> 238 us
  local copies, waits for them, and re-layouts: 80 us -> 13.2 us
  Pallas kernels: 0 us -> 51.5 us
  matrix products: 47.9 us -> 0 us
  other arithmetic: 42.4 us -> 4.13 us
  loops' own time: 38.2 us -> 0 us
  blocking collectives: 27.3 us -> 0 us
  between operations: 37.6 us -> 13.3 us
  starting transfers between devices: 3.91 us -> 19.1 us
    all_gather x2, waiting for transfers between devices: 1.55 us -> 159 us  [the longest x1 128 us: body(): weights = lax.all_gather(packed, SP, axis=0, tiled=True)]
    psum x1 -> x0, waiting for transfers between devices: 109 us -> none  [body(): full_rows = lax.psum(term + placed, 'tp')]
    reduce_scatter x0 -> x2, waiting for transfers between devices: none -> 79.1 us  [the longest x1 40.7 us: body(): down = lax.psum_scatter(terms, 'tp', scatter_dimension=0, tiled=False)]
    pallas_call x0 -> x5, Pallas kernels: none -> 51.5 us  [the longest x1 19.7 us: body(): pl.pallas_call(proj_kernel, grid=(lanes,), in_specs=[whole((parts, tokens...]
    dot_general x7 -> x0, matrix products: 47.9 us -> none  [the longest x1 18.2 us: body(): value = jnp.dot(normed_rows, pieces[1], preferred_element_type=jnp.float32)]
    unnamed x5 -> x4, waiting for transfers between devices: 39.4 us -> 0.07 us
    another operation x1 -> x0, loops' own time: 38.2 us -> none  [body(): local_end, before = lax.scan(advance, empty_state(heads, DH), elements)]
    dynamic_update_slice x48 -> x0, local copies, waits for them, and re-layouts: 33.1 us -> none  [body(): local_end, before = lax.scan(advance, empty_state(heads, DH), elements)]
  transfers between devices with their start and end apart: 5 -> 9, of which waited for: 4 -> 5; matrix products, arithmetic and copies ran while one was open for 9% -> 1% of each run, Pallas kernels for 0% -> 1%
where the time goes in v1:
time: 340 us
  waiting for transfers between devices  238 us (70%)
  Pallas kernels  51.5 us (15%)
  starting transfers between devices  19.1 us (6%)
  between operations  13.3 us (4%)
  local copies, waits for them, and re-layouts  13.2 us (4%)
  other arithmetic  4.13 us (1%)
    all_gather x1, waiting for transfers between devices, body(): weights = lax.all_gather(packed, SP, axis=0, tiled=True)  128 us
    reduce_scatter x1, waiting for transfers between devices, body(): down = lax.psum_scatter(terms, 'tp', scatter_dimension=0, tiled=False)  40.7 us
    reduce_scatter x1, waiting for transfers between devices, body(): attended = lax.psum_scatter(share, 'tp', scatter_dimension=0, tiled=False)  38.4 us
    all_gather x1, waiting for transfers between devices, body(): full = lax.all_gather(residual_own.astype(BF16), 'tp', axis=0, tiled=False)  30.4 us
    pallas_call x1, Pallas kernels, body(): pl.pallas_call(proj_kernel, grid=(lanes,), in_specs=[whole((parts, tokens...  19.7 us
    ppermute x4, starting transfers between devices, body(): lax.ppermute(pay, SP, [(i, i + k) for i in range(count - k)])  15.4 us
    pallas_call x1, Pallas kernels, body(): pl.pallas_call(down_kernel, grid=(parts // pieces,), in_specs=[whole((tok...  15.2 us
    pallas_call x1, Pallas kernels, body(): pl.pallas_call(mix_kernel, grid=(parts,), in_specs=[whole((tokens, width)...  9.33 us
  transfers between devices with their start and end apart: 9, of which 5 were waited for; matrix products, arithmetic and copies ran while one was open for 1% of the time, Pallas kernels for 1%

profile of v1, /device:TPU:0, one launch (start us, length us, event | category | flops | bytes accessed | tf_op | source)
XLA Modules:
  0.0 339.7 jit_solution(9050743885481156214)
XLA Ops:
  6.5 1.3 reshape.13.doc_ref
  7.9 1.9 copy.19.k_ref
  9.7 1.9 copy.20.v_ref
  11.7 3.6 %state.1 = (bf16[112,192]{1,0:T(8,128)(2,1)}, f32[8,768]{1,0:T(8,128)}, f32[768,8]{1,0:T(8,128)}) custom-call(bf16[768,192]{1,0:T(8,128)(2,1)} %copy.19.k_ref, bf16[768,192]{1,0:T(8,128)(2,1)} %copy.20.v_ref, f32[2,768]{1,0:T(2,128)} %in_ref.1, f32[2,768]{1,0:T(2,128)} %forget_ref.1, s32[1,768]{1,0:T(1,128)} %reshape.13.doc_ref), custom_call_target="tpu_custom_call" | custom-call | tf_op jit(solution)/shard_map/state/pallas_call | solution.py:306
  15.3 3.9 %collective-permute-start.3 = (bf16[112,192]{1,0:T(8,128)(2,1)}, bf16[112,192]{1,0:T(8,128)(2,1)S(1)}, u32[]{:S(2)}, u32[]{:S(2)}) collective-permute-start(bf16[112,192]{1,0:T(8,128)(2,1)} %get-tuple-element.15), channel_id=1, source_target_pairs={{0,32},{8,40},{16,48},{24,56},{32,64},{40,72},{48,80},{56,88},{64,... | collective-permute-start | bytes 129032 | tf_op jit(solution)/shard_map/ppermute | solution.py:319
  19.2 4.7 %collective-permute-start.2 = (bf16[112,192]{1,0:T(8,128)(2,1)}, bf16[112,192]{1,0:T(8,128)(2,1)S(1)}, u32[]{:S(2)}, u32[]{:S(2)}) collective-permute-start(bf16[112,192]{1,0:T(8,128)(2,1)} %get-tuple-element.15), channel_id=1, source_target_pairs={{0,24},{8,32},{16,40},{24,48},{32,56},{40,64},{48,72},{56,80},{64,... | collective-permute-start | bytes 129032 | tf_op jit(solution)/shard_map/ppermute | solution.py:319
  23.9 4.1 %collective-permute-start.1 = (bf16[112,192]{1,0:T(8,128)(2,1)}, bf16[112,192]{1,0:T(8,128)(2,1)S(1)}, u32[]{:S(2)}, u32[]{:S(2)}) collective-permute-start(bf16[112,192]{1,0:T(8,128)(2,1)} %get-tuple-element.15), channel_id=1, source_target_pairs={{0,16},{8,24},{16,32},{24,40},{32,48},{40,56},{48,64},{56,72},{64,... | collective-permute-start | bytes 129032 | tf_op jit(solution)/shard_map/ppermute | solution.py:319
  28.0 2.8 collective-permute-start
  30.8 0.9 copy.21.q_ref
  31.7 0.9 copy.22.gate_ref
  32.6 3.6 %local.1.local_ref = f32[768,192]{1,0:T(8,128)} custom-call(bf16[768,192]{1,0:T(8,128)(2,1)} %copy.21.q_ref, bf16[768,192]{1,0:T(8,128)(2,1)} %copy.19.k_ref, bf16[768,192]{1,0:T(8,128)(2,1)} %copy.20.v_ref, f32[8,768]{1,0:T(8,128)} %get-tuple-element.13.row_ref, f32[768,8]{1,0:T(8,128)} %get-tuple-element.14.col_ref.doc_ref), custom_call_target="tpu_custom_call" | custom-call | tf_op jit(solution)/shard_map/local/pallas_call | solution.py:321
  36.2 0.0 collective-permute-done.3.refs_3_
  36.2 0.0 collective-permute-done.2.refs_2_
  36.3 0.0 collective-permute-done.refs_0_
  36.3 0.6 copy-done.5
  36.9 0.0 copy-done.6
  36.9 0.0 copy-done.7
  36.9 0.0 copy-done.8
  36.9 9.3 %mix.1 = (bf16[8,768,384]{2,1,0:T(8,128)(2,1)}, f32[16,128]{1,0:T(8,128)}) custom-call(bf16[768,192]{1,0:T(8,128)(2,1)} %copy.21.q_ref, bf16[768,192]{1,0:T(8,128)(2,1)} %copy.22.gate_ref, f32[768,192]{1,0:T(8,128)} %local.1.local_ref, f32[8,768]{1,0:T(8,128)} %get-tuple-element.13.row_ref, f32[768,8]{1,0:T(8,128)} %get-tuple-element.14.col_ref.doc_ref, ...), custom_call_target="tpu_custom_call" | custom-call | tf_op jit(solution)/shard_map/mix/pallas_call | solution.py:326
  46.3 0.0 reduce-scatter.3.cloned.1.call-update
  46.3 0.0 copy-start.2
  46.3 0.0 all-gather.6.cloned.1.call-start
  46.4 38.4 %reduce-scatter.3.cloned.1.call-done = bf16[1,768,384]{2,1,0:T(8,128)(2,1)} async-done(((bf16[8,768,384]{2,1,0:T(8,128)(2,1)}), bf16[1,768,384]{2,1,0:T(8,128)(2,1)}) %reduce-scatter.3.cloned.1.call-update) | async-done | bytes 589840 | tf_op jit(solution)/shard_map/reduce_scatter | solution.py:347
  84.8 2.0 fusion.1
  86.8 0.0 all-gather.6.cloned.1.call-update
  86.8 0.0 all-gather.4.cloned.1.call-start
  86.9 0.0 slice-start
  86.9 0.0 slice-start.2
  86.9 0.0 slice-start.3
  87.0 0.7 slice-done
  87.7 0.2 slice-done.1
  87.9 0.1 slice-done.3
  88.1 1.8 concatenate.9
  89.8 0.0 all-gather.4.cloned.1.call-update
  89.9 0.0 reduce-scatter.5.cloned.1.call-start
  89.9 30.4 %all-gather.6.cloned.1.call-done = bf16[6144,384]{1,0:T(8,128)(2,1)} async-done(((bf16[768,384]{1,0:T(8,128)(2,1)}), bf16[6144,384]{1,0:T(8,128)(2,1)}) %all-gather.6.cloned.1.call-update) | async-done | bytes 4718608 | tf_op jit(solution)/shard_map/all_gather | solution.py:349
  120.3 128.2 %all-gather.4.cloned.1.call-done.wg_ref.wv_ref.wt_ref.w_ref = bf16[3072,3200]{1,0:T(8,128)(2,1)} async-done(((bf16[192,3200]{1,0:T(8,128)(2,1)}), bf16[3072,3200]{1,0:T(8,128)(2,1)}) %all-gather.4.cloned.1.call-update) | async-done | bytes 19660816 | tf_op jit(solution)/shard_map/all_gather | solution.py:295
  248.6 19.7 %proj.1 = (bf16[768,1024]{1,0:T(8,128)(2,1)}, bf16[768,1024]{1,0:T(8,128)(2,1)}, bf16[768,128]{1,0:T(8,128)(2,1)}) custom-call(bf16[8,768,384]{2,1,0:T(8,128)(2,1)} %bitcast.11, f32[1,3072]{1,0:T(1,128)} %bitcast.14, bf16[3072,3200]{1,0:T(8,128)(2,1)} %all-gather.4.cloned.1.call-done.wg_ref.wv_ref.wt_ref.w_ref, ...), custom_call_target="tpu_custom_call" | custom-call | tf_op jit(solution)/shard_map/proj/pallas_call | solution.py:353
  268.3 0.7 slice.37
  269.0 0.7 slice.36
  269.7 3.5 %collective-permute-start.4 = (bf16[8,1152]{1,0:T(8,128)(2,1)S(1)}, bf16[8,1152]{1,0:T(8,128)(2,1)S(1)}, u32[]{:S(2)}, u32[]{:S(2)}) collective-permute-start(bf16[8,1152]{1,0:T(8,128)(2,1)S(1)} %pad_maximum_fusion), channel_id=1, source_target_pairs={{0,8},{8,16},{16,24},{24,32},{32,40},{40,48},{48,56},{56,64},{64,7... | collective-permute-start | bytes 55304 | tf_op jit(solution)/shard_map/ppermute | solution.py:377
  273.3 0.7 concatenate.11.taps_ref
  274.0 0.5 collective-permute-done.4.edge_ref
  274.6 0.6 copy-done.9
  275.1 15.2 %down.1 = bf16[8,768,384]{2,1,0:T(8,128)(2,1)} custom-call(bf16[768,1024]{1,0:T(8,128)(2,1)} %get-tuple-element.17.gate_ref, bf16[768,1024]{1,0:T(8,128)(2,1)} %get-tuple-element.18.value_ref, bf16[768,128]{1,0:T(8,128)(2,1)} %get-tuple-element.19.tail_ref, bf16[8,1152]{1,0:T(8,128)(2,1)} %copy-done.9, f32[16,128]{1,0:T(8,128)} %get-tuple-element.20.ids_ref, ...), custom_call_target="tpu_custom_call" | custom-call | tf_op jit(solution)/shard_map/down/pallas_call | solution.py:383
  290.3 0.0 reduce-scatter.5.cloned.1.call-update
  290.3 40.7 %reduce-scatter.5.cloned.1.call-done = bf16[1,768,384]{2,1,0:T(8,128)(2,1)} async-done(((bf16[8,768,384]{2,1,0:T(8,128)(2,1)}), bf16[1,768,384]{2,1,0:T(8,128)(2,1)}) %reduce-scatter.5.cloned.1.call-update) | async-done | bytes 589840 | tf_op jit(solution)/shard_map/reduce_scatter | solution.py:403
  331.1 2.1 fusion
  (28 shorter events, 0.1 us)
Async XLA Ops:
  6.5 24.2 %copy-start.3 = (bf16[768,192]{0,1:T(8,128)(2,1)S(1)}, bf16[768,192]{0,1:T(8,128)(2,1)}, u32[]{:S(2)}) copy-start(bf16[768,192]{0,1:T(8,128)(2,1)} %param.16) | copy-start | bytes 884740
  6.5 78.2 %reduce-scatter.3.cloned.1.call-start = ((), (), s32[]{:S(2)}) async-start(), calls=%async_computation.2 | async-start | bytes 5308416 | tf_op jit(solution)/shard_map/reduce_scatter | solution.py:347
  9.7 22.0 %copy-start.4 = (bf16[768,192]{0,1:T(8,128)(2,1)S(1)}, bf16[768,192]{0,1:T(8,128)(2,1)}, u32[]{:S(2)}) copy-start(bf16[768,192]{0,1:T(8,128)(2,1)} %param.19) | copy-start | bytes 884740
  15.3 20.9 %collective-permute-start.3 = (bf16[112,192]{1,0:T(8,128)(2,1)}, bf16[112,192]{1,0:T(8,128)(2,1)S(1)}, u32[]{:S(2)}, u32[]{:S(2)}) collective-permute-start(bf16[112,192]{1,0:T(8,128)(2,1)} %get-tuple-element.15), channel_id=1, source_target_pairs={{0,32},{8,40},{16,48},{24,56},{32,64},{40,72},{48,80},{56,88},{64,... | collective-permute-start | bytes 129032 | tf_op jit(solution)/shard_map/ppermute | solution.py:319
  19.2 17.0 %collective-permute-start.2 = (bf16[112,192]{1,0:T(8,128)(2,1)}, bf16[112,192]{1,0:T(8,128)(2,1)S(1)}, u32[]{:S(2)}, u32[]{:S(2)}) collective-permute-start(bf16[112,192]{1,0:T(8,128)(2,1)} %get-tuple-element.15), channel_id=1, source_target_pairs={{0,24},{8,32},{16,40},{24,48},{32,56},{40,64},{48,72},{56,80},{64,... | collective-permute-start | bytes 129032 | tf_op jit(solution)/shard_map/ppermute | solution.py:319
  23.9 12.4 %collective-permute-start.1 = (bf16[112,192]{1,0:T(8,128)(2,1)}, bf16[112,192]{1,0:T(8,128)(2,1)S(1)}, u32[]{:S(2)}, u32[]{:S(2)}) collective-permute-start(bf16[112,192]{1,0:T(8,128)(2,1)} %get-tuple-element.15), channel_id=1, source_target_pairs={{0,16},{8,24},{16,32},{24,40},{32,48},{40,56},{48,64},{56,72},{64,... | collective-permute-start | bytes 129032 | tf_op jit(solution)/shard_map/ppermute | solution.py:319
  28.0 8.3 %collective-permute-start = (bf16[112,192]{1,0:T(8,128)(2,1)}, bf16[112,192]{1,0:T(8,128)(2,1)S(1)}, u32[]{:S(2)}, u32[]{:S(2)}) collective-permute-start(bf16[112,192]{1,0:T(8,128)(2,1)} %get-tuple-element.15), channel_id=1, source_target_pairs={{0,8},{8,16},{16,24},{24,32},{32,40},{40,48},{48,56},{56,64},{64,7... | collective-permute-start | bytes 129032 | tf_op jit(solution)/shard_map/ppermute | solution.py:319
  36.2 0.6 copy-start.5
  36.2 0.6 copy-start.6
  36.3 0.6 copy-start.7
  36.3 0.6 copy-start.8
  46.3 38.5 %copy-start = (bf16[768,384]{1,0:T(8,128)(2,1)S(1)}, bf16[768,384]{1,0:T(8,128)(2,1)}, u32[]{:S(2)}) copy-start(bf16[768,384]{1,0:T(8,128)(2,1)} %param.15) | copy-start | bytes 1769476
  46.3 40.6 %copy-start.2 = (bf16[1056,192]{0,1:T(8,128)(2,1)S(1)}, bf16[1056,192]{0,1:T(8,128)(2,1)}, u32[]{:S(2)}) copy-start(bf16[1056,192]{0,1:T(8,128)(2,1)} %param.29) | copy-start | bytes 1216516
  46.3 74.0 %all-gather.6.cloned.1.call-start = ((), (), s32[]{:S(2)}) async-start(), calls=%async_computation.5 | async-start | bytes 5308416 | tf_op jit(solution)/shard_map/all_gather | solution.py:349
  86.8 161.8 %all-gather.4.cloned.1.call-start = ((), (), s32[]{:S(2)}) async-start(), calls=%async_computation.3 | async-start | bytes 20889600 | tf_op jit(solution)/shard_map/all_gather | solution.py:295
  86.9 0.8 slice-start
  86.9 1.0 slice-start.1
  86.9 1.0 slice-start.2
  86.9 1.1 slice-start.3
  89.9 241.2 %reduce-scatter.5.cloned.1.call-start = ((), (), s32[]{:S(2)}) async-start(), calls=%async_computation.4 | async-start | bytes 5308416 | tf_op jit(solution)/shard_map/reduce_scatter | solution.py:403
  248.6 24.7 %slice-start.4 = ((f32[3,1056]{1,0:T(4,128)}), f32[3,32]{1,0:T(4,128)S(1)}, s32[]{:S(2)}) async-start(f32[3,1056]{1,0:T(4,128)} %param.28), calls=%async_computation.10 | async-start | bytes 4096 | tf_op jit(solution)/shard_map/slice | solution.py:300
  248.6 24.7 %slice-start.5 = ((f32[3,1056]{1,0:T(4,128)}), f32[3,1024]{1,0:T(4,128)S(1)}, s32[]{:S(2)}) async-start(f32[3,1056]{1,0:T(4,128)} %param.28), calls=%async_computation.11 | async-start | bytes 32768 | tf_op jit(solution)/shard_map/slice | solution.py:298
  269.7 4.8 %collective-permute-start.4 = (bf16[8,1152]{1,0:T(8,128)(2,1)S(1)}, bf16[8,1152]{1,0:T(8,128)(2,1)S(1)}, u32[]{:S(2)}, u32[]{:S(2)}) collective-permute-start(bf16[8,1152]{1,0:T(8,128)(2,1)S(1)} %pad_maximum_fusion), channel_id=1, source_target_pairs={{0,8},{8,16},{16,24},{24,32},{32,40},{40,48},{48,56},{56,64},{64,7... | collective-permute-start | bytes 55304 | tf_op jit(solution)/shard_map/ppermute | solution.py:377
  274.6 0.6 copy-start.9
  290.3 40.8 %copy-start.1 = (bf16[1,768,384]{2,1,0:T(8,128)(2,1)S(1)}, bf16[1,768,384]{2,1,0:T(8,128)(2,1)}, u32[]{:S(2)}) copy-start(bf16[1,768,384]{2,1,0:T(8,128)(2,1)} %reduce-scatter.3.cloned.1.call-done) | copy-start | bytes 1769476
Sparse Core Ops, SparseCore 0:
  46.4 38.3 reduce-scatter.2
  86.9 33.3 all-gather.5
  122.5 126.0 all-gather.3
  290.5 40.5 reduce-scatter.4

commit v2 on v1

v2 whole, which is shorter than its diff:
```python
import jax
import jax.numpy as jnp
from jax import lax
from jax.experimental import pallas as pl
from jax.experimental.pallas import tpu as pltpu
from jax.sharding import Mesh
from jax.sharding import PartitionSpec as P


DH = 96
DOC_MAX = 3072
SP = ("z", "x")
TP = ("y", "c")
ABSENT = -1e30
HALO = 16
EPS = 1e-06
HEAD_FLOOR = 1.0
F32 = jnp.float32
BF16 = jnp.bfloat16


def in_first_head(shape):
    return lax.broadcasted_iota(jnp.int32, shape, len(shape) - 1) < DH


def state_kernel(k_ref, v_ref, in_ref, forget_ref, doc_ref, pay_ref, row_ref, col_ref, scr):
    tokens, width = k_ref.shape
    lane = lax.broadcasted_iota(jnp.int32, (8, tokens), 1)
    doc = jnp.broadcast_to(doc_ref[...].astype(F32), (8, tokens))
    scr[...] = jnp.zeros_like(scr)
    scr[0:2, :] = forget_ref[...]
    raw = scr[...]
    total = jnp.minimum(raw, 0.0) - jnp.log1p(jnp.exp(-jnp.abs(raw)))
    step = 1
    while step < tokens:
        total = total + jnp.where(lane >= step, pltpu.roll(total, step, 1), 0.0)
        step *= 2
    scr[0:2, :] = in_ref[...]
    rest = scr[...] - total
    peak = rest
    step = 1
    while step < tokens:
        near = (lane >= step) & (pltpu.roll(doc, step, 1) == doc)
        peak = jnp.maximum(peak, jnp.where(near, pltpu.roll(peak, step, 1), ABSENT))
        step *= 2
    end_doc = doc[:, tokens - 1 : tokens]
    end_peak = peak[:, tokens - 1 : tokens]
    end_total = total[:, tokens - 1 : tokens]
    weight = jnp.where(doc == end_doc, jnp.exp(jnp.minimum(rest - end_peak, 0.0)), 0.0)
    row_ref[...] = jnp.zeros_like(row_ref)
    row_ref[0:2, :] = total[0:2, :]
    row_ref[2:4, :] = peak[0:2, :]
    row_ref[4:6, :] = weight[0:2, :]
    row_ref[6:7, :] = doc[0:1, :]
    scr[...] = row_ref[...]
    cols = scr[...].T
    col_ref[...] = cols
    row_ref[4:6, :] = rest[0:2, :]
    first = in_first_head((tokens, width))
    spread = jnp.where(first, cols[:, 4:5], cols[:, 5:6])
    weighted = (k_ref[...].astype(F32) * (spread * DH**-0.5)).astype(BF16)
    state = lax.dot_general(
        weighted, v_ref[...], (((0,), (0,)), ((), ())), preferred_element_type=F32
    )
    small = in_first_head((DH, width))
    pay_ref[0:DH, :] = jnp.where(small, state[0:DH, :], state[DH:, :]).astype(BF16)

    line = in_first_head((1, width))

    def spread_heads(x):
        return jnp.where(line, x[0:1, :], x[1:2, :])

    def split(x):
        high = x.astype(BF16).astype(F32)
        mid = (x - high).astype(BF16).astype(F32)
        return high, mid, x - high - mid

    lines = [
        *split(spread_heads(end_total + end_peak)),
        *split(spread_heads(end_total)),
        jnp.broadcast_to(end_doc[0:1, :] + 1.0, (1, width)),
        jnp.broadcast_to(doc[0:1, tokens - 2 : tokens - 1] + 1.0, (1, width)),
    ]
    place = lax.broadcasted_iota(jnp.int32, (16, width), 0)
    table = jnp.zeros((16, width), F32)
    for k, value in enumerate(lines):
        table = jnp.where(place == k, value, table)
    pay_ref[DH:, :] = table.astype(BF16)


def local_kernel(q_ref, k_ref, v_ref, row_ref, col_ref, out_ref):
    tokens, width = q_ref.shape
    block = 256
    for start in range(0, tokens, block):
        stop = start + block
        keys = k_ref[0:stop, :]
        vals = v_ref[0:stop, :]
        q = q_ref[start:stop, :]
        first = in_first_head((block, width))
        at = lax.broadcasted_iota(jnp.int32, (block, stop), 0) + start
        source = lax.broadcasted_iota(jnp.int32, (block, stop), 1)
        seen = (at >= source) & (row_ref[6:7, 0:stop] == col_ref[start:stop, 6:7])
        found = []
        for h in range(2):
            mine = jnp.where(first if h == 0 else jnp.logical_not(first), q, jnp.zeros_like(q))
            scores = lax.dot_general(
                mine, keys, (((1,), (1,)), ((), ())), preferred_element_type=F32
            )
            gap = row_ref[4 + h : 5 + h, 0:stop] - col_ref[start:stop, 2 + h : 3 + h]
            part = (scores * jnp.exp(jnp.where(seen, gap, ABSENT))).astype(BF16)
            found.append(jnp.dot(part, vals, preferred_element_type=F32))
        out_ref[start:stop, :] = jnp.where(first, found[0], found[1])


def mix_kernel(
    order_ref, q_ref, gate_ref, local_ref, row_ref, col_ref, gain_ref, w_ref, *refs
):
    pays, (out_ref, near_ref, far_ref, mix_ref) = refs[:-4], refs[-4:]
    tokens, width = q_ref.shape

    @pl.when(pl.program_id(0) == 0)
    def _():
        own = row_ref[6:7, 0:1] + 1.0
        behind = jnp.zeros((1, width), F32)
        peaks, goods = [], []
        for ref in pays:
            table = ref[DH:, :].astype(F32)
            good = table[6:7, :] == own
            peaks.append(
                jnp.where(good, table[0:1, :] + table[1:2, :] + table[2:3, :] + behind, ABSENT)
            )
            goods.append(good)
            behind = behind + (table[3:4, :] + table[4:5, :] + table[5:6, :])
        best = peaks[0]
        for value in peaks[1:]:
            best = jnp.maximum(best, value)
        state = jnp.zeros((DH, width), F32)
        for ref, value, good in zip(pays, peaks, goods):
            state = state + jnp.where(good, jnp.exp(value - best), 0.0) * ref[0:DH, :].astype(F32)
        small = in_first_head((DH, width))
        whole = jnp.concatenate(
            [jnp.where(small, state, 0.0), jnp.where(small, 0.0, state)], axis=0
        ).astype(BF16)
        carried = jnp.dot(q_ref[...], whole, preferred_element_type=F32)
        first = in_first_head((tokens, width))
        total = jnp.where(first, col_ref[:, 0:1], col_ref[:, 1:2])
        peak = total + jnp.where(first, col_ref[:, 2:3], col_ref[:, 3:4])
        inter = jnp.where(col_ref[:, 6:7] + 1.0 == own, total + best, ABSENT)
        top = jnp.maximum(peak, inter)
        memory = (
            jnp.exp(peak - top) * (local_ref[...] * DH**-0.5) + jnp.exp(inter - top) * carried
        )
        square = memory * memory
        mean_0 = jnp.sum(jnp.where(first, square, 0.0), axis=1, keepdims=True) / DH
        mean_1 = jnp.sum(jnp.where(first, 0.0, square), axis=1, keepdims=True) / DH
        norm = jnp.where(first, lax.rsqrt(mean_0 + HEAD_FLOOR), lax.rsqrt(mean_1 + HEAD_FLOOR))
        gate = gate_ref[...].astype(F32)
        mix_ref[...] = (memory * norm * gain_ref[...] * (1.0 / (1.0 + jnp.exp(-gate)))).astype(BF16)

        ids = pays[0][DH:, :].astype(F32)
        last, second = ids[6:7, 0:1], ids[7:8, 0:1]
        doc = jnp.broadcast_to(col_ref[:, 6:7], (tokens, 128)) + 1.0
        row = lax.broadcasted_iota(jnp.int32, (tokens, 128), 0)
        one = jnp.where(row == 0, last, pltpu.roll(doc, 1, 0))
        two = jnp.where(row == 0, second, jnp.where(row == 1, last, pltpu.roll(doc, 2, 0)))
        near_ref[...] = (one == doc).astype(F32)
        far_ref[...] = (two == doc).astype(F32)

    out_ref[0] = jnp.dot(mix_ref[...], w_ref[...], preferred_element_type=F32).astype(BF16)


def norm_kernel(order_ref, *refs):
    pieces, (gain_ref, out_ref, send_ref) = refs[:-3], refs[-3:]
    tokens, cols = pieces[0].shape
    model = out_ref.shape[1]
    i = pl.program_id(0)
    square = jnp.zeros((tokens, cols), F32)
    for ref in pieces:
        r = ref[...].astype(F32)
        square = square + r * r
    mean = jnp.sum(square, axis=1, keepdims=True) / model
    scale = lax.rsqrt(mean + EPS)
    rows = pl.ds(pl.multiple_of(HALO + i * tokens, 16), tokens)
    for p, ref in enumerate(pieces):
        cut = pl.ds(pl.multiple_of(order_ref[p] * cols, 128), cols)
        done = (ref[...].astype(F32) * scale * gain_ref[0:1, cut]).astype(BF16)
        out_ref[rows, cut] = done
        send_ref[:, cut] = done[tokens - HALO :, :]


def mixer_kernel(
    order_ref,
    x_ref,
    near_ref,
    far_ref,
    taps_ref,
    wg_ref,
    wv_ref,
    wt_ref,
    wda_ref,
    wdb_ref,
    wdta_ref,
    wdtb_ref,
    out_ref,
    gate_scr,
    value_scr,
    h_scr,
):
    tokens = near_ref.shape[0]
    tiles, _, tile = taps_ref.shape
    tiles -= 1
    main = tiles * tile
    j = pl.program_id(0)

    def hidden(gate, value, taps, rows):
        near, far = near_ref[rows, :], far_ref[rows, :]
        one = pltpu.roll(gate, 1, 0)[HALO:, :]
        two = pltpu.roll(gate, 2, 0)[HALO:, :]
        conv = (
            taps[2:3, :] * gate[HALO:, :]
            + taps[1:2, :] * (near * one)
            + taps[0:1, :] * (far * two)
        )
        return conv / (1.0 + jnp.exp(-conv)) * value

    block = 96

    def finish(slot, at):
        for start in range(0, tokens, block):
            for half in range(0, tile, 128):
                lanes = slice(half, half + 128)
                done = hidden(
                    gate_scr[slot, start : start + block + HALO, lanes].astype(F32),
                    value_scr[slot, start + HALO : start + HALO + block, lanes].astype(F32),
                    taps_ref[at, :, lanes],
                    slice(start, start + block),
                )
                spot = pl.multiple_of(at * tile + half, 128)
                h_scr[start : start + block, pl.ds(spot, 128)] = done.astype(BF16)

    @pl.when(j < tiles)
    def _():
        gate_scr[j % 2] = jnp.dot(x_ref[...], wg_ref[...], preferred_element_type=F32).astype(BF16)
        value_scr[j % 2] = jnp.dot(x_ref[...], wv_ref[...], preferred_element_type=F32).astype(BF16)

    @pl.when((j > 0) & (j <= tiles))
    def _():
        finish((j - 1) % 2, j - 1)

    @pl.when(j == tiles)
    def _():
        both = jnp.dot(x_ref[...], wt_ref[...], preferred_element_type=F32).astype(BF16)
        for start in range(0, tokens, block):
            part = both[start : start + block + HALO, :].astype(F32)
            lane = lax.broadcasted_iota(jnp.int32, (block, 128), 1)
            mine = (lane >= 64) & (lane < 96)
            done = hidden(
                pltpu.roll(part, 64, 1),
                pltpu.roll(part, 32, 1)[HALO:, :],
                taps_ref[tiles, :, 0:128],
                slice(start, start + block),
            )
            h_scr[start : start + block, main:] = jnp.where(mine, done, 0.0).astype(BF16)

    @pl.when(j > tiles)
    def _():
        contract = (((1,), (1,)), ((), ()))
        for p, (wd_ref, wdt_ref) in enumerate(((wda_ref, wdta_ref), (wdb_ref, wdtb_ref))):
            out_ref[p] = (
                lax.dot_general(h_scr[:, 0:main], wd_ref[...], contract, preferred_element_type=F32)
                + lax.dot_general(
                    h_scr[:, main:], wdt_ref[...], contract, preferred_element_type=F32
                )
            ).astype(BF16)


def added(*terms):
    total = terms[0].astype(F32)
    for term in terms[1:]:
        total = total + term.astype(F32)
    return total


def shifted(value, by):
    ring = lax.axis_size("y")
    return lax.ppermute(value, "y", [(i, (i + by) % ring) for i in range(ring)])


def swapped(value):
    return lax.ppermute(value, "c", [(0, 1), (1, 0)])


def summed_over_tp(shares):
    half = shares.shape[2] // 2
    other = swapped(shares[1])
    pair = [added(shares[0, k], other[k]).astype(BF16) for k in range(4)]
    up = shifted(pair[2][:half], 1)
    down = shifted(pair[2][half:], -1)
    up = jnp.concatenate([added(pair[1][:half], up).astype(BF16), pair[1][half:]], axis=0)
    down = jnp.concatenate([pair[3][:half], added(pair[3][half:], down).astype(BF16)], axis=0)
    return added(pair[0], shifted(up, 1), shifted(down, -1))


def gathered_over_tp(own):
    half = own.shape[0] // 2
    below, above = shifted(own, 1), shifted(own, -1)
    far = jnp.concatenate([shifted(below[:half], 1), shifted(above[half:], -1)], axis=0)
    mine = [own, below, above, far]
    return mine + [swapped(part) for part in mine]


def shape(dims, dtype):
    return jax.ShapeDtypeStruct(dims, dtype)


def whole(dims):
    return pl.BlockSpec(dims, lambda *_: (0,) * len(dims))


def layer(
    resid,
    query,
    keys,
    values,
    out_gate,
    in_gate,
    forget,
    doc_ids,
    head_gain,
    w_out,
    ffn_gain,
    w_gate,
    w_value,
    conv_taps,
    w_down,
):
    tokens, width = query.shape
    cols = resid.shape[1]
    parts = w_out.shape[1] // cols
    model = w_out.shape[1]
    hidden = w_gate.shape[1]
    main = hidden // 128 * 128
    spare = hidden - main
    down_t = w_down.T
    packed = jnp.concatenate(
        [
            w_gate[:, :main],
            w_value[:, :main],
            down_t[:, :main],
            w_gate[:, main:],
            w_value[:, main:],
            down_t[:, main:],
            jnp.zeros((w_gate.shape[0], 128 - 3 * spare), BF16),
        ],
        axis=1,
    )
    weights = lax.all_gather(packed, SP, axis=0, tiled=True)
    tile = 256
    tiles = main // tile
    spot = 2 * spare
    taps = jnp.concatenate(
        [
            jnp.swapaxes(conv_taps[:, :main].reshape(3, tiles, tile), 0, 1),
            jnp.pad(conv_taps[:, main:], ((0, 0), (spot, tile - spot - spare)))[None],
        ],
        axis=0,
    )

    pay, rows, cols_aux = pl.pallas_call(
        state_kernel,
        out_shape=(
            shape((DH + 16, width), BF16),
            shape((8, tokens), F32),
            shape((tokens, 8), F32),
        ),
        scratch_shapes=[pltpu.VMEM((8, tokens), F32)],
        name="state",
    )(keys, values, in_gate, forget, doc_ids.reshape(1, tokens))
    count = lax.axis_size(SP)
    reach = -(-(DOC_MAX - 1) // tokens)
    pays = [
        lax.ppermute(pay, SP, [(i, i + k) for i in range(count - k)]) for k in range(1, reach + 1)
    ]
    local = pl.pallas_call(
        local_kernel,
        out_shape=shape((tokens, width), F32),
        name="local",
    )(query, keys, values, rows, cols_aux)
    chip, core = lax.axis_index("y"), lax.axis_index("c")
    ring, cores = lax.axis_size("y"), lax.axis_size("c")
    chips = (chip + jnp.arange(ring, dtype=jnp.int32)) % ring
    sides = core ^ jnp.arange(cores, dtype=jnp.int32)
    order = (chips[None, :] * cores + sides[:, None]).reshape(-1)
    share, near, far = pl.pallas_call(
        mix_kernel,
        grid_spec=pltpu.PrefetchScalarGridSpec(
            num_scalar_prefetch=1,
            grid=(parts,),
            in_specs=[
                whole((tokens, width)),
                whole((tokens, width)),
                whole((tokens, width)),
                whole((8, tokens)),
                whole((tokens, 8)),
                whole((1, width)),
                pl.BlockSpec((width, cols), lambda j, order: (0, order[j])),
                *[whole((DH + 16, width)) for _ in pays],
            ],
            out_specs=(
                pl.BlockSpec((1, tokens, cols), lambda j, order: (j, 0, 0)),
                whole((tokens, 128)),
                whole((tokens, 128)),
            ),
            scratch_shapes=[pltpu.VMEM((tokens, width), BF16)],
        ),
        out_shape=(
            shape((parts, tokens, cols), BF16),
            shape((tokens, 128), F32),
            shape((tokens, 128), F32),
        ),
        name="mix",
    )(order, query, out_gate, local, rows, cols_aux, head_gain.reshape(1, width), w_out, *pays)
    attended = summed_over_tp(share.reshape(cores, ring, tokens, cols))
    residual_own = resid.astype(F32) + attended
    pieces = gathered_over_tp(residual_own.astype(BF16))
    came = (chip + jnp.array([0, -1, 1, 2], jnp.int32)) % ring
    places = (came[None, :] * cores + sides[:, None]).reshape(-1)
    block = 96
    normed, send = pl.pallas_call(
        norm_kernel,
        grid_spec=pltpu.PrefetchScalarGridSpec(
            num_scalar_prefetch=1,
            grid=(tokens // block,),
            in_specs=[
                *[pl.BlockSpec((block, cols), lambda i, places: (i, 0)) for _ in pieces],
                whole((1, model)),
            ],
            out_specs=(whole((tokens + HALO, model)), whole((HALO, model))),
        ),
        out_shape=(shape((tokens + HALO, model), BF16), shape((HALO, model), BF16)),
        compiler_params=pltpu.CompilerParams(vmem_limit_bytes=40 * 2**20),
        name="norm",
    )(places, *pieces, ffn_gain.reshape(1, model))
    edge = lax.ppermute(send, SP, [(i, i + 1) for i in range(count - 1)])
    normed = lax.dynamic_update_slice(normed, edge, (0, 0))
    first = tiles + 1
    tail_at = 3 * main // 128

    def down_at(k, col):
        return lambda j, order: (order[2 * jnp.maximum(j - first, 0) + k], col)

    terms = pl.pallas_call(
        mixer_kernel,
        grid_spec=pltpu.PrefetchScalarGridSpec(
            num_scalar_prefetch=1,
            grid=(first + parts // 2,),
            in_specs=[
                pl.BlockSpec(
                    (tokens + HALO, model), lambda j, order: (0, 0), pipeline_mode=pl.Buffered(1)
                ),
                whole((tokens, 128)),
                whole((tokens, 128)),
                whole((tiles + 1, 3, tile)),
                pl.BlockSpec((model, tile), lambda j, order: (0, jnp.minimum(j, tiles - 1))),
                pl.BlockSpec(
                    (model, tile), lambda j, order: (0, tiles + jnp.minimum(j, tiles - 1))
                ),
                pl.BlockSpec((model, 128), lambda j, order: (0, tail_at)),
                pl.BlockSpec((cols, main), down_at(0, 2)),
                pl.BlockSpec((cols, main), down_at(1, 2)),
                pl.BlockSpec((cols, 128), down_at(0, tail_at)),
                pl.BlockSpec((cols, 128), down_at(1, tail_at)),
            ],
            out_specs=pl.BlockSpec(
                (2, tokens, cols), lambda j, order: (jnp.maximum(j - first, 0), 0, 0)
            ),
            scratch_shapes=[
                pltpu.VMEM((2, tokens + HALO, tile), BF16),
                pltpu.VMEM((2, tokens + HALO, tile), BF16),
                pltpu.VMEM((tokens, main + 128), BF16),
            ],
        ),
        out_shape=shape((parts, tokens, cols), BF16),
        compiler_params=pltpu.CompilerParams(vmem_limit_bytes=56 * 2**20),
        name="mixer",
    )(order, normed, near, far, taps, *[weights] * 7)
    down = summed_over_tp(terms.reshape(cores, ring, tokens, cols))
    return (residual_own + down).astype(BF16)


def solution(mesh):
    torus = Mesh(mesh.devices.reshape(4, 4, 4, 2), ("z", "x", "y", "c"))
    placed = (
        P(SP, TP),
        P(SP, TP),
        P(SP, TP),
        P(SP, TP),
        P(SP, TP),
        P(TP, SP),
        P(TP, SP),
        P(SP),
        P(TP),
        P(TP, None),
        P(),
        P(SP, TP),
        P(SP, TP),
        P(None, TP),
        P(TP, SP),
    )
    return jax.shard_map(layer, mesh=torus, in_specs=placed, out_specs=P(SP, TP), check_vma=False)
```

time: 340 us -> 217 us (0.64)
  waiting for transfers between devices: 238 us -> 82.5 us
  starting transfers between devices: 19.1 us -> 40 us
  local copies, waits for them, and re-layouts: 13.2 us -> 18 us
  Pallas kernels: 51.5 us -> 56 us
    all_gather x2 -> x1, waiting for transfers between devices: 159 us -> 14 us  [layer(): weights = lax.all_gather(packed, SP, axis=0, tiled=True)]
    reduce_scatter x2 -> x0, waiting for transfers between devices: 79.1 us -> none  [the longest x1 40.7 us: body(): down = lax.psum_scatter(terms, 'tp', scatter_dimension=0, tiled=False)]
    ppermute x5 -> x23, waiting for transfers between devices: 0.55 us -> 68.5 us  [the longest x12 54.9 us: shifted(): return lax.ppermute(value, 'y', [(i, (i + by) % ring) for i in range(ring)])]
    ppermute x5 -> x23, starting transfers between devices: 19 us -> 40 us  [the longest x12 20.1 us: shifted(): return lax.ppermute(value, 'y', [(i, (i + by) % ring) for i in range(ring)])]
    pallas_call x5, Pallas kernels: 51.5 us -> 56 us  [the longest x1 30.4 us: layer(): pl.pallas_call(mixer_kernel, grid_spec=pltpu.PrefetchScalarGridSpec(num_s...]
    slice x16 -> x23, local copies, waits for them, and re-layouts: 2.53 us -> 6.87 us  [the longest x2 4.11 us: summed_over_tp(): other = swapped(shares[1])]
    unnamed x24 -> x47, local copies, waits for them, and re-layouts: 6.91 us -> 6.02 us
  transfers between devices with their start and end apart: 9 -> 24, of which waited for: 5 -> 11; matrix products, arithmetic and copies ran while one was open for 1% -> 6% of each run, Pallas kernels for 1% -> 12%
where the time goes in v2:
time: 217 us; the launch traced here: 216 us
  waiting for transfers between devices  82.5 us (38%)
  Pallas kernels  56 us (26%)
  starting transfers between devices  40 us (18%)
  local copies, waits for them, and re-layouts  18 us (8%)
  between operations  13.8 us (6%)
  other arithmetic  5.84 us (3%)
    ppermute x12, waiting for transfers between devices, shifted(): return lax.ppermute(value, 'y', [(i, (i + by) % ring) for i in range(ring)])  54.9 us
    pallas_call x1, Pallas kernels, layer(): pl.pallas_call(mixer_kernel, grid_spec=pltpu.PrefetchScalarGridSpec(num_s...  30.4 us
    ppermute x12, starting transfers between devices, shifted(): return lax.ppermute(value, 'y', [(i, (i + by) % ring) for i in range(ring)])  20.1 us
    ppermute x4, starting transfers between devices, layer(): lax.ppermute(pay, SP, [(i, i + k) for i in range(count - k)])  16.7 us
    all_gather x1, waiting for transfers between devices, layer(): weights = lax.all_gather(packed, SP, axis=0, tiled=True)  14 us
    pallas_call x1, Pallas kernels, layer(): pl.pallas_call(mix_kernel, grid_spec=pltpu.PrefetchScalarGridSpec(num_sca...  10.3 us
    ppermute x6, waiting for transfers between devices, swapped(): return lax.ppermute(value, 'c', [(0, 1), (1, 0)])  9.22 us
    pallas_call x1, Pallas kernels, layer(): pl.pallas_call(norm_kernel, grid_spec=pltpu.PrefetchScalarGridSpec(num_sc...  8.14 us
  transfers between devices with their start and end apart: 24, of which 11 were waited for; matrix products, arithmetic and copies ran while one was open for 6% of the time, Pallas kernels for 12%

profile of v2, /device:TPU:0, one launch (start us, length us, event | category | flops | bytes accessed | tf_op | source)
XLA Modules:
  0.0 216.1 jit_solution(15397757551611329547)
XLA Ops:
  6.5 1.1 slice.178
  7.6 0.8 slice.179
  8.5 1.8 concatenate.25
  10.3 0.9 copy-done.10
  11.2 1.0 copy.20.k_ref
  12.2 0.9 copy.21.v_ref
  13.1 0.6 reshape.85.doc_ref
  13.7 3.6 %state.1 = (bf16[112,192]{1,0:T(8,128)(2,1)}, f32[8,768]{1,0:T(8,128)}, f32[768,8]{1,0:T(8,128)}) custom-call(bf16[768,192]{1,0:T(8,128)(2,1)} %copy.20.k_ref, bf16[768,192]{1,0:T(8,128)(2,1)} %copy.21.v_ref, f32[2,768]{1,0:T(2,128)} %in_ref.1, f32[2,768]{1,0:T(2,128)} %forget_ref.1, s32[1,768]{1,0:T(1,128)} %reshape.85.doc_ref), custom_call_target="tpu_custom_call" | custom-call | tf_op jit(solution)/shard_map/state/pallas_call | solution.py:369
  17.3 3.5 %collective-permute-start = (bf16[112,192]{1,0:T(8,128)(2,1)}, bf16[112,192]{1,0:T(8,128)(2,1)S(1)}, u32[]{:S(2)}, u32[]{:S(2)}) collective-permute-start(bf16[112,192]{1,0:T(8,128)(2,1)} %get-tuple-element.15), channel_id=1, source_target_pairs={{0,8},{8,16},{16,24},{24,32},{32,40},{40,48},{48,56},{56,64},{64,7... | collective-permute-start | bytes 129032 | tf_op jit(solution)/shard_map/ppermute | solution.py:382
  20.8 4.6 %collective-permute-start.1 = (bf16[112,192]{1,0:T(8,128)(2,1)}, bf16[112,192]{1,0:T(8,128)(2,1)S(1)}, u32[]{:S(2)}, u32[]{:S(2)}) collective-permute-start(bf16[112,192]{1,0:T(8,128)(2,1)} %get-tuple-element.15), channel_id=1, source_target_pairs={{0,16},{8,24},{16,32},{24,40},{32,48},{40,56},{48,64},{56,72},{64,... | collective-permute-start | bytes 129032 | tf_op jit(solution)/shard_map/ppermute | solution.py:382
  25.5 4.7 %collective-permute-start.2 = (bf16[112,192]{1,0:T(8,128)(2,1)}, bf16[112,192]{1,0:T(8,128)(2,1)S(1)}, u32[]{:S(2)}, u32[]{:S(2)}) collective-permute-start(bf16[112,192]{1,0:T(8,128)(2,1)} %get-tuple-element.15), channel_id=1, source_target_pairs={{0,24},{8,32},{16,40},{24,48},{32,56},{40,64},{48,72},{56,80},{64,... | collective-permute-start | bytes 129032 | tf_op jit(solution)/shard_map/ppermute | solution.py:382
  30.2 3.8 %collective-permute-start.3 = (bf16[112,192]{1,0:T(8,128)(2,1)}, bf16[112,192]{1,0:T(8,128)(2,1)S(1)}, u32[]{:S(2)}, u32[]{:S(2)}) collective-permute-start(bf16[112,192]{1,0:T(8,128)(2,1)} %get-tuple-element.15), channel_id=1, source_target_pairs={{0,32},{8,40},{16,48},{24,56},{32,64},{40,72},{48,80},{56,88},{64,... | collective-permute-start | bytes 129032 | tf_op jit(solution)/shard_map/ppermute | solution.py:382
  34.0 0.6 broadcast_add_fusion
  34.6 0.9 copy.22.q_ref
  35.5 0.6 add.122.order_ref
  36.2 0.9 copy.23.gate_ref
  37.1 3.6 %local.1.local_ref = f32[768,192]{1,0:T(8,128)} custom-call(bf16[768,192]{1,0:T(8,128)(2,1)} %copy.22.q_ref, bf16[768,192]{1,0:T(8,128)(2,1)} %copy.20.k_ref, bf16[768,192]{1,0:T(8,128)(2,1)} %copy.21.v_ref, f32[8,768]{1,0:T(8,128)} %get-tuple-element.13.row_ref, f32[768,8]{1,0:T(8,128)} %get-tuple-element.14.col_ref), custom_call_target="tpu_custom_call" | custom-call | tf_op jit(solution)/shard_map/local/pallas_call | solution.py:384
  40.8 0.6 copy-done.15
  41.4 10.3 %mix.1 = (bf16[8,768,384]{2,1,0:T(8,128)(2,1)}, f32[768,128]{1,0:T(8,128)}, f32[768,128]{1,0:T(8,128)}) custom-call(s32[8]{0:T(128)} %add.122.order_ref, bf16[768,192]{1,0:T(8,128)(2,1)} %copy.22.q_ref, bf16[768,192]{1,0:T(8,128)(2,1)} %copy.23.gate_ref, f32[768,192]{1,0:T(8,128)} %local.1.local_ref, f32[8,768]{1,0:T(8,128)} %get-tuple-element.13.row_ref, ...), custom_call_target="tpu_custom_call" | custom-call | tf_op jit(solution)/shard_map/mix/pallas_call | solution.py:394
  51.7 2.1 slice.123
  53.9 4.5 %collective-permute-done.4 = bf16[4,768,384]{2,1,0:T(8,128)(2,1)S(1)} collective-permute-done((bf16[4,768,384]{2,1,0:T(8,128)(2,1)S(1)}, bf16[4,768,384]{2,1,0:T(8,128)(2,1)S(1)}, u32[]{:S(2)}, u32[]{:S(2)}) %collective-permute-start.4) | collective-permute-done | bytes 2359328 | tf_op jit(solution)/shard_map/ppermute | solution.py:290
  58.9 1.7 collective-permute-start.5
  60.7 1.7 collective-permute-start.7
  62.4 7.0 %collective-permute-done.5 = bf16[384,384]{1,0:T(8,128)(2,1)S(1)} collective-permute-done((bf16[384,384]{1,0:T(8,128)(2,1)S(1)}, bf16[384,384]{1,0:T(8,128)(2,1)S(1)}, u32[]{:S(2)}, u32[]{:S(2)}) %collective-permute-start.5) | collective-permute-done | bytes 294944 | tf_op jit(solution)/shard_map/ppermute | solution.py:286
  70.0 3.0 %collective-permute-start.8 = (bf16[768,384]{1,0:T(8,128)(2,1)S(1)}, bf16[768,384]{1,0:T(8,128)(2,1)S(1)}, u32[]{:S(2)}, u32[]{:S(2)}) collective-permute-start(bf16[768,384]{1,0:T(8,128)(2,1)S(1)} %pad_maximum_fusion.1), channel_id=1, source_target_pairs={{0,6},{2,0},{4,2},{6,4},{1,7},{3,1},{5,3},{7,5},{8,14},{10,8},{12,... | collective-permute-start | bytes 1769480 | tf_op jit(solution)/shard_map/ppermute | solution.py:286
  73.1 12.5 %collective-permute-done.6 = bf16[768,384]{1,0:T(8,128)(2,1)S(1)} collective-permute-done((bf16[768,384]{1,0:T(8,128)(2,1)S(1)}, bf16[768,384]{1,0:T(8,128)(2,1)S(1)}, u32[]{:S(2)}, u32[]{:S(2)}) %collective-permute-start.6) | collective-permute-done | bytes 589856 | tf_op jit(solution)/shard_map/ppermute | solution.py:286
  86.9 3.0 %collective-permute-start.10 = (bf16[768,384]{1,0:T(8,128)(2,1)S(1)}, bf16[768,384]{1,0:T(8,128)(2,1)S(1)}, u32[]{:S(2)}, u32[]{:S(2)}) collective-permute-start(bf16[768,384]{1,0:T(8,128)(2,1)S(1)} %fusion.12.refs_0_), channel_id=1, source_target_pairs={{0,6},{2,0},{4,2},{6,4},{1,7},{3,1},{5,3},{7,5},{8,14},{10,8},{12,... | collective-permute-start | bytes 1769480 | tf_op jit(solution)/shard_map/ppermute | solution.py:286
  89.8 12.0 %collective-permute-done.9.refs_1_ = bf16[768,384]{1,0:T(8,128)(2,1)S(1)} collective-permute-done((bf16[768,384]{1,0:T(8,128)(2,1)S(1)}, bf16[768,384]{1,0:T(8,128)(2,1)S(1)}, u32[]{:S(2)}, u32[]{:S(2)}) %collective-permute-start.9) | collective-permute-done | bytes 589856 | tf_op jit(solution)/shard_map/ppermute | solution.py:286
  102.0 3.3 %collective-permute-start.12 = (bf16[384,384]{1,0:T(8,128)(2,1)S(1)}, bf16[384,384]{1,0:T(8,128)(2,1)S(1)}, u32[]{:S(2)}, u32[]{:S(2)}) collective-permute-start(bf16[384,384]{1,0:T(8,128)(2,1)S(1)} %slice.177), channel_id=1, source_target_pairs={{0,6},{2,0},{4,2},{6,4},{1,7},{3,1},{5,3},{7,5},{8,14},{10,8},{12,... | collective-permute-start | bytes 884744 | tf_op jit(solution)/shard_map/ppermute | solution.py:286
  105.8 4.3 %collective-permute-done.11 = bf16[384,384]{1,0:T(8,128)(2,1)S(1)} collective-permute-done((bf16[384,384]{1,0:T(8,128)(2,1)S(1)}, bf16[384,384]{1,0:T(8,128)(2,1)S(1)}, u32[]{:S(2)}, u32[]{:S(2)}) %collective-permute-start.11) | collective-permute-done | bytes 294944 | tf_op jit(solution)/shard_map/ppermute | solution.py:286
  110.2 0.5 slice.140
  110.8 0.7 add.136.order_ref
  111.5 0.7 pad_bitcast_fusion
  112.4 8.1 %norm.1 = (bf16[784,3072]{1,0:T(8,128)(2,1)}, bf16[16,3072]{1,0:T(8,128)(2,1)S(1)}) custom-call(s32[8]{0:T(128)S(1)} %add.136.order_ref, bf16[768,384]{1,0:T(8,128)(2,1)S(1)} %fusion.12.refs_0_, bf16[768,384]{1,0:T(8,128)(2,1)S(1)} %collective-permute-done.9.refs_1_, bf16[768,384]{1,0:T(8,128)(2,1)S(1)} %collective-permute-done.10.refs_2_, ...), custom_call_target="tpu_custom_call" | custom-call | tf_op jit(solution)/shard_map/norm/pallas_call | solution.py:429
  120.5 2.4 %collective-permute-start.17 = (bf16[16,3072]{1,0:T(8,128)(2,1)S(1)}, bf16[16,3072]{1,0:T(8,128)(2,1)S(1)}, u32[]{:S(2)}, u32[]{:S(2)}) collective-permute-start(bf16[16,3072]{1,0:T(8,128)(2,1)S(1)} %get-tuple-element.18), channel_id=1, source_target_pairs={{0,8},{8,16},{16,24},{24,32},{32,40},{40,48},{48,56},{56,64},{64,7... | collective-permute-start | bytes 294920 | tf_op jit(solution)/shard_map/ppermute | solution.py:444
  123.0 0.6 pad_maximum_fusion.4.taps_ref
  123.6 4.3 %collective-permute-done.17 = bf16[16,3072]{1,0:T(8,128)(2,1)S(1)} collective-permute-done((bf16[16,3072]{1,0:T(8,128)(2,1)S(1)}, bf16[16,3072]{1,0:T(8,128)(2,1)S(1)}, u32[]{:S(2)}, u32[]{:S(2)}) %collective-permute-start.17) | collective-permute-done | bytes 98336 | tf_op jit(solution)/shard_map/ppermute | solution.py:444
  127.9 0.6 constant_dynamic-update-slice_fusion.2.x_ref
  128.5 14.0 %all-gather.2.cloned.1.call-done.wg_ref.wv_ref.wt_ref.wda_ref.wdb_ref.wdta_ref.wdtb_ref = bf16[3072,3200]{1,0:T(8,128)(2,1)} async-done(((bf16[192,3200]{1,0:T(8,128)(2,1)}), bf16[3072,3200]{1,0:T(8,128)(2,1)}) %all-gather.2.cloned.1.call-update) | async-done | bytes 19660816 | tf_op jit(solution)/shard_map/all_gather | solution.py:357
  142.6 30.4 %mixer.1 = bf16[8,768,384]{2,1,0:T(8,128)(2,1)} custom-call(s32[8]{0:T(128)} %add.122.order_ref, bf16[784,3072]{1,0:T(8,128)(2,1)} %constant_dynamic-update-slice_fusion.2.x_ref, f32[768,128]{1,0:T(8,128)} %get-tuple-element.19.near_ref, f32[768,128]{1,0:T(8,128)} %get-tuple-element.20.far_ref, f32[5,3,256]{2,1,0:T(4,128)} %pad_maximum_fusion.4.taps_ref, ...), custom_call_target="tpu_custom_call" | custom-call | tf_op jit(solution)/shard_map/mixer/pallas_call | solution.py:452
  173.0 2.1 slice.181
  175.1 4.5 %collective-permute-done.18 = bf16[4,768,384]{2,1,0:T(8,128)(2,1)S(1)} collective-permute-done((bf16[4,768,384]{2,1,0:T(8,128)(2,1)S(1)}, bf16[4,768,384]{2,1,0:T(8,128)(2,1)S(1)}, u32[]{:S(2)}, u32[]{:S(2)}) %collective-permute-start.18) | collective-permute-done | bytes 2359328 | tf_op jit(solution)/shard_map/ppermute | solution.py:290
  180.2 1.6 collective-permute-start.19
  181.8 1.8 collective-permute-start.21
  183.6 6.9 %collective-permute-done.19 = bf16[384,384]{1,0:T(8,128)(2,1)S(1)} collective-permute-done((bf16[384,384]{1,0:T(8,128)(2,1)S(1)}, bf16[384,384]{1,0:T(8,128)(2,1)S(1)}, u32[]{:S(2)}, u32[]{:S(2)}) %collective-permute-start.19) | collective-permute-done | bytes 294944 | tf_op jit(solution)/shard_map/ppermute | solution.py:286
  191.2 3.0 %collective-permute-start.22 = (bf16[768,384]{1,0:T(8,128)(2,1)S(1)}, bf16[768,384]{1,0:T(8,128)(2,1)S(1)}, u32[]{:S(2)}, u32[]{:S(2)}) collective-permute-start(bf16[768,384]{1,0:T(8,128)(2,1)S(1)} %pad_maximum_fusion.3), channel_id=1, source_target_pairs={{0,6},{2,0},{4,2},{6,4},{1,7},{3,1},{5,3},{7,5},{8,14},{10,8},{12,... | collective-permute-start | bytes 1769480 | tf_op jit(solution)/shard_map/ppermute | solution.py:286
  194.2 12.3 %collective-permute-done.20 = bf16[768,384]{1,0:T(8,128)(2,1)S(1)} collective-permute-done((bf16[768,384]{1,0:T(8,128)(2,1)S(1)}, bf16[768,384]{1,0:T(8,128)(2,1)S(1)}, u32[]{:S(2)}, u32[]{:S(2)}) %collective-permute-start.20) | collective-permute-done | bytes 589856 | tf_op jit(solution)/shard_map/ppermute | solution.py:286
  206.5 2.7 %add_convert_fusion = bf16[768,384]{1,0:T(8,128)(2,1)} fusion(bf16[768,384]{1,0:T(8,128)(2,1)S(1)} %collective-permute-done.22, bf16[768,384]{1,0:T(8,128)(2,1)S(1)} %collective-permute-done.20, bf16[4,768,384]{2,1,0:T(8,128)(2,1)S(1)} %collective-permute-done.18, bf16[2,4,768,384]{3,2,1,0:T(8,128)(2,1)S(1)} %bitcast.100, bf16[768,384]{1,0:T(8,128)(2,1)S(1)} %copy-done.9, ...), kind=kLoop, calls=%fused_computation.16 | loop fusion | flops 6488064 | bytes 5898240 | tf_op jit(solution)/shard_map/convert_element_type | solution.py:488
  (100 shorter events, 5.1 us)
Async XLA Ops:
  6.5 136.0 %all-gather.2.cloned.1.call-start = ((), (), s32[]{:S(2)}) async-start(), calls=%async_computation | async-start | bytes 20889600 | tf_op jit(solution)/shard_map/all_gather | solution.py:357
  6.5 1.9 slice-start
  6.5 1.9 slice-start.1
  6.5 1.9 slice-start.2
  6.5 2.0 slice-start.3
  10.3 1.0 copy-start.10
  10.3 1.9 copy-start.11
  10.3 2.8 %copy-start.19 = (s32[768]{0:T(1024)S(1)}, s32[768]{0:T(1024)}, u32[]{:S(2)}) copy-start(s32[768]{0:T(1024)} %param.23) | copy-start | bytes 9220
  11.2 22.8 %copy-start.20 = (s32[4]{0:T(128)S(1)}, s32[4]{0:T(128)}, u32[]{:S(2)}) copy-start(s32[4]{0:T(128)} %constant.37.clone) | copy-start | bytes 52
  11.2 23.4 %copy-start.12 = (bf16[768,192]{0,1:T(8,128)(2,1)S(1)}, bf16[768,192]{0,1:T(8,128)(2,1)}, u32[]{:S(2)}) copy-start(bf16[768,192]{0,1:T(8,128)(2,1)} %param.17) | copy-start | bytes 884740
  12.2 24.0 %copy-start.13 = (bf16[768,192]{0,1:T(8,128)(2,1)S(1)}, bf16[768,192]{0,1:T(8,128)(2,1)}, u32[]{:S(2)}) copy-start(bf16[768,192]{0,1:T(8,128)(2,1)} %param.20) | copy-start | bytes 884740
  17.3 23.4 %collective-permute-start = (bf16[112,192]{1,0:T(8,128)(2,1)}, bf16[112,192]{1,0:T(8,128)(2,1)S(1)}, u32[]{:S(2)}, u32[]{:S(2)}) collective-permute-start(bf16[112,192]{1,0:T(8,128)(2,1)} %get-tuple-element.15), channel_id=1, source_target_pairs={{0,8},{8,16},{16,24},{24,32},{32,40},{40,48},{48,56},{56,64},{64,7... | collective-permute-start | bytes 129032 | tf_op jit(solution)/shard_map/ppermute | solution.py:382
  20.8 19.9 %collective-permute-start.1 = (bf16[112,192]{1,0:T(8,128)(2,1)}, bf16[112,192]{1,0:T(8,128)(2,1)S(1)}, u32[]{:S(2)}, u32[]{:S(2)}) collective-permute-start(bf16[112,192]{1,0:T(8,128)(2,1)} %get-tuple-element.15), channel_id=1, source_target_pairs={{0,16},{8,24},{16,32},{24,40},{32,48},{40,56},{48,64},{56,72},{64,... | collective-permute-start | bytes 129032 | tf_op jit(solution)/shard_map/ppermute | solution.py:382
  25.5 15.3 %collective-permute-start.2 = (bf16[112,192]{1,0:T(8,128)(2,1)}, bf16[112,192]{1,0:T(8,128)(2,1)S(1)}, u32[]{:S(2)}, u32[]{:S(2)}) collective-permute-start(bf16[112,192]{1,0:T(8,128)(2,1)} %get-tuple-element.15), channel_id=1, source_target_pairs={{0,24},{8,32},{16,40},{24,48},{32,56},{40,64},{48,72},{56,80},{64,... | collective-permute-start | bytes 129032 | tf_op jit(solution)/shard_map/ppermute | solution.py:382
  30.2 10.6 %collective-permute-start.3 = (bf16[112,192]{1,0:T(8,128)(2,1)}, bf16[112,192]{1,0:T(8,128)(2,1)S(1)}, u32[]{:S(2)}, u32[]{:S(2)}) collective-permute-start(bf16[112,192]{1,0:T(8,128)(2,1)} %get-tuple-element.15), channel_id=1, source_target_pairs={{0,32},{8,40},{16,48},{24,56},{32,64},{40,72},{48,80},{56,88},{64,... | collective-permute-start | bytes 129032 | tf_op jit(solution)/shard_map/ppermute | solution.py:382
  40.7 0.7 copy-start.17
  40.8 0.7 copy-start.18
  51.7 6.7 %copy-start.2 = (bf16[8,768,384]{2,1,0:T(8,128)(2,1)S(1)}, bf16[8,768,384]{2,1,0:T(8,128)(2,1)}, u32[]{:S(2)}) copy-start(bf16[8,768,384]{2,1,0:T(8,128)(2,1)} %get-tuple-element.16) | copy-start | bytes 14155780
  53.8 4.6 %collective-permute-start.4 = (bf16[4,768,384]{2,1,0:T(8,128)(2,1)S(1)}, bf16[4,768,384]{2,1,0:T(8,128)(2,1)S(1)}, u32[]{:S(2)}, u32[]{:S(2)}) collective-permute-start(bf16[4,768,384]{2,1,0:T(8,128)(2,1)S(1)} %slice.123), channel_id=1, source_target_pairs={{0,1},{1,0},{2,3},{3,2},{4,5},{5,4},{6,7},{7,6},{8,9},{9,8},{10,11... | collective-permute-start | bytes 7077896 | tf_op jit(solution)/shard_map/ppermute | solution.py:290
  58.4 27.2 %copy-start.3 = (bf16[4,768,384]{2,1,0:T(8,128)(2,1)}, bf16[4,768,384]{2,1,0:T(8,128)(2,1)S(1)}, u32[]{:S(2)}) copy-start(bf16[4,768,384]{2,1,0:T(8,128)(2,1)S(1)} %collective-permute-done.4) | copy-start | bytes 7077892
  58.9 10.5 %collective-permute-start.5 = (bf16[384,384]{1,0:T(8,128)(2,1)S(1)}, bf16[384,384]{1,0:T(8,128)(2,1)S(1)}, u32[]{:S(2)}, u32[]{:S(2)}) collective-permute-start(bf16[384,384]{1,0:T(8,128)(2,1)S(1)} %get-tuple-element.29), channel_id=1, source_target_pairs={{0,2},{2,4},{4,6},{6,0},{1,3},{3,5},{5,7},{7,1},{8,10},{10,12},{12... | collective-permute-start | bytes 884744 | tf_op jit(solution)/shard_map/ppermute | solution.py:286
  60.7 9.2 %collective-permute-start.7 = (bf16[384,384]{1,0:T(8,128)(2,1)S(1)}, bf16[384,384]{1,0:T(8,128)(2,1)S(1)}, u32[]{:S(2)}, u32[]{:S(2)}) collective-permute-start(bf16[384,384]{1,0:T(8,128)(2,1)S(1)} %get-tuple-element.30), channel_id=1, source_target_pairs={{0,6},{2,0},{4,2},{6,4},{1,7},{3,1},{5,3},{7,5},{8,14},{10,8},{12,... | collective-permute-start | bytes 884744 | tf_op jit(solution)/shard_map/ppermute | solution.py:286
  69.5 16.1 %copy-start.4 = (bf16[768,384]{1,0:T(8,128)(2,1)S(1)}, bf16[768,384]{1,0:T(8,128)(2,1)}, u32[]{:S(2)}) copy-start(bf16[768,384]{1,0:T(8,128)(2,1)} %param.16) | copy-start | bytes 1769476
  69.6 16.0 %collective-permute-start.6 = (bf16[768,384]{1,0:T(8,128)(2,1)S(1)}, bf16[768,384]{1,0:T(8,128)(2,1)S(1)}, u32[]{:S(2)}, u32[]{:S(2)}) collective-permute-start(bf16[768,384]{1,0:T(8,128)(2,1)S(1)} %pad_maximum_fusion), channel_id=1, source_target_pairs={{0,2},{2,4},{4,6},{6,0},{1,3},{3,5},{5,7},{7,1},{8,10},{10,12},{12... | collective-permute-start | bytes 1769480 | tf_op jit(solution)/shard_map/ppermute | solution.py:286
  70.0 15.5 %collective-permute-start.8 = (bf16[768,384]{1,0:T(8,128)(2,1)S(1)}, bf16[768,384]{1,0:T(8,128)(2,1)S(1)}, u32[]{:S(2)}, u32[]{:S(2)}) collective-permute-start(bf16[768,384]{1,0:T(8,128)(2,1)S(1)} %pad_maximum_fusion.1), channel_id=1, source_target_pairs={{0,6},{2,0},{4,2},{6,4},{1,7},{3,1},{5,3},{7,5},{8,14},{10,8},{12,... | collective-permute-start | bytes 1769480 | tf_op jit(solution)/shard_map/ppermute | solution.py:286
  85.6 0.8 copy-start.6
  85.6 1.0 copy-start.8
  86.6 23.6 %copy-start.14 = (f32[3,1056]{1,0:T(4,128)S(1)}, f32[3,1056]{1,0:T(4,128)}, u32[]{:S(2)}) copy-start(f32[3,1056]{1,0:T(4,128)} %param.29) | copy-start | bytes 38020
  86.6 25.8 %copy-start = (f32[3072]{0:T(1024)S(1)}, f32[3072]{0:T(1024)}, u32[]{:S(2)}) copy-start(f32[3072]{0:T(1024)} %param.26) | copy-start | bytes 36868
  86.6 15.2 %collective-permute-start.9 = (bf16[768,384]{1,0:T(8,128)(2,1)S(1)}, bf16[768,384]{1,0:T(8,128)(2,1)S(1)}, u32[]{:S(2)}, u32[]{:S(2)}) collective-permute-start(bf16[768,384]{1,0:T(8,128)(2,1)S(1)} %fusion.12.refs_0_), channel_id=1, source_target_pairs={{0,2},{2,4},{4,6},{6,0},{1,3},{3,5},{5,7},{7,1},{8,10},{10,12},{12... | collective-permute-start | bytes 1769480 | tf_op jit(solution)/shard_map/ppermute | solution.py:286
  86.9 15.1 %collective-permute-start.10 = (bf16[768,384]{1,0:T(8,128)(2,1)S(1)}, bf16[768,384]{1,0:T(8,128)(2,1)S(1)}, u32[]{:S(2)}, u32[]{:S(2)}) collective-permute-start(bf16[768,384]{1,0:T(8,128)(2,1)S(1)} %fusion.12.refs_0_), channel_id=1, source_target_pairs={{0,6},{2,0},{4,2},{6,4},{1,7},{3,1},{5,3},{7,5},{8,14},{10,8},{12,... | collective-permute-start | bytes 1769480 | tf_op jit(solution)/shard_map/ppermute | solution.py:286
  101.8 8.2 %collective-permute-start.11 = (bf16[384,384]{1,0:T(8,128)(2,1)S(1)}, bf16[384,384]{1,0:T(8,128)(2,1)S(1)}, u32[]{:S(2)}, u32[]{:S(2)}) collective-permute-start(bf16[384,384]{1,0:T(8,128)(2,1)S(1)} %slice.176), channel_id=1, source_target_pairs={{0,2},{2,4},{4,6},{6,0},{1,3},{3,5},{5,7},{7,1},{8,10},{10,12},{12... | collective-permute-start | bytes 884744 | tf_op jit(solution)/shard_map/ppermute | solution.py:286
  102.0 8.1 %collective-permute-start.12 = (bf16[384,384]{1,0:T(8,128)(2,1)S(1)}, bf16[384,384]{1,0:T(8,128)(2,1)S(1)}, u32[]{:S(2)}, u32[]{:S(2)}) collective-permute-start(bf16[384,384]{1,0:T(8,128)(2,1)S(1)} %slice.177), channel_id=1, source_target_pairs={{0,6},{2,0},{4,2},{6,4},{1,7},{3,1},{5,3},{7,5},{8,14},{10,8},{12,... | collective-permute-start | bytes 884744 | tf_op jit(solution)/shard_map/ppermute | solution.py:286
  105.2 6.9 %collective-permute-start.13 = (bf16[768,384]{1,0:T(8,128)(2,1)S(1)}, bf16[768,384]{1,0:T(8,128)(2,1)S(1)}, u32[]{:S(2)}, u32[]{:S(2)}) collective-permute-start(bf16[768,384]{1,0:T(8,128)(2,1)S(1)} %fusion.12.refs_0_), channel_id=1, source_target_pairs={{0,1},{1,0},{2,3},{3,2},{4,5},{5,4},{6,7},{7,6},{8,9},{9,8},{10,11... | collective-permute-start | bytes 1769480 | tf_op jit(solution)/shard_map/ppermute | solution.py:290
  105.2 6.9 %collective-permute-start.14 = (bf16[768,384]{1,0:T(8,128)(2,1)S(1)}, bf16[768,384]{1,0:T(8,128)(2,1)S(1)}, u32[]{:S(2)}, u32[]{:S(2)}) collective-permute-start(bf16[768,384]{1,0:T(8,128)(2,1)S(1)} %collective-permute-done.9.refs_1_), channel_id=1, source_target_pairs={{0,1},{1,0},{2,3},{3,2},{4,5},{5,4},{6,7},{7,6},{8,9},{9,8},{10,11... | collective-permute-start | bytes 1769480 | tf_op jit(solution)/shard_map/ppermute | solution.py:290
  105.8 6.4 %collective-permute-start.15 = (bf16[768,384]{1,0:T(8,128)(2,1)S(1)}, bf16[768,384]{1,0:T(8,128)(2,1)}, u32[]{:S(2)}, u32[]{:S(2)}) collective-permute-start(bf16[768,384]{1,0:T(8,128)(2,1)S(1)} %collective-permute-done.10.refs_2_), channel_id=1, source_target_pairs={{0,1},{1,0},{2,3},{3,2},{4,5},{5,4},{6,7},{7,6},{8,9},{9,8},{10,11... | collective-permute-start | bytes 1769480 | tf_op jit(solution)/shard_map/ppermute | solution.py:290
  110.1 2.2 %collective-permute-start.16 = (bf16[768,384]{1,0:T(8,128)(2,1)S(1)}, bf16[768,384]{1,0:T(8,128)(2,1)}, u32[]{:S(2)}, u32[]{:S(2)}) collective-permute-start(bf16[768,384]{1,0:T(8,128)(2,1)S(1)} %constant_dynamic-update-slice_fusion.refs_3_), channel_id=1, source_target_pairs={{0,1},{1,0},{2,3},{3,2},{4,5},{5,4},{6,7},{7,6},{8,9},{9,8},{10,11... | collective-permute-start | bytes 1769480 | tf_op jit(solution)/shard_map/ppermute | solution.py:290
  112.4 10.6 %slice-start.4 = ((f32[3,1056]{1,0:T(4,128)}), f32[3,1024]{1,0:T(4,128)S(1)}, s32[]{:S(2)}) async-start(f32[3,1056]{1,0:T(4,128)} %param.29), calls=%async_computation.5 | async-start | bytes 32768 | tf_op jit(solution)/shard_map/slice | solution.py:363
  120.5 7.4 %collective-permute-start.17 = (bf16[16,3072]{1,0:T(8,128)(2,1)S(1)}, bf16[16,3072]{1,0:T(8,128)(2,1)S(1)}, u32[]{:S(2)}, u32[]{:S(2)}) collective-permute-start(bf16[16,3072]{1,0:T(8,128)(2,1)S(1)} %get-tuple-element.18), channel_id=1, source_target_pairs={{0,8},{8,16},{16,24},{24,32},{32,40},{40,48},{48,56},{56,64},{64,7... | collective-permute-start | bytes 294920 | tf_op jit(solution)/shard_map/ppermute | solution.py:444
  172.9 6.7 %copy-start.1 = (bf16[8,768,384]{2,1,0:T(8,128)(2,1)S(1)}, bf16[8,768,384]{2,1,0:T(8,128)(2,1)}, u32[]{:S(2)}) copy-start(bf16[8,768,384]{2,1,0:T(8,128)(2,1)} %mixer.1) | copy-start | bytes 14155780
  175.0 4.6 %collective-permute-start.18 = (bf16[4,768,384]{2,1,0:T(8,128)(2,1)S(1)}, bf16[4,768,384]{2,1,0:T(8,128)(2,1)S(1)}, u32[]{:S(2)}, u32[]{:S(2)}) collective-permute-start(bf16[4,768,384]{2,1,0:T(8,128)(2,1)S(1)} %slice.181), channel_id=1, source_target_pairs={{0,1},{1,0},{2,3},{3,2},{4,5},{5,4},{6,7},{7,6},{8,9},{9,8},{10,11... | collective-permute-start | bytes 7077896 | tf_op jit(solution)/shard_map/ppermute | solution.py:290
  180.2 10.3 %collective-permute-start.19 = (bf16[384,384]{1,0:T(8,128)(2,1)S(1)}, bf16[384,384]{1,0:T(8,128)(2,1)S(1)}, u32[]{:S(2)}, u32[]{:S(2)}) collective-permute-start(bf16[384,384]{1,0:T(8,128)(2,1)S(1)} %get-tuple-element.27), channel_id=1, source_target_pairs={{0,2},{2,4},{4,6},{6,0},{1,3},{3,5},{5,7},{7,1},{8,10},{10,12},{12... | collective-permute-start | bytes 884744 | tf_op jit(solution)/shard_map/ppermute | solution.py:286
  181.8 9.3 %collective-permute-start.21 = (bf16[384,384]{1,0:T(8,128)(2,1)S(1)}, bf16[384,384]{1,0:T(8,128)(2,1)S(1)}, u32[]{:S(2)}, u32[]{:S(2)}) collective-permute-start(bf16[384,384]{1,0:T(8,128)(2,1)S(1)} %get-tuple-element.28), channel_id=1, source_target_pairs={{0,6},{2,0},{4,2},{6,4},{1,7},{3,1},{5,3},{7,5},{8,14},{10,8},{12,... | collective-permute-start | bytes 884744 | tf_op jit(solution)/shard_map/ppermute | solution.py:286
  190.7 15.8 %copy-start.5 = (bf16[768,384]{1,0:T(8,128)(2,1)S(1)}, bf16[768,384]{1,0:T(8,128)(2,1)}, u32[]{:S(2)}) copy-start(bf16[768,384]{1,0:T(8,128)(2,1)} %param.16) | copy-start | bytes 1769476
  190.7 15.8 %copy-start.7 = (bf16[768,384]{1,0:T(8,128)(2,1)S(1)}, bf16[768,384]{1,0:T(8,128)(2,1)}, u32[]{:S(2)}) copy-start(bf16[768,384]{1,0:T(8,128)(2,1)} %copy-done.6) | copy-start | bytes 1769476
  190.7 15.8 %copy-start.9 = (bf16[768,384]{1,0:T(8,128)(2,1)S(1)}, bf16[768,384]{1,0:T(8,128)(2,1)}, u32[]{:S(2)}) copy-start(bf16[768,384]{1,0:T(8,128)(2,1)} %copy-done.8) | copy-start | bytes 1769476
  190.7 15.8 %collective-permute-start.20 = (bf16[768,384]{1,0:T(8,128)(2,1)S(1)}, bf16[768,384]{1,0:T(8,128)(2,1)S(1)}, u32[]{:S(2)}, u32[]{:S(2)}) collective-permute-start(bf16[768,384]{1,0:T(8,128)(2,1)S(1)} %pad_maximum_fusion.2), channel_id=1, source_target_pairs={{0,2},{2,4},{4,6},{6,0},{1,3},{3,5},{5,7},{7,1},{8,10},{10,12},{12... | collective-permute-start | bytes 1769480 | tf_op jit(solution)/shard_map/ppermute | solution.py:286
  191.2 15.3 %collective-permute-start.22 = (bf16[768,384]{1,0:T(8,128)(2,1)S(1)}, bf16[768,384]{1,0:T(8,128)(2,1)S(1)}, u32[]{:S(2)}, u32[]{:S(2)}) collective-permute-start(bf16[768,384]{1,0:T(8,128)(2,1)S(1)} %pad_maximum_fusion.3), channel_id=1, source_target_pairs={{0,6},{2,0},{4,2},{6,4},{1,7},{3,1},{5,3},{7,5},{8,14},{10,8},{12,... | collective-permute-start | bytes 1769480 | tf_op jit(solution)/shard_map/ppermute | solution.py:286
  (2 other events, 1.3 us)
Sparse Core Ops, SparseCore 0:
  10.4 132.0 all-gather.1

commit v3 on v2

--- a/solution.py
+++ b/solution.py
@@ -21,6 +21,17 @@
 
 def in_first_head(shape):
     return lax.broadcasted_iota(jnp.int32, shape, len(shape) - 1) < DH
+
+
+def pack_kernel(gate_ref, value_ref, down_ref, out_ref):
+    rows, hidden = gate_ref.shape
+    main = hidden // 128 * 128
+    tails = []
+    for k, ref in enumerate((gate_ref, value_ref, down_ref)):
+        out_ref[:, k * main : (k + 1) * main] = ref[:, :main]
+        tails.append(ref[:, main:])
+    tails.append(jnp.zeros((rows, 128 - 3 * (hidden - main)), BF16))
+    out_ref[:, 3 * main :] = jnp.concatenate(tails, axis=1)
 
 
 def state_kernel(k_ref, v_ref, in_ref, forget_ref, doc_ref, pay_ref, row_ref, col_ref, scr):
@@ -188,6 +199,12 @@
         send_ref[:, cut] = done[tokens - HALO :, :]
 
 
+def down_product(h, w):
+    return lax.dot_general(
+        h, w, (((1,), (1,)), ((), ())), preferred_element_type=F32
+    ).astype(BF16)
+
+
 def mixer_kernel(
     order_ref,
     x_ref,
@@ -196,21 +213,39 @@
     taps_ref,
     wg_ref,
     wv_ref,
-    wt_ref,
-    wda_ref,
-    wdb_ref,
-    wdta_ref,
-    wdtb_ref,
-    out_ref,
+    w_ref,
+    h_ref,
+    swap_ref,
+    own_ref,
     gate_scr,
     value_scr,
-    h_scr,
+    tail_scr,
+    down_scr,
+    sems,
 ):
     tokens = near_ref.shape[0]
     tiles, _, tile = taps_ref.shape
     tiles -= 1
     main = tiles * tile
+    cols = down_scr.shape[1]
     j = pl.program_id(0)
+    copies = [pltpu.make_async_copy(w_ref.at[:, pl.ds(3 * main, 128)], tail_scr, sems.at[0])]
+    for k in range(2):
+        rows = pl.ds(pl.multiple_of(order_ref[k] * cols, 128), cols)
+        copies.append(
+            pltpu.make_async_copy(
+                w_ref.at[rows, pl.ds(2 * main, main)],
+                down_scr.at[k, :, pl.ds(0, main)],
+                sems.at[1 + 2 * k],
+            )
+        )
+        copies.append(
+            pltpu.make_async_copy(
+                w_ref.at[rows, pl.ds(3 * main, 128)],
+                down_scr.at[k, :, pl.ds(main, 128)],
+                sems.at[2 + 2 * k],
+            )
+        )
 
     def hidden(gate, value, taps, rows):
         near, far = near_ref[rows, :], far_ref[rows, :]
@@ -221,7 +256,8 @@
             + taps[1:2, :] * (near * one)
             + taps[0:1, :] * (far * two)
         )
-        return conv / (1.0 + jnp.exp(-conv)) * value
+        scaled = 0.5 * conv
+        return (scaled + scaled * jnp.tanh(scaled)) * value
 
     block = 96
 
@@ -230,28 +266,36 @@
             for half in range(0, tile, 128):
                 lanes = slice(half, half + 128)
                 done = hidden(
-                    gate_scr[slot, start : start + block + HALO, lanes].astype(F32),
-                    value_scr[slot, start + HALO : start + HALO + block, lanes].astype(F32),
+                    gate_scr[slot, start : start + block + HALO, lanes],
+                    value_scr[slot, start + HALO : start + HALO + block, lanes],
                     taps_ref[at, :, lanes],
                     slice(start, start + block),
                 )
                 spot = pl.multiple_of(at * tile + half, 128)
-                h_scr[start : start + block, pl.ds(spot, 128)] = done.astype(BF16)
-
-    @pl.when(j < tiles)
+                h_ref[start : start + block, pl.ds(spot, 128)] = done.astype(BF16)
+
+    def project(slot):
+        gate_scr[slot] = jnp.dot(x_ref[...], wg_ref[...], preferred_element_type=F32)
+        value_scr[slot] = jnp.dot(x_ref[...], wv_ref[...], preferred_element_type=F32)
+
+    @pl.when(j == 0)
     def _():
-        gate_scr[j % 2] = jnp.dot(x_ref[...], wg_ref[...], preferred_element_type=F32).astype(BF16)
-        value_scr[j % 2] = jnp.dot(x_ref[...], wv_ref[...], preferred_element_type=F32).astype(BF16)
-
-    @pl.when((j > 0) & (j <= tiles))
+        for copy in copies:
+            copy.start()
+        project(0)
+
+    @pl.when((j > 0) & (j < tiles))
     def _():
+        project(j % 2)
         finish((j - 1) % 2, j - 1)
 
     @pl.when(j == tiles)
     def _():
-        both = jnp.dot(x_ref[...], wt_ref[...], preferred_element_type=F32).astype(BF16)
+        copies[0].wait()
+        both = jnp.dot(x_ref[...], tail_scr[...], preferred_element_type=F32)
+        finish((tiles - 1) % 2, tiles - 1)
         for start in range(0, tokens, block):
-            part = both[start : start + block + HALO, :].astype(F32)
+            part = both[start : start + block + HALO, :]
             lane = lax.broadcasted_iota(jnp.int32, (block, 128), 1)
             mine = (lane >= 64) & (lane < 96)
             done = hidden(
@@ -260,18 +304,45 @@
                 taps_ref[tiles, :, 0:128],
                 slice(start, start + block),
             )
-            h_scr[start : start + block, main:] = jnp.where(mine, done, 0.0).astype(BF16)
+            h_ref[start : start + block, main:] = jnp.where(mine, done, 0.0).astype(BF16)
 
     @pl.when(j > tiles)
     def _():
-        contract = (((1,), (1,)), ((), ()))
-        for p, (wd_ref, wdt_ref) in enumerate(((wda_ref, wdta_ref), (wdb_ref, wdtb_ref))):
-            out_ref[p] = (
-                lax.dot_general(h_scr[:, 0:main], wd_ref[...], contract, preferred_element_type=F32)
-                + lax.dot_general(
-                    h_scr[:, main:], wdt_ref[...], contract, preferred_element_type=F32
-                )
-            ).astype(BF16)
+        for copy in copies[1:]:
+            copy.wait()
+        swap_ref[0] = down_product(h_ref[...], down_scr[0])
+        own_ref[0] = down_product(h_ref[...], down_scr[1])
+
+
+def down_kernel(order_ref, h_ref, wa_ref, wb_ref, ta_ref, tb_ref, swap_ref, own_ref):
+    count = swap_ref.shape[0]
+    main = wa_ref.shape[1]
+    both = ((wa_ref, ta_ref), (wb_ref, tb_ref))
+
+    def put(ref, k, w_ref, t_ref):
+        ref[k] = (
+            lax.dot_general(
+                h_ref[:, :main], w_ref[...], (((1,), (1,)), ((), ())), preferred_element_type=F32
+            )
+            + lax.dot_general(
+                h_ref[:, main:], t_ref[...], (((1,), (1,)), ((), ())), preferred_element_type=F32
+            )
+        ).astype(BF16)
+
+    if count == 1:
+        put(swap_ref, 0, *both[0])
+        put(own_ref, 0, *both[1])
+        return
+
+    @pl.when(pl.program_id(0) == 0)
+    def _():
+        for k in range(2):
+            put(swap_ref, k, *both[k])
+
+    @pl.when(pl.program_id(0) == 1)
+    def _():
+        for k in range(2):
+            put(own_ref, k, *both[k])
 
 
 def added(*terms):
@@ -290,15 +361,21 @@
     return lax.ppermute(value, "c", [(0, 1), (1, 0)])
 
 
-def summed_over_tp(shares):
-    half = shares.shape[2] // 2
-    other = swapped(shares[1])
-    pair = [added(shares[0, k], other[k]).astype(BF16) for k in range(4)]
-    up = shifted(pair[2][:half], 1)
-    down = shifted(pair[2][half:], -1)
-    up = jnp.concatenate([added(pair[1][:half], up).astype(BF16), pair[1][half:]], axis=0)
-    down = jnp.concatenate([pair[3][:half], added(pair[3][half:], down).astype(BF16)], axis=0)
-    return added(pair[0], shifted(up, 1), shifted(down, -1))
+def summed_over_tp(far, sides, near):
+    swap, own = far()
+    pair = added(own[0], swapped(swap)[0]).astype(BF16)
+    half = pair.shape[0] // 2
+    up = shifted(pair[:half], 1)
+    down = shifted(pair[half:], -1)
+    swap, own = sides()
+    other = swapped(swap)
+    pair = [added(own[k], other[k]) for k in range(2)]
+    up = jnp.concatenate([added(pair[0][:half], up), pair[0][half:]], axis=0).astype(BF16)
+    down = jnp.concatenate([pair[1][:half], added(pair[1][half:], down)], axis=0).astype(BF16)
+    up = shifted(up, 1)
+    down = shifted(down, -1)
+    swap, own = near()
+    return added(own[0], swapped(swap)[0], up, down)
 
 
 def gathered_over_tp(own):
@@ -341,19 +418,11 @@
     hidden = w_gate.shape[1]
     main = hidden // 128 * 128
     spare = hidden - main
-    down_t = w_down.T
-    packed = jnp.concatenate(
-        [
-            w_gate[:, :main],
-            w_value[:, :main],
-            down_t[:, :main],
-            w_gate[:, main:],
-            w_value[:, main:],
-            down_t[:, main:],
-            jnp.zeros((w_gate.shape[0], 128 - 3 * spare), BF16),
-        ],
-        axis=1,
-    )
+    packed = pl.pallas_call(
+        pack_kernel,
+        out_shape=shape((w_gate.shape[0], 3 * main + 128), BF16),
+        name="pack",
+    )(w_gate, w_value, w_down.T)
     weights = lax.all_gather(packed, SP, axis=0, tiled=True)
     tile = 256
     tiles = main // tile
@@ -390,8 +459,9 @@
     ring, cores = lax.axis_size("y"), lax.axis_size("c")
     chips = (chip + jnp.arange(ring, dtype=jnp.int32)) % ring
     sides = core ^ jnp.arange(cores, dtype=jnp.int32)
-    order = (chips[None, :] * cores + sides[:, None]).reshape(-1)
-    share, near, far = pl.pallas_call(
+    to = chips[None, :] * cores + sides[:, None]
+    order = jnp.stack([to[1, 2], to[0, 2], to[1, 1], to[1, 3], to[0, 1], to[0, 3], to[1, 0], to[0, 0]])
+    share, near, far_flags = pl.pallas_call(
         mix_kernel,
         grid_spec=pltpu.PrefetchScalarGridSpec(
             num_scalar_prefetch=1,
@@ -420,7 +490,11 @@
         ),
         name="mix",
     )(order, query, out_gate, local, rows, cols_aux, head_gain.reshape(1, width), w_out, *pays)
-    attended = summed_over_tp(share.reshape(cores, ring, tokens, cols))
+    attended = summed_over_tp(
+        lambda: (share[0:1], share[1:2]),
+        lambda: (share[2:4], share[4:6]),
+        lambda: (share[6:7], share[7:8]),
+    )
     residual_own = resid.astype(F32) + attended
     pieces = gathered_over_tp(residual_own.astype(BF16))
     came = (chip + jnp.array([0, -1, 1, 2], jnp.int32)) % ring
@@ -443,48 +517,74 @@
     )(places, *pieces, ffn_gain.reshape(1, model))
     edge = lax.ppermute(send, SP, [(i, i + 1) for i in range(count - 1)])
     normed = lax.dynamic_update_slice(normed, edge, (0, 0))
-    first = tiles + 1
     tail_at = 3 * main // 128
-
-    def down_at(k, col):
-        return lambda j, order: (order[2 * jnp.maximum(j - first, 0) + k], col)
-
-    terms = pl.pallas_call(
-        mixer_kernel,
-        grid_spec=pltpu.PrefetchScalarGridSpec(
-            num_scalar_prefetch=1,
-            grid=(first + parts // 2,),
-            in_specs=[
-                pl.BlockSpec(
-                    (tokens + HALO, model), lambda j, order: (0, 0), pipeline_mode=pl.Buffered(1)
+    part = shape((1, tokens, cols), BF16)
+
+    def far():
+        return pl.pallas_call(
+            mixer_kernel,
+            grid_spec=pltpu.PrefetchScalarGridSpec(
+                num_scalar_prefetch=1,
+                grid=(tiles + 2,),
+                in_specs=[
+                    pl.BlockSpec(
+                        (tokens + HALO, model),
+                        lambda j, order: (0, 0),
+                        pipeline_mode=pl.Buffered(1),
+                    ),
+                    whole((tokens, 128)),
+                    whole((tokens, 128)),
+                    whole((tiles + 1, 3, tile)),
+                    pl.BlockSpec((model, tile), lambda j, order: (0, jnp.minimum(j, tiles - 1))),
+                    pl.BlockSpec(
+                        (model, tile), lambda j, order: (0, tiles + jnp.minimum(j, tiles - 1))
+                    ),
+                    pl.BlockSpec(memory_space=pl.ANY),
+                ],
+                out_specs=(
+                    whole((tokens, main + 128)),
+                    whole((1, tokens, cols)),
+                    whole((1, tokens, cols)),
                 ),
-                whole((tokens, 128)),
-                whole((tokens, 128)),
-                whole((tiles + 1, 3, tile)),
-                pl.BlockSpec((model, tile), lambda j, order: (0, jnp.minimum(j, tiles - 1))),
-                pl.BlockSpec(
-                    (model, tile), lambda j, order: (0, tiles + jnp.minimum(j, tiles - 1))
-                ),
-                pl.BlockSpec((model, 128), lambda j, order: (0, tail_at)),
-                pl.BlockSpec((cols, main), down_at(0, 2)),
-                pl.BlockSpec((cols, main), down_at(1, 2)),
-                pl.BlockSpec((cols, 128), down_at(0, tail_at)),
-                pl.BlockSpec((cols, 128), down_at(1, tail_at)),
-            ],
-            out_specs=pl.BlockSpec(
-                (2, tokens, cols), lambda j, order: (jnp.maximum(j - first, 0), 0, 0)
+                scratch_shapes=[
+                    pltpu.VMEM((2, tokens + HALO, tile), F32),
+                    pltpu.VMEM((2, tokens + HALO, tile), F32),
+                    pltpu.VMEM((model, 128), BF16),
+                    pltpu.VMEM((2, cols, main + 128), BF16),
+                    pltpu.SemaphoreType.DMA((5,)),
+                ],
             ),
-            scratch_shapes=[
-                pltpu.VMEM((2, tokens + HALO, tile), BF16),
-                pltpu.VMEM((2, tokens + HALO, tile), BF16),
-                pltpu.VMEM((tokens, main + 128), BF16),
-            ],
-        ),
-        out_shape=shape((parts, tokens, cols), BF16),
-        compiler_params=pltpu.CompilerParams(vmem_limit_bytes=56 * 2**20),
-        name="mixer",
-    )(order, normed, near, far, taps, *[weights] * 7)
-    down = summed_over_tp(terms.reshape(cores, ring, tokens, cols))
+            out_shape=(shape((tokens, main + 128), BF16), part, part),
+            compiler_params=pltpu.CompilerParams(vmem_limit_bytes=56 * 2**20),
+            name="mixer",
+        )(order, normed, near, far_flags, taps, weights, weights, weights)
+
+    hidden, *far_parts = far()
+
+    def further(at, count):
+        def spot(k, col):
+            return lambda j, order: (order[at + 2 * j + k], col)
+
+        many = shape((count, tokens, cols), BF16)
+        return pl.pallas_call(
+            down_kernel,
+            grid_spec=pltpu.PrefetchScalarGridSpec(
+                num_scalar_prefetch=1,
+                grid=(count,),
+                in_specs=[
+                    whole((tokens, main + 128)),
+                    pl.BlockSpec((cols, main), spot(0, 2)),
+                    pl.BlockSpec((cols, main), spot(1, 2)),
+                    pl.BlockSpec((cols, 128), spot(0, tail_at)),
+                    pl.BlockSpec((cols, 128), spot(1, tail_at)),
+                ],
+                out_specs=(whole((count, tokens, cols)), whole((count, tokens, cols))),
+            ),
+            out_shape=(many, many),
+            compiler_params=pltpu.CompilerParams(vmem_limit_bytes=40 * 2**20),
+        )(order, hidden, *[weights] * 4)
+
+    down = summed_over_tp(lambda: far_parts, lambda: further(2, 2), lambda: further(6, 1))
     return (residual_own + down).astype(BF16)
 
 

time: 217 us -> 214 us (0.986)
  waiting for transfers between devices: 82.5 us -> 68.2 us
  Pallas kernels: 56 us -> 60.8 us
  local copies, waits for them, and re-layouts: 18 us -> 22.3 us
  starting transfers between devices: 40 us -> 42.2 us
    ppermute x6 -> x10, waiting for transfers between devices: 9.22 us -> 1.52 us  [swapped(): return lax.ppermute(value, 'c', [(0, 1), (1, 0)])]
    all_gather x1, waiting for transfers between devices: 14 us -> 7.75 us  [layer(): weights = lax.all_gather(packed, SP, axis=0, tiled=True)]
    another operation x0 -> x1, local copies, waits for them, and re-layouts: none -> 5.73 us  [layer(): jnp.stack([to[1, 2], to[0, 2], to[1, 1], to[1, 3], to[0, 1], to[0, 3], to...]
    pallas_call x1 -> x4, Pallas kernels: 30.4 us -> 35.1 us  [the longest x1 22.4 us: far(): pl.pallas_call(mixer_kernel, grid_spec=pltpu.PrefetchScalarGridSpec(num_s...]
    unnamed x47 -> x55, local copies, waits for them, and re-layouts: 6.02 us -> 7.46 us
    slice x18 -> x9, local copies, waits for them, and re-layouts: 6.27 us -> 5.62 us  [the longest x1 2.79 us: layer(): share[6:7]]
  transfers between devices with their start and end apart: 24 -> 28, of which waited for: 11 -> 9; matrix products, arithmetic and copies ran while one was open for 6% -> 10% of each run, Pallas kernels for 12% -> 14%
where the time goes in v3:
time: 214 us; the launch traced here: 213 us
  waiting for transfers between devices  68.2 us (32%)
  Pallas kernels  60.8 us (28%)
  starting transfers between devices  42.2 us (20%)
  local copies, waits for them, and re-layouts  22.3 us (10%)
  between operations  13.9 us (6%)
  other arithmetic  5.55 us (3%)
    ppermute x12, waiting for transfers between devices, shifted(): return lax.ppermute(value, 'y', [(i, (i + by) % ring) for i in range(ring)])  54.4 us
    pallas_call x1, Pallas kernels, far(): pl.pallas_call(mixer_kernel, grid_spec=pltpu.PrefetchScalarGridSpec(num_s...  22.4 us
    ppermute x12, starting transfers between devices, shifted(): return lax.ppermute(value, 'y', [(i, (i + by) % ring) for i in range(ring)])  20 us
    ppermute x4, starting transfers between devices, layer(): lax.ppermute(pay, SP, [(i, i + k) for i in range(count - k)])  16.7 us
    pallas_call x2, Pallas kernels, further(): pl.pallas_call(down_kernel, grid_spec=pltpu.PrefetchScalarGridSpec(num_sc...  10.4 us
    pallas_call x1, Pallas kernels, layer(): pl.pallas_call(mix_kernel, grid_spec=pltpu.PrefetchScalarGridSpec(num_sca...  10.3 us
    pallas_call x1, Pallas kernels, layer(): pl.pallas_call(norm_kernel, grid_spec=pltpu.PrefetchScalarGridSpec(num_sc...  8.16 us
    all_gather x1, waiting for transfers between devices, layer(): weights = lax.all_gather(packed, SP, axis=0, tiled=True)  7.75 us
  transfers between devices with their start and end apart: 28, of which 9 were waited for; matrix products, arithmetic and copies ran while one was open for 10% of the time, Pallas kernels for 14%

profile of v3, /device:TPU:0, one launch (start us, length us, event | category | flops | bytes accessed | tf_op | source)
XLA Modules:
  0.0 212.9 jit_solution(2849486338305554396)
XLA Ops:
  6.5 2.4 %pack.1 = bf16[192,3200]{1,0:T(8,128)(2,1)} custom-call(bf16[192,1056]{1,0:T(8,128)(2,1)} %gate_ref.2, bf16[192,1056]{1,0:T(8,128)(2,1)} %value_ref.1, bf16[192,1056]{1,0:T(8,128)(2,1)} %bitcast.75), custom_call_target="tpu_custom_call" | custom-call | tf_op jit(solution)/shard_map/pack/pallas_call | solution.py:421
  9.0 0.9 copy-done.13
  9.9 0.9 copy.20.k_ref
  10.8 0.9 copy.21.v_ref
  11.8 0.6 reshape.81.doc_ref
  12.4 3.6 %state.1 = (bf16[112,192]{1,0:T(8,128)(2,1)}, f32[8,768]{1,0:T(8,128)}, f32[768,8]{1,0:T(8,128)}) custom-call(bf16[768,192]{1,0:T(8,128)(2,1)} %copy.20.k_ref, bf16[768,192]{1,0:T(8,128)(2,1)} %copy.21.v_ref, f32[2,768]{1,0:T(2,128)} %in_ref.1, f32[2,768]{1,0:T(2,128)} %forget_ref.1, s32[1,768]{1,0:T(1,128)} %reshape.81.doc_ref), custom_call_target="tpu_custom_call" | custom-call | tf_op jit(solution)/shard_map/state/pallas_call | solution.py:438
  16.0 3.5 %collective-permute-start = (bf16[112,192]{1,0:T(8,128)(2,1)}, bf16[112,192]{1,0:T(8,128)(2,1)S(1)}, u32[]{:S(2)}, u32[]{:S(2)}) collective-permute-start(bf16[112,192]{1,0:T(8,128)(2,1)} %get-tuple-element.22), channel_id=1, source_target_pairs={{0,8},{8,16},{16,24},{24,32},{32,40},{40,48},{48,56},{56,64},{64,7... | collective-permute-start | bytes 129032 | tf_op jit(solution)/shard_map/ppermute | solution.py:451
  19.5 4.6 %collective-permute-start.1 = (bf16[112,192]{1,0:T(8,128)(2,1)}, bf16[112,192]{1,0:T(8,128)(2,1)S(1)}, u32[]{:S(2)}, u32[]{:S(2)}) collective-permute-start(bf16[112,192]{1,0:T(8,128)(2,1)} %get-tuple-element.22), channel_id=1, source_target_pairs={{0,16},{8,24},{16,32},{24,40},{32,48},{40,56},{48,64},{56,72},{64,... | collective-permute-start | bytes 129032 | tf_op jit(solution)/shard_map/ppermute | solution.py:451
  24.1 4.7 %collective-permute-start.2 = (bf16[112,192]{1,0:T(8,128)(2,1)}, bf16[112,192]{1,0:T(8,128)(2,1)S(1)}, u32[]{:S(2)}, u32[]{:S(2)}) collective-permute-start(bf16[112,192]{1,0:T(8,128)(2,1)} %get-tuple-element.22), channel_id=1, source_target_pairs={{0,24},{8,32},{16,40},{24,48},{32,56},{40,64},{48,72},{56,80},{64,... | collective-permute-start | bytes 129032 | tf_op jit(solution)/shard_map/ppermute | solution.py:451
  28.8 3.8 %collective-permute-start.3 = (bf16[112,192]{1,0:T(8,128)(2,1)}, bf16[112,192]{1,0:T(8,128)(2,1)S(1)}, u32[]{:S(2)}, u32[]{:S(2)}) collective-permute-start(bf16[112,192]{1,0:T(8,128)(2,1)} %get-tuple-element.22), channel_id=1, source_target_pairs={{0,32},{8,40},{16,48},{24,56},{32,64},{40,72},{48,80},{56,88},{64,... | collective-permute-start | bytes 129032 | tf_op jit(solution)/shard_map/ppermute | solution.py:451
  32.7 0.7 broadcast_add_fusion
  33.4 0.7 fusion.23
  34.1 0.9 copy.22.q_ref
  35.0 0.9 copy.23.gate_ref
  35.9 3.6 %local.1.local_ref = f32[768,192]{1,0:T(8,128)} custom-call(bf16[768,192]{1,0:T(8,128)(2,1)} %copy.22.q_ref, bf16[768,192]{1,0:T(8,128)(2,1)} %copy.20.k_ref, bf16[768,192]{1,0:T(8,128)(2,1)} %copy.21.v_ref, f32[8,768]{1,0:T(8,128)} %get-tuple-element.20.row_ref, f32[768,8]{1,0:T(8,128)} %get-tuple-element.21.col_ref), custom_call_target="tpu_custom_call" | custom-call | tf_op jit(solution)/shard_map/local/pallas_call | solution.py:453
  39.5 5.7 %stack.3.order_ref = s32[8]{0:T(128)} concatenate(s32[1]{0:T(128)} %bitcast, s32[1]{0:T(128)} %bitcast.1, s32[1]{0:T(128)} %bitcast.2, s32[1]{0:T(128)} %bitcast.3, s32[1]{0:T(128)} %bitcast.4, s32[1]{0:T(128)} %bitcast.5, s32[1]{0:T(128)} %bitcast.6, s32[1]{0:T(128)} %bitcast.7), dimensions={0} | concatenate | bytes 64 | tf_op jit(solution)/shard_map/stack | solution.py:463
  45.9 10.3 %mix.1 = (bf16[8,768,384]{2,1,0:T(8,128)(2,1)}, f32[768,128]{1,0:T(8,128)}, f32[768,128]{1,0:T(8,128)}) custom-call(s32[8]{0:T(128)} %stack.3.order_ref, bf16[768,192]{1,0:T(8,128)(2,1)} %copy.22.q_ref, bf16[768,192]{1,0:T(8,128)(2,1)} %copy.23.gate_ref, f32[768,192]{1,0:T(8,128)} %local.1.local_ref, f32[8,768]{1,0:T(8,128)} %get-tuple-element.20.row_ref, ...), custom_call_target="tpu_custom_call" | custom-call | tf_op jit(solution)/shard_map/mix/pallas_call | solution.py:464
  56.2 1.9 slice.165
  58.2 2.8 %fusion.22 = (bf16[1,768,384]{2,1,0:T(8,128)(2,1)S(1)}, bf16[1,768,384]{2,1,0:T(8,128)(2,1)S(1)}) fusion(bf16[8,768,384]{2,1,0:T(8,128)(2,1)} %get-tuple-element.23), kind=kLoop, calls=%fused_computation.60 | loop fusion | bytes 2359296 | tf_op jit(solution)/shard_map/slice | solution.py:496
  61.6 1.5 collective-permute-done.6
  63.5 1.6 collective-permute-start.7
  65.2 1.7 collective-permute-start.9
  67.0 6.9 %collective-permute-done.7 = bf16[384,384]{1,0:T(8,128)(2,1)S(1)} collective-permute-done((bf16[384,384]{1,0:T(8,128)(2,1)S(1)}, bf16[384,384]{1,0:T(8,128)(2,1)S(1)}, u32[]{:S(2)}, u32[]{:S(2)}) %collective-permute-start.7) | collective-permute-done | bytes 294944 | tf_op jit(solution)/shard_map/ppermute | solution.py:357
  74.6 3.0 %collective-permute-start.10 = (bf16[768,384]{1,0:T(8,128)(2,1)S(1)}, bf16[768,384]{1,0:T(8,128)(2,1)S(1)}, u32[]{:S(2)}, u32[]{:S(2)}) collective-permute-start(bf16[768,384]{1,0:T(8,128)(2,1)S(1)} %pad_maximum_fusion.1), channel_id=1, source_target_pairs={{0,6},{2,0},{4,2},{6,4},{1,7},{3,1},{5,3},{7,5},{8,14},{10,8},{12,... | collective-permute-start | bytes 1769480 | tf_op jit(solution)/shard_map/ppermute | solution.py:357
  77.6 12.4 %collective-permute-done.8 = bf16[768,384]{1,0:T(8,128)(2,1)S(1)} collective-permute-done((bf16[768,384]{1,0:T(8,128)(2,1)S(1)}, bf16[768,384]{1,0:T(8,128)(2,1)S(1)}, u32[]{:S(2)}, u32[]{:S(2)}) %collective-permute-start.8) | collective-permute-done | bytes 589856 | tf_op jit(solution)/shard_map/ppermute | solution.py:357
  91.4 2.8 %collective-permute-start.12 = (bf16[768,384]{1,0:T(8,128)(2,1)S(1)}, bf16[768,384]{1,0:T(8,128)(2,1)S(1)}, u32[]{:S(2)}, u32[]{:S(2)}) collective-permute-start(bf16[768,384]{1,0:T(8,128)(2,1)S(1)} %fusion.21.refs_0_), channel_id=1, source_target_pairs={{0,6},{2,0},{4,2},{6,4},{1,7},{3,1},{5,3},{7,5},{8,14},{10,8},{12,... | collective-permute-start | bytes 1769480 | tf_op jit(solution)/shard_map/ppermute | solution.py:357
  94.2 11.9 %collective-permute-done.11.refs_1_ = bf16[768,384]{1,0:T(8,128)(2,1)S(1)} collective-permute-done((bf16[768,384]{1,0:T(8,128)(2,1)S(1)}, bf16[768,384]{1,0:T(8,128)(2,1)S(1)}, u32[]{:S(2)}, u32[]{:S(2)}) %collective-permute-start.11) | collective-permute-done | bytes 589856 | tf_op jit(solution)/shard_map/ppermute | solution.py:357
  106.3 3.3 %collective-permute-start.14 = (bf16[384,384]{1,0:T(8,128)(2,1)S(1)}, bf16[384,384]{1,0:T(8,128)(2,1)S(1)}, u32[]{:S(2)}, u32[]{:S(2)}) collective-permute-start(bf16[384,384]{1,0:T(8,128)(2,1)S(1)} %slice.212), channel_id=1, source_target_pairs={{0,6},{2,0},{4,2},{6,4},{1,7},{3,1},{5,3},{7,5},{8,14},{10,8},{12,... | collective-permute-start | bytes 884744 | tf_op jit(solution)/shard_map/ppermute | solution.py:357
  110.1 4.2 %collective-permute-done.13 = bf16[384,384]{1,0:T(8,128)(2,1)S(1)} collective-permute-done((bf16[384,384]{1,0:T(8,128)(2,1)S(1)}, bf16[384,384]{1,0:T(8,128)(2,1)S(1)}, u32[]{:S(2)}, u32[]{:S(2)}) %collective-permute-start.13) | collective-permute-done | bytes 294944 | tf_op jit(solution)/shard_map/ppermute | solution.py:357
  114.6 0.6 slice.186
  115.2 0.8 add.144.order_ref
  116.0 0.8 pad_bitcast_fusion
  116.8 8.2 %norm.1 = (bf16[784,3072]{1,0:T(8,128)(2,1)}, bf16[16,3072]{1,0:T(8,128)(2,1)S(1)}) custom-call(s32[8]{0:T(128)S(1)} %add.144.order_ref, bf16[768,384]{1,0:T(8,128)(2,1)S(1)} %fusion.21.refs_0_, bf16[768,384]{1,0:T(8,128)(2,1)S(1)} %collective-permute-done.11.refs_1_, bf16[768,384]{1,0:T(8,128)(2,1)S(1)} %collective-permute-done.12.refs_2_, ...), custom_call_target="tpu_custom_call" | custom-call | tf_op jit(solution)/shard_map/norm/pallas_call | solution.py:503
  124.9 3.1 %collective-permute-start.19 = (bf16[16,3072]{1,0:T(8,128)(2,1)S(1)}, bf16[16,3072]{1,0:T(8,128)(2,1)S(1)}, u32[]{:S(2)}, u32[]{:S(2)}) collective-permute-start(bf16[16,3072]{1,0:T(8,128)(2,1)S(1)} %get-tuple-element.25), channel_id=1, source_target_pairs={{0,8},{8,16},{16,24},{24,32},{32,40},{40,48},{48,56},{56,64},{64,7... | collective-permute-start | bytes 294920 | tf_op jit(solution)/shard_map/ppermute | solution.py:518
  128.0 0.6 pad_maximum_fusion.4.taps_ref
  128.7 4.5 %collective-permute-done.19 = bf16[16,3072]{1,0:T(8,128)(2,1)S(1)} collective-permute-done((bf16[16,3072]{1,0:T(8,128)(2,1)S(1)}, bf16[16,3072]{1,0:T(8,128)(2,1)S(1)}, u32[]{:S(2)}, u32[]{:S(2)}) %collective-permute-start.19) | collective-permute-done | bytes 98336 | tf_op jit(solution)/shard_map/ppermute | solution.py:518
  133.2 0.7 constant_dynamic-update-slice_fusion.2.x_ref
  133.8 7.8 %all-gather.2.cloned.1.call-done.wg_ref.wv_ref.w_ref.wa_ref.wb_ref.ta_ref.tb_ref = bf16[3072,3200]{1,0:T(8,128)(2,1)} async-done(((bf16[192,3200]{1,0:T(8,128)(2,1)}), bf16[3072,3200]{1,0:T(8,128)(2,1)}) %all-gather.2.cloned.1.call-update) | async-done | bytes 19660816 | tf_op jit(solution)/shard_map/all_gather | solution.py:426
  141.6 22.4 %mixer.1 = (bf16[768,1152]{1,0:T(8,128)(2,1)}, bf16[1,768,384]{2,1,0:T(8,128)(2,1)}, bf16[1,768,384]{2,1,0:T(8,128)(2,1)}) custom-call(s32[8]{0:T(128)} %stack.3.order_ref, bf16[784,3072]{1,0:T(8,128)(2,1)} %constant_dynamic-update-slice_fusion.2.x_ref, f32[768,128]{1,0:T(8,128)} %get-tuple-element.26.near_ref, f32[768,128]{1,0:T(8,128)} %get-tuple-element.27.far_ref, ...), custom_call_target="tpu_custom_call" | custom-call | tf_op jit(solution)/shard_map/mixer/pallas_call | solution.py:524
  164.0 1.5 copy-done
  165.5 6.3 %shard_map.155 = (bf16[2,768,384]{2,1,0:T(8,128)(2,1)S(1)}, bf16[2,768,384]{2,1,0:T(8,128)(2,1)S(1)}) custom-call(s32[8]{0:T(128)S(1)} %copy-done.1, bf16[768,1152]{1,0:T(8,128)(2,1)S(1)} %copy-done, bf16[3072,3200]{1,0:T(8,128)(2,1)} %all-gather.2.cloned.1.call-done.wg_ref.wv_ref.w_ref.wa_ref.wb_ref.ta_ref.tb_ref, ...), custom_call_target="tpu_custom_call" | custom-call | tf_op jit(solution)/shard_map/pallas_call | solution.py:569
  172.4 4.1 %shard_map.154 = (bf16[1,768,384]{2,1,0:T(8,128)(2,1)S(1)}, bf16[1,768,384]{2,1,0:T(8,128)(2,1)S(1)}) custom-call(s32[8]{0:T(128)S(1)} %copy-done.1, bf16[768,1152]{1,0:T(8,128)(2,1)S(1)} %copy-done, bf16[3072,3200]{1,0:T(8,128)(2,1)} %all-gather.2.cloned.1.call-done.wg_ref.wv_ref.w_ref.wa_ref.wb_ref.ta_ref.tb_ref, ...), custom_call_target="tpu_custom_call" | custom-call | tf_op jit(solution)/shard_map/pallas_call | solution.py:569
  177.1 1.6 collective-permute-start.23
  178.6 1.7 collective-permute-start.25
  180.7 6.8 %collective-permute-done.23 = bf16[384,384]{1,0:T(8,128)(2,1)S(1)} collective-permute-done((bf16[384,384]{1,0:T(8,128)(2,1)S(1)}, bf16[384,384]{1,0:T(8,128)(2,1)S(1)}, u32[]{:S(2)}, u32[]{:S(2)}) %collective-permute-start.23) | collective-permute-done | bytes 294944 | tf_op jit(solution)/shard_map/ppermute | solution.py:357
  188.2 3.0 %collective-permute-start.26 = (bf16[768,384]{1,0:T(8,128)(2,1)S(1)}, bf16[768,384]{1,0:T(8,128)(2,1)S(1)}, u32[]{:S(2)}, u32[]{:S(2)}) collective-permute-start(bf16[768,384]{1,0:T(8,128)(2,1)S(1)} %pad_maximum_fusion.3), channel_id=1, source_target_pairs={{0,6},{2,0},{4,2},{6,4},{1,7},{3,1},{5,3},{7,5},{8,14},{10,8},{12,... | collective-permute-start | bytes 1769480 | tf_op jit(solution)/shard_map/ppermute | solution.py:357
  191.2 12.2 %collective-permute-done.24 = bf16[768,384]{1,0:T(8,128)(2,1)S(1)} collective-permute-done((bf16[768,384]{1,0:T(8,128)(2,1)S(1)}, bf16[768,384]{1,0:T(8,128)(2,1)S(1)}, u32[]{:S(2)}, u32[]{:S(2)}) %collective-permute-start.24) | collective-permute-done | bytes 589856 | tf_op jit(solution)/shard_map/ppermute | solution.py:357
  203.5 2.6 %fusion.2 = bf16[768,384]{1,0:T(8,128)(2,1)} fusion(bf16[768,384]{1,0:T(8,128)(2,1)S(1)} %collective-permute-done.26, bf16[768,384]{1,0:T(8,128)(2,1)S(1)} %collective-permute-done.24, bf16[1,768,384]{2,1,0:T(8,128)(2,1)S(1)} %collective-permute-done.20, bf16[1,768,384]{2,1,0:T(8,128)(2,1)S(1)} %get-tuple-element.29, bf16[768,384]{1,0:T(8,128)(2,1)S(1)} %copy-done.11, ...), kind=kLoop, calls=%fused_computation.3 | loop fusion | flops 5308416 | bytes 5898240 | tf_op jit(solution)/shard_map/convert_element_type | solution.py:588
  (109 shorter events, 7.2 us)
Async XLA Ops:
  6.5 135.1 %all-gather.2.cloned.1.call-start = ((), (), s32[]{:S(2)}) async-start(), calls=%async_computation | async-start | bytes 20889600 | tf_op jit(solution)/shard_map/all_gather | solution.py:426
  9.0 1.9 copy-start.14
  9.0 2.8 %copy-start.22 = (s32[768]{0:T(1024)S(1)}, s32[768]{0:T(1024)}, u32[]{:S(2)}) copy-start(s32[768]{0:T(1024)} %param.23) | copy-start | bytes 9220
  9.9 22.8 %copy-start.23 = (s32[4]{0:T(128)S(1)}, s32[4]{0:T(128)}, u32[]{:S(2)}) copy-start(s32[4]{0:T(128)} %constant.35.clone) | copy-start | bytes 52
  9.9 24.1 %copy-start.15 = (bf16[768,192]{0,1:T(8,128)(2,1)S(1)}, bf16[768,192]{0,1:T(8,128)(2,1)}, u32[]{:S(2)}) copy-start(bf16[768,192]{0,1:T(8,128)(2,1)} %param.17) | copy-start | bytes 884740
  10.8 24.1 %copy-start.16 = (bf16[768,192]{0,1:T(8,128)(2,1)S(1)}, bf16[768,192]{0,1:T(8,128)(2,1)}, u32[]{:S(2)}) copy-start(bf16[768,192]{0,1:T(8,128)(2,1)} %param.20) | copy-start | bytes 884740
  16.0 29.2 %collective-permute-start = (bf16[112,192]{1,0:T(8,128)(2,1)}, bf16[112,192]{1,0:T(8,128)(2,1)S(1)}, u32[]{:S(2)}, u32[]{:S(2)}) collective-permute-start(bf16[112,192]{1,0:T(8,128)(2,1)} %get-tuple-element.22), channel_id=1, source_target_pairs={{0,8},{8,16},{16,24},{24,32},{32,40},{40,48},{48,56},{56,64},{64,7... | collective-permute-start | bytes 129032 | tf_op jit(solution)/shard_map/ppermute | solution.py:451
  19.5 25.7 %collective-permute-start.1 = (bf16[112,192]{1,0:T(8,128)(2,1)}, bf16[112,192]{1,0:T(8,128)(2,1)S(1)}, u32[]{:S(2)}, u32[]{:S(2)}) collective-permute-start(bf16[112,192]{1,0:T(8,128)(2,1)} %get-tuple-element.22), channel_id=1, source_target_pairs={{0,16},{8,24},{16,32},{24,40},{32,48},{40,56},{48,64},{56,72},{64,... | collective-permute-start | bytes 129032 | tf_op jit(solution)/shard_map/ppermute | solution.py:451
  24.1 21.1 %collective-permute-start.2 = (bf16[112,192]{1,0:T(8,128)(2,1)}, bf16[112,192]{1,0:T(8,128)(2,1)S(1)}, u32[]{:S(2)}, u32[]{:S(2)}) collective-permute-start(bf16[112,192]{1,0:T(8,128)(2,1)} %get-tuple-element.22), channel_id=1, source_target_pairs={{0,24},{8,32},{16,40},{24,48},{32,56},{40,64},{48,72},{56,80},{64,... | collective-permute-start | bytes 129032 | tf_op jit(solution)/shard_map/ppermute | solution.py:451
  28.8 16.4 %collective-permute-start.3 = (bf16[112,192]{1,0:T(8,128)(2,1)}, bf16[112,192]{1,0:T(8,128)(2,1)S(1)}, u32[]{:S(2)}, u32[]{:S(2)}) collective-permute-start(bf16[112,192]{1,0:T(8,128)(2,1)} %get-tuple-element.22), channel_id=1, source_target_pairs={{0,32},{8,40},{16,48},{24,56},{32,64},{40,72},{48,80},{56,88},{64,... | collective-permute-start | bytes 129032 | tf_op jit(solution)/shard_map/ppermute | solution.py:451
  56.2 6.9 %copy-start.3 = (bf16[8,768,384]{2,1,0:T(8,128)(2,1)S(1)}, bf16[8,768,384]{2,1,0:T(8,128)(2,1)}, u32[]{:S(2)}) copy-start(bf16[8,768,384]{2,1,0:T(8,128)(2,1)} %get-tuple-element.23) | copy-start | bytes 14155780
  58.1 5.0 %collective-permute-start.5 = (bf16[2,768,384]{2,1,0:T(8,128)(2,1)S(1)}, bf16[2,768,384]{2,1,0:T(8,128)(2,1)S(1)}, u32[]{:S(2)}, u32[]{:S(2)}) collective-permute-start(bf16[2,768,384]{2,1,0:T(8,128)(2,1)S(1)} %slice.165), channel_id=1, source_target_pairs={{0,1},{1,0},{2,3},{3,2},{4,5},{5,4},{6,7},{7,6},{8,9},{9,8},{10,11... | collective-permute-start | bytes 3538952 | tf_op jit(solution)/shard_map/ppermute | solution.py:361
  61.0 2.1 collective-permute-start.6
  61.1 16.5 %collective-permute-start.4 = (bf16[1,768,384]{2,1,0:T(8,128)(2,1)S(1)}, bf16[1,768,384]{2,1,0:T(8,128)(2,1)S(1)}, u32[]{:S(2)}, u32[]{:S(2)}) collective-permute-start(bf16[1,768,384]{2,1,0:T(8,128)(2,1)S(1)} %get-tuple-element.37), channel_id=1, source_target_pairs={{0,1},{1,0},{2,3},{3,2},{4,5},{5,4},{6,7},{7,6},{8,9},{9,8},{10,11... | collective-permute-start | bytes 1769480 | tf_op jit(solution)/shard_map/ppermute | solution.py:361
  63.5 10.4 %collective-permute-start.7 = (bf16[384,384]{1,0:T(8,128)(2,1)S(1)}, bf16[384,384]{1,0:T(8,128)(2,1)S(1)}, u32[]{:S(2)}, u32[]{:S(2)}) collective-permute-start(bf16[384,384]{1,0:T(8,128)(2,1)S(1)} %get-tuple-element.44), channel_id=1, source_target_pairs={{0,2},{2,4},{4,6},{6,0},{1,3},{3,5},{5,7},{7,1},{8,10},{10,12},{12... | collective-permute-start | bytes 884744 | tf_op jit(solution)/shard_map/ppermute | solution.py:357
  65.2 9.2 %collective-permute-start.9 = (bf16[384,384]{1,0:T(8,128)(2,1)S(1)}, bf16[384,384]{1,0:T(8,128)(2,1)S(1)}, u32[]{:S(2)}, u32[]{:S(2)}) collective-permute-start(bf16[384,384]{1,0:T(8,128)(2,1)S(1)} %get-tuple-element.45), channel_id=1, source_target_pairs={{0,6},{2,0},{4,2},{6,4},{1,7},{3,1},{5,3},{7,5},{8,14},{10,8},{12,... | collective-permute-start | bytes 884744 | tf_op jit(solution)/shard_map/ppermute | solution.py:357
  74.0 15.9 %copy-start.4 = (bf16[768,384]{1,0:T(8,128)(2,1)S(1)}, bf16[768,384]{1,0:T(8,128)(2,1)}, u32[]{:S(2)}) copy-start(bf16[768,384]{1,0:T(8,128)(2,1)} %param.16) | copy-start | bytes 1769476
  74.0 15.9 %collective-permute-start.8 = (bf16[768,384]{1,0:T(8,128)(2,1)S(1)}, bf16[768,384]{1,0:T(8,128)(2,1)S(1)}, u32[]{:S(2)}, u32[]{:S(2)}) collective-permute-start(bf16[768,384]{1,0:T(8,128)(2,1)S(1)} %pad_maximum_fusion), channel_id=1, source_target_pairs={{0,2},{2,4},{4,6},{6,0},{1,3},{3,5},{5,7},{7,1},{8,10},{10,12},{12... | collective-permute-start | bytes 1769480 | tf_op jit(solution)/shard_map/ppermute | solution.py:357
  74.6 15.4 %collective-permute-start.10 = (bf16[768,384]{1,0:T(8,128)(2,1)S(1)}, bf16[768,384]{1,0:T(8,128)(2,1)S(1)}, u32[]{:S(2)}, u32[]{:S(2)}) collective-permute-start(bf16[768,384]{1,0:T(8,128)(2,1)S(1)} %pad_maximum_fusion.1), channel_id=1, source_target_pairs={{0,6},{2,0},{4,2},{6,4},{1,7},{3,1},{5,3},{7,5},{8,14},{10,8},{12,... | collective-permute-start | bytes 1769480 | tf_op jit(solution)/shard_map/ppermute | solution.py:357
  77.6 12.8 %copy-start.6 = (bf16[1,768,384]{2,1,0:T(8,128)(2,1)}, bf16[1,768,384]{2,1,0:T(8,128)(2,1)S(1)}, u32[]{:S(2)}) copy-start(bf16[1,768,384]{2,1,0:T(8,128)(2,1)S(1)} %collective-permute-done.4) | copy-start | bytes 1769476
  90.0 1.0 copy-start.10
  91.0 23.6 %copy-start.17 = (f32[3,1056]{1,0:T(4,128)S(1)}, f32[3,1056]{1,0:T(4,128)}, u32[]{:S(2)}) copy-start(f32[3,1056]{1,0:T(4,128)} %param.29) | copy-start | bytes 38020
  91.0 25.7 %copy-start.2 = (f32[3072]{0:T(1024)S(1)}, f32[3072]{0:T(1024)}, u32[]{:S(2)}) copy-start(f32[3072]{0:T(1024)} %param.26) | copy-start | bytes 36868
  91.0 15.1 %collective-permute-start.11 = (bf16[768,384]{1,0:T(8,128)(2,1)S(1)}, bf16[768,384]{1,0:T(8,128)(2,1)S(1)}, u32[]{:S(2)}, u32[]{:S(2)}) collective-permute-start(bf16[768,384]{1,0:T(8,128)(2,1)S(1)} %fusion.21.refs_0_), channel_id=1, source_target_pairs={{0,2},{2,4},{4,6},{6,0},{1,3},{3,5},{5,7},{7,1},{8,10},{10,12},{12... | collective-permute-start | bytes 1769480 | tf_op jit(solution)/shard_map/ppermute | solution.py:357
  91.4 14.8 %collective-permute-start.12 = (bf16[768,384]{1,0:T(8,128)(2,1)S(1)}, bf16[768,384]{1,0:T(8,128)(2,1)S(1)}, u32[]{:S(2)}, u32[]{:S(2)}) collective-permute-start(bf16[768,384]{1,0:T(8,128)(2,1)S(1)} %fusion.21.refs_0_), channel_id=1, source_target_pairs={{0,6},{2,0},{4,2},{6,4},{1,7},{3,1},{5,3},{7,5},{8,14},{10,8},{12,... | collective-permute-start | bytes 1769480 | tf_op jit(solution)/shard_map/ppermute | solution.py:357
  106.1 8.1 %collective-permute-start.13 = (bf16[384,384]{1,0:T(8,128)(2,1)S(1)}, bf16[384,384]{1,0:T(8,128)(2,1)S(1)}, u32[]{:S(2)}, u32[]{:S(2)}) collective-permute-start(bf16[384,384]{1,0:T(8,128)(2,1)S(1)} %slice.211), channel_id=1, source_target_pairs={{0,2},{2,4},{4,6},{6,0},{1,3},{3,5},{5,7},{7,1},{8,10},{10,12},{12... | collective-permute-start | bytes 884744 | tf_op jit(solution)/shard_map/ppermute | solution.py:357
  106.3 8.0 %collective-permute-start.14 = (bf16[384,384]{1,0:T(8,128)(2,1)S(1)}, bf16[384,384]{1,0:T(8,128)(2,1)S(1)}, u32[]{:S(2)}, u32[]{:S(2)}) collective-permute-start(bf16[384,384]{1,0:T(8,128)(2,1)S(1)} %slice.212), channel_id=1, source_target_pairs={{0,6},{2,0},{4,2},{6,4},{1,7},{3,1},{5,3},{7,5},{8,14},{10,8},{12,... | collective-permute-start | bytes 884744 | tf_op jit(solution)/shard_map/ppermute | solution.py:357
  109.5 7.2 %collective-permute-start.15 = (bf16[768,384]{1,0:T(8,128)(2,1)S(1)}, bf16[768,384]{1,0:T(8,128)(2,1)S(1)}, u32[]{:S(2)}, u32[]{:S(2)}) collective-permute-start(bf16[768,384]{1,0:T(8,128)(2,1)S(1)} %fusion.21.refs_0_), channel_id=1, source_target_pairs={{0,1},{1,0},{2,3},{3,2},{4,5},{5,4},{6,7},{7,6},{8,9},{9,8},{10,11... | collective-permute-start | bytes 1769480 | tf_op jit(solution)/shard_map/ppermute | solution.py:361
  109.5 7.2 %collective-permute-start.16 = (bf16[768,384]{1,0:T(8,128)(2,1)S(1)}, bf16[768,384]{1,0:T(8,128)(2,1)S(1)}, u32[]{:S(2)}, u32[]{:S(2)}) collective-permute-start(bf16[768,384]{1,0:T(8,128)(2,1)S(1)} %collective-permute-done.11.refs_1_), channel_id=1, source_target_pairs={{0,1},{1,0},{2,3},{3,2},{4,5},{5,4},{6,7},{7,6},{8,9},{9,8},{10,11... | collective-permute-start | bytes 1769480 | tf_op jit(solution)/shard_map/ppermute | solution.py:361
  110.1 6.7 %collective-permute-start.17 = (bf16[768,384]{1,0:T(8,128)(2,1)S(1)}, bf16[768,384]{1,0:T(8,128)(2,1)}, u32[]{:S(2)}, u32[]{:S(2)}) collective-permute-start(bf16[768,384]{1,0:T(8,128)(2,1)S(1)} %collective-permute-done.12.refs_2_), channel_id=1, source_target_pairs={{0,1},{1,0},{2,3},{3,2},{4,5},{5,4},{6,7},{7,6},{8,9},{9,8},{10,11... | collective-permute-start | bytes 1769480 | tf_op jit(solution)/shard_map/ppermute | solution.py:361
  114.3 2.4 %collective-permute-start.18 = (bf16[768,384]{1,0:T(8,128)(2,1)S(1)}, bf16[768,384]{1,0:T(8,128)(2,1)}, u32[]{:S(2)}, u32[]{:S(2)}) collective-permute-start(bf16[768,384]{1,0:T(8,128)(2,1)S(1)} %constant_dynamic-update-slice_fusion.refs_3_), channel_id=1, source_target_pairs={{0,1},{1,0},{2,3},{3,2},{4,5},{5,4},{6,7},{7,6},{8,9},{9,8},{10,11... | collective-permute-start | bytes 1769480 | tf_op jit(solution)/shard_map/ppermute | solution.py:361
  116.7 11.3 %slice-start = ((f32[3,1056]{1,0:T(4,128)}), f32[3,1024]{1,0:T(4,128)S(1)}, s32[]{:S(2)}) async-start(f32[3,1056]{1,0:T(4,128)} %param.29), calls=%async_computation.1 | async-start | bytes 32768 | tf_op jit(solution)/shard_map/slice | solution.py:432
  124.9 8.3 %collective-permute-start.19 = (bf16[16,3072]{1,0:T(8,128)(2,1)S(1)}, bf16[16,3072]{1,0:T(8,128)(2,1)S(1)}, u32[]{:S(2)}, u32[]{:S(2)}) collective-permute-start(bf16[16,3072]{1,0:T(8,128)(2,1)S(1)} %get-tuple-element.25), channel_id=1, source_target_pairs={{0,8},{8,16},{16,24},{24,32},{32,40},{40,48},{48,56},{56,64},{64,7... | collective-permute-start | bytes 294920 | tf_op jit(solution)/shard_map/ppermute | solution.py:518
  141.6 22.4 %copy-start.1 = (s32[8]{0:T(128)S(1)}, s32[8]{0:T(128)}, u32[]{:S(2)}) copy-start(s32[8]{0:T(128)} %stack.3.order_ref) | copy-start | bytes 100
  164.0 1.5 copy-start
  165.5 6.4 %copy-start.24 = (bf16[1,768,384]{2,1,0:T(8,128)(2,1)S(1)}, bf16[1,768,384]{2,1,0:T(8,128)(2,1)}, u32[]{:S(2)}) copy-start(bf16[1,768,384]{2,1,0:T(8,128)(2,1)} %get-tuple-element.34) | copy-start | bytes 1769476
  171.8 8.6 %collective-permute-start.21 = (bf16[2,768,384]{2,1,0:T(8,128)(2,1)S(1)}, bf16[2,768,384]{2,1,0:T(8,128)(2,1)S(1)}, u32[]{:S(2)}, u32[]{:S(2)}) collective-permute-start(bf16[2,768,384]{2,1,0:T(8,128)(2,1)S(1)} %get-tuple-element.32), channel_id=1, source_target_pairs={{0,1},{1,0},{2,3},{3,2},{4,5},{5,4},{6,7},{7,6},{8,9},{9,8},{10,11... | collective-permute-start | bytes 3538952 | tf_op jit(solution)/shard_map/ppermute | solution.py:361
  171.9 5.0 %copy-start.12 = (bf16[1,768,384]{2,1,0:T(8,128)(2,1)S(1)}, bf16[1,768,384]{2,1,0:T(8,128)(2,1)}, u32[]{:S(2)}) copy-start(bf16[1,768,384]{2,1,0:T(8,128)(2,1)} %get-tuple-element.33) | copy-start | bytes 1769476
  171.9 5.0 %collective-permute-start.22 = (bf16[1,768,384]{2,1,0:T(8,128)(2,1)S(1)}, bf16[1,768,384]{2,1,0:T(8,128)(2,1)S(1)}, u32[]{:S(2)}, u32[]{:S(2)}) collective-permute-start(bf16[1,768,384]{2,1,0:T(8,128)(2,1)S(1)} %copy-done.24), channel_id=1, source_target_pairs={{0,1},{1,0},{2,3},{3,2},{4,5},{5,4},{6,7},{7,6},{8,9},{9,8},{10,11... | collective-permute-start | bytes 1769480 | tf_op jit(solution)/shard_map/ppermute | solution.py:361
  176.4 14.8 %collective-permute-start.20 = (bf16[1,768,384]{2,1,0:T(8,128)(2,1)S(1)}, bf16[1,768,384]{2,1,0:T(8,128)(2,1)S(1)}, u32[]{:S(2)}, u32[]{:S(2)}) collective-permute-start(bf16[1,768,384]{2,1,0:T(8,128)(2,1)S(1)} %get-tuple-element.30), channel_id=1, source_target_pairs={{0,1},{1,0},{2,3},{3,2},{4,5},{5,4},{6,7},{7,6},{8,9},{9,8},{10,11... | collective-permute-start | bytes 1769480 | tf_op jit(solution)/shard_map/ppermute | solution.py:361
  177.1 10.4 %collective-permute-start.23 = (bf16[384,384]{1,0:T(8,128)(2,1)S(1)}, bf16[384,384]{1,0:T(8,128)(2,1)S(1)}, u32[]{:S(2)}, u32[]{:S(2)}) collective-permute-start(bf16[384,384]{1,0:T(8,128)(2,1)S(1)} %get-tuple-element.42), channel_id=1, source_target_pairs={{0,2},{2,4},{4,6},{6,0},{1,3},{3,5},{5,7},{7,1},{8,10},{10,12},{12... | collective-permute-start | bytes 884744 | tf_op jit(solution)/shard_map/ppermute | solution.py:357
  178.6 9.4 %collective-permute-start.25 = (bf16[384,384]{1,0:T(8,128)(2,1)S(1)}, bf16[384,384]{1,0:T(8,128)(2,1)S(1)}, u32[]{:S(2)}, u32[]{:S(2)}) collective-permute-start(bf16[384,384]{1,0:T(8,128)(2,1)S(1)} %get-tuple-element.43), channel_id=1, source_target_pairs={{0,6},{2,0},{4,2},{6,4},{1,7},{3,1},{5,3},{7,5},{8,14},{10,8},{12,... | collective-permute-start | bytes 884744 | tf_op jit(solution)/shard_map/ppermute | solution.py:357
  187.6 15.8 %collective-permute-start.24 = (bf16[768,384]{1,0:T(8,128)(2,1)S(1)}, bf16[768,384]{1,0:T(8,128)(2,1)S(1)}, u32[]{:S(2)}, u32[]{:S(2)}) collective-permute-start(bf16[768,384]{1,0:T(8,128)(2,1)S(1)} %pad_maximum_fusion.2), channel_id=1, source_target_pairs={{0,2},{2,4},{4,6},{6,0},{1,3},{3,5},{5,7},{7,1},{8,10},{10,12},{12... | collective-permute-start | bytes 1769480 | tf_op jit(solution)/shard_map/ppermute | solution.py:357
  188.0 15.5 %copy-start.5 = (bf16[768,384]{1,0:T(8,128)(2,1)S(1)}, bf16[768,384]{1,0:T(8,128)(2,1)}, u32[]{:S(2)}) copy-start(bf16[768,384]{1,0:T(8,128)(2,1)} %param.16) | copy-start | bytes 1769476
  188.0 15.5 %copy-start.7 = (bf16[1,768,384]{2,1,0:T(8,128)(2,1)S(1)}, bf16[1,768,384]{2,1,0:T(8,128)(2,1)}, u32[]{:S(2)}) copy-start(bf16[1,768,384]{2,1,0:T(8,128)(2,1)} %copy-done.6) | copy-start | bytes 1769476
  188.0 15.5 %copy-start.9 = (bf16[768,384]{1,0:T(8,128)(2,1)S(1)}, bf16[768,384]{1,0:T(8,128)(2,1)}, u32[]{:S(2)}) copy-start(bf16[768,384]{1,0:T(8,128)(2,1)} %copy-done.8) | copy-start | bytes 1769476
  188.0 15.5 %copy-start.11 = (bf16[768,384]{1,0:T(8,128)(2,1)S(1)}, bf16[768,384]{1,0:T(8,128)(2,1)}, u32[]{:S(2)}) copy-start(bf16[768,384]{1,0:T(8,128)(2,1)} %copy-done.10) | copy-start | bytes 1769476
  188.2 15.3 %collective-permute-start.26 = (bf16[768,384]{1,0:T(8,128)(2,1)S(1)}, bf16[768,384]{1,0:T(8,128)(2,1)S(1)}, u32[]{:S(2)}, u32[]{:S(2)}) collective-permute-start(bf16[768,384]{1,0:T(8,128)(2,1)S(1)} %pad_maximum_fusion.3), channel_id=1, source_target_pairs={{0,6},{2,0},{4,2},{6,4},{1,7},{3,1},{5,3},{7,5},{8,14},{10,8},{12,... | collective-permute-start | bytes 1769480 | tf_op jit(solution)/shard_map/ppermute | solution.py:357
  (6 other events, 4.4 us)
Sparse Core Ops, SparseCore 0:
  9.5 132.0 all-gather.1

commit v4 on v2

--- a/solution.py
+++ b/solution.py
@@ -21,6 +21,17 @@
 
 def in_first_head(shape):
     return lax.broadcasted_iota(jnp.int32, shape, len(shape) - 1) < DH
+
+
+def pack_kernel(gate_ref, value_ref, down_ref, out_ref):
+    rows, hidden = gate_ref.shape
+    main = hidden // 128 * 128
+    tails = []
+    for k, ref in enumerate((gate_ref, value_ref, down_ref)):
+        out_ref[:, k * main : (k + 1) * main] = ref[:, :main]
+        tails.append(ref[:, main:])
+    tails.append(jnp.zeros((rows, 128 - 3 * (hidden - main)), BF16))
+    out_ref[:, 3 * main :] = jnp.concatenate(tails, axis=1)
 
 
 def state_kernel(k_ref, v_ref, in_ref, forget_ref, doc_ref, pay_ref, row_ref, col_ref, scr):
@@ -115,7 +126,8 @@
 def mix_kernel(
     order_ref, q_ref, gate_ref, local_ref, row_ref, col_ref, gain_ref, w_ref, *refs
 ):
-    pays, (out_ref, near_ref, far_ref, mix_ref) = refs[:-4], refs[-4:]
+    w_own_ref, *pays = refs[:-5]
+    swap_ref, own_out_ref, near_ref, far_ref, mix_ref = refs[-5:]
     tokens, width = q_ref.shape
 
     @pl.when(pl.program_id(0) == 0)
@@ -166,7 +178,9 @@
         near_ref[...] = (one == doc).astype(F32)
         far_ref[...] = (two == doc).astype(F32)
 
-    out_ref[0] = jnp.dot(mix_ref[...], w_ref[...], preferred_element_type=F32).astype(BF16)
+    mix = mix_ref[...]
+    swap_ref[0] = jnp.dot(mix, w_ref[...], preferred_element_type=F32).astype(BF16)
+    own_out_ref[0] = jnp.dot(mix, w_own_ref[...], preferred_element_type=F32).astype(BF16)
 
 
 def norm_kernel(order_ref, *refs):
@@ -197,20 +211,37 @@
     wg_ref,
     wv_ref,
     wt_ref,
-    wda_ref,
-    wdb_ref,
-    wdta_ref,
-    wdtb_ref,
-    out_ref,
+    w_ref,
+    h_ref,
+    swap_ref,
+    own_ref,
     gate_scr,
     value_scr,
-    h_scr,
+    tail_scr,
+    down_scr,
+    sems,
 ):
     tokens = near_ref.shape[0]
     tiles, _, tile = taps_ref.shape
     tiles -= 1
     main = tiles * tile
+    parts, cols, _ = down_scr.shape
     j = pl.program_id(0)
+
+    def copies(n):
+        rows = pl.ds(pl.multiple_of(order_ref[n] * cols, 128), cols)
+        return (
+            pltpu.make_async_copy(
+                w_ref.at[rows, pl.ds(2 * main, main)],
+                down_scr.at[n, :, pl.ds(0, main)],
+                sems.at[2 * n],
+            ),
+            pltpu.make_async_copy(
+                w_ref.at[rows, pl.ds(3 * main, 128)],
+                down_scr.at[n, :, pl.ds(main, 128)],
+                sems.at[2 * n + 1],
+            ),
+        )
 
     def hidden(gate, value, taps, rows):
         near, far = near_ref[rows, :], far_ref[rows, :]
@@ -221,7 +252,8 @@
             + taps[1:2, :] * (near * one)
             + taps[0:1, :] * (far * two)
         )
-        return conv / (1.0 + jnp.exp(-conv)) * value
+        scaled = 0.5 * conv
+        return (scaled + scaled * jnp.tanh(scaled)) * value
 
     block = 96
 
@@ -230,28 +262,19 @@
             for half in range(0, tile, 128):
                 lanes = slice(half, half + 128)
                 done = hidden(
-                    gate_scr[slot, start : start + block + HALO, lanes].astype(F32),
-                    value_scr[slot, start + HALO : start + HALO + block, lanes].astype(F32),
+                    gate_scr[slot, start : start + block + HALO, lanes],
+                    value_scr[slot, start + HALO : start + HALO + block, lanes],
                     taps_ref[at, :, lanes],
                     slice(start, start + block),
                 )
-                spot = pl.multiple_of(at * tile + half, 128)
-                h_scr[start : start + block, pl.ds(spot, 128)] = done.astype(BF16)
-
-    @pl.when(j < tiles)
-    def _():
-        gate_scr[j % 2] = jnp.dot(x_ref[...], wg_ref[...], preferred_element_type=F32).astype(BF16)
-        value_scr[j % 2] = jnp.dot(x_ref[...], wv_ref[...], preferred_element_type=F32).astype(BF16)
-
-    @pl.when((j > 0) & (j <= tiles))
-    def _():
-        finish((j - 1) % 2, j - 1)
-
-    @pl.when(j == tiles)
-    def _():
-        both = jnp.dot(x_ref[...], wt_ref[...], preferred_element_type=F32).astype(BF16)
+                spot = at * tile + half
+                if not isinstance(at, int):
+                    spot = pl.multiple_of(spot, 128)
+                h_ref[start : start + block, pl.ds(spot, 128)] = done.astype(BF16)
+
+    def finish_tail():
         for start in range(0, tokens, block):
-            part = both[start : start + block + HALO, :].astype(F32)
+            part = tail_scr[start : start + block + HALO, :]
             lane = lax.broadcasted_iota(jnp.int32, (block, 128), 1)
             mine = (lane >= 64) & (lane < 96)
             done = hidden(
@@ -260,18 +283,72 @@
                 taps_ref[tiles, :, 0:128],
                 slice(start, start + block),
             )
-            h_scr[start : start + block, main:] = jnp.where(mine, done, 0.0).astype(BF16)
+            h_ref[start : start + block, main:] = jnp.where(mine, done, 0.0).astype(BF16)
+
+    def project(slot):
+        gate_scr[slot] = jnp.dot(x_ref[...], wg_ref[...], preferred_element_type=F32)
+        value_scr[slot] = jnp.dot(x_ref[...], wv_ref[...], preferred_element_type=F32)
+
+    def product(n, cuts):
+        total = None
+        for cut in cuts:
+            term = lax.dot_general(
+                h_ref[:, cut],
+                down_scr[n, :, cut],
+                (((1,), (1,)), ((), ())),
+                preferred_element_type=F32,
+            )
+            total = term if total is None else total + term
+        return total.astype(BF16)
+
+    @pl.when(j == 0)
+    def _():
+        for n in range(parts):
+            for copy in copies(n):
+                copy.start()
+        tail_scr[...] = jnp.dot(x_ref[...], wt_ref[...], preferred_element_type=F32)
+        project(0)
+
+    @pl.when(j == 1)
+    def _():
+        project(1)
+        finish_tail()
+        finish(0, 0)
+
+    @pl.when((j > 1) & (j < tiles))
+    def _():
+        project(j % 2)
+        finish((j - 1) % 2, j - 1)
+
+    @pl.when(j >= tiles)
+    def _():
+        for k in range(2):
+            for copy in copies(2 * (j - tiles) + k):
+                copy.wait()
+
+    @pl.when(j == tiles)
+    def _():
+        finish((tiles - 1) % 2, tiles - 1)
+        known = main - tile
+        cuts = (slice(0, known), slice(main, main + 128), slice(known, main))
+        swap_ref[0] = product(0, cuts)
+        own_ref[0] = product(1, cuts)
 
     @pl.when(j > tiles)
     def _():
-        contract = (((1,), (1,)), ((), ()))
-        for p, (wd_ref, wdt_ref) in enumerate(((wda_ref, wdta_ref), (wdb_ref, wdtb_ref))):
-            out_ref[p] = (
-                lax.dot_general(h_scr[:, 0:main], wd_ref[...], contract, preferred_element_type=F32)
-                + lax.dot_general(
-                    h_scr[:, main:], wdt_ref[...], contract, preferred_element_type=F32
-                )
-            ).astype(BF16)
+        n = 2 * (j - tiles)
+        swap_ref[0] = product(n, (slice(None),))
+        own_ref[0] = product(n + 1, (slice(None),))
+
+
+def down_kernel(order_ref, h_ref, wa_ref, wb_ref, ta_ref, tb_ref, swap_ref, own_ref):
+    main = wa_ref.shape[1]
+    contract = (((1,), (1,)), ((), ()))
+    for ref, w_ref, t_ref in ((swap_ref, wa_ref, ta_ref), (own_ref, wb_ref, tb_ref)):
+        ref[0] = (
+            lax.dot_general(h_ref[:, :main], w_ref[...], contract, preferred_element_type=F32)
+            + lax.dot_general(h_ref[:, main:], t_ref[...], contract, preferred_element_type=F32)
+        ).astype(BF16)
 
 
 def added(*terms):
@@ -290,15 +367,20 @@
     return lax.ppermute(value, "c", [(0, 1), (1, 0)])
 
 
-def summed_over_tp(shares):
-    half = shares.shape[2] // 2
-    other = swapped(shares[1])
-    pair = [added(shares[0, k], other[k]).astype(BF16) for k in range(4)]
-    up = shifted(pair[2][:half], 1)
-    down = shifted(pair[2][half:], -1)
-    up = jnp.concatenate([added(pair[1][:half], up).astype(BF16), pair[1][half:]], axis=0)
-    down = jnp.concatenate([pair[3][:half], added(pair[3][half:], down).astype(BF16)], axis=0)
-    return added(pair[0], shifted(up, 1), shifted(down, -1))
+def summed_over_tp(swap, own, last):
+    other = swapped(swap)
+    far, up, down = (added(own[k], other[k]) for k in range(3))
+    half = far.shape[0] // 2
+    far = far.astype(BF16)
+    far_up, far_down = shifted(far[:half], 1), shifted(far[half:], -1)
+    below = shifted(up[half:].astype(BF16), 1)
+    above = shifted(down[:half].astype(BF16), -1)
+    swap, own = last()
+    near = added(own, swapped(swap))
+    up = (up[:half] + far_up.astype(F32)).astype(BF16)
+    down = (down[half:] + far_down.astype(F32)).astype(BF16)
+    up, down = shifted(up, 1), shifted(down, -1)
+    return added(near[:half], up, above), added(near[half:], below, down)
 
 
 def gathered_over_tp(own):
@@ -336,24 +418,15 @@
 ):
     tokens, width = query.shape
     cols = resid.shape[1]
-    parts = w_out.shape[1] // cols
     model = w_out.shape[1]
     hidden = w_gate.shape[1]
     main = hidden // 128 * 128
     spare = hidden - main
-    down_t = w_down.T
-    packed = jnp.concatenate(
-        [
-            w_gate[:, :main],
-            w_value[:, :main],
-            down_t[:, :main],
-            w_gate[:, main:],
-            w_value[:, main:],
-            down_t[:, main:],
-            jnp.zeros((w_gate.shape[0], 128 - 3 * spare), BF16),
-        ],
-        axis=1,
-    )
+    packed = pl.pallas_call(
+        pack_kernel,
+        out_shape=shape((w_gate.shape[0], 3 * main + 128), BF16),
+        name="pack",
+    )(w_gate, w_value, w_down.T)
     weights = lax.all_gather(packed, SP, axis=0, tiled=True)
     tile = 256
     tiles = main // tile
@@ -388,14 +461,14 @@
     )(query, keys, values, rows, cols_aux)
     chip, core = lax.axis_index("y"), lax.axis_index("c")
     ring, cores = lax.axis_size("y"), lax.axis_size("c")
-    chips = (chip + jnp.arange(ring, dtype=jnp.int32)) % ring
-    sides = core ^ jnp.arange(cores, dtype=jnp.int32)
-    order = (chips[None, :] * cores + sides[:, None]).reshape(-1)
-    share, near, far = pl.pallas_call(
+    order = (chip + jnp.array([2, 2, 1, 1, 3, 3, 0, 0], jnp.int32)) % ring * cores + (
+        core ^ jnp.array([1, 0] * ring, jnp.int32)
+    )
+    swap, own, near, far_flags = pl.pallas_call(
         mix_kernel,
         grid_spec=pltpu.PrefetchScalarGridSpec(
             num_scalar_prefetch=1,
-            grid=(parts,),
+            grid=(ring,),
             in_specs=[
                 whole((tokens, width)),
                 whole((tokens, width)),
@@ -403,10 +476,12 @@
                 whole((8, tokens)),
                 whole((tokens, 8)),
                 whole((1, width)),
-                pl.BlockSpec((width, cols), lambda j, order: (0, order[j])),
+                pl.BlockSpec((width, cols), lambda j, order: (0, order[2 * j])),
+                pl.BlockSpec((width, cols), lambda j, order: (0, order[2 * j + 1])),
                 *[whole((DH + 16, width)) for _ in pays],
             ],
             out_specs=(
+                pl.BlockSpec((1, tokens, cols), lambda j, order: (j, 0, 0)),
                 pl.BlockSpec((1, tokens, cols), lambda j, order: (j, 0, 0)),
                 whole((tokens, 128)),
                 whole((tokens, 128)),
@@ -414,17 +489,19 @@
             scratch_shapes=[pltpu.VMEM((tokens, width), BF16)],
         ),
         out_shape=(
-            shape((parts, tokens, cols), BF16),
+            shape((ring, tokens, cols), BF16),
+            shape((ring, tokens, cols), BF16),
             shape((tokens, 128), F32),
             shape((tokens, 128), F32),
         ),
         name="mix",
-    )(order, query, out_gate, local, rows, cols_aux, head_gain.reshape(1, width), w_out, *pays)
-    attended = summed_over_tp(share.reshape(cores, ring, tokens, cols))
-    residual_own = resid.astype(F32) + attended
+    )(order, query, out_gate, local, rows, cols_aux, head_gain.reshape(1, width), w_out, w_out, *pays)
+    attended = summed_over_tp(swap[:3], own[:3], lambda: (swap[3], own[3]))
+    residual_own = resid.astype(F32) + jnp.concatenate(attended, axis=0)
     pieces = gathered_over_tp(residual_own.astype(BF16))
-    came = (chip + jnp.array([0, -1, 1, 2], jnp.int32)) % ring
-    places = (came[None, :] * cores + sides[:, None]).reshape(-1)
+    places = (chip + jnp.array([0, ring - 1, 1, 2] * 2, jnp.int32)) % ring * cores + (
+        core ^ jnp.array([0] * ring + [1] * ring, jnp.int32)
+    )
     block = 96
     normed, send = pl.pallas_call(
         norm_kernel,
@@ -443,17 +520,13 @@
     )(places, *pieces, ffn_gain.reshape(1, model))
     edge = lax.ppermute(send, SP, [(i, i + 1) for i in range(count - 1)])
     normed = lax.dynamic_update_slice(normed, edge, (0, 0))
-    first = tiles + 1
     tail_at = 3 * main // 128
-
-    def down_at(k, col):
-        return lambda j, order: (order[2 * jnp.maximum(j - first, 0) + k], col)
-
-    terms = pl.pallas_call(
+    sent = 2 * (ring - 1)
+    hidden, swap, own = pl.pallas_call(
         mixer_kernel,
         grid_spec=pltpu.PrefetchScalarGridSpec(
             num_scalar_prefetch=1,
-            grid=(first + parts // 2,),
+            grid=(tiles + ring - 1,),
             in_specs=[
                 pl.BlockSpec(
                     (tokens + HALO, model), lambda j, order: (0, 0), pipeline_mode=pl.Buffered(1)
@@ -465,27 +538,64 @@
                 pl.BlockSpec(
                     (model, tile), lambda j, order: (0, tiles + jnp.minimum(j, tiles - 1))
                 ),
-                pl.BlockSpec((model, 128), lambda j, order: (0, tail_at)),
-                pl.BlockSpec((cols, main), down_at(0, 2)),
-                pl.BlockSpec((cols, main), down_at(1, 2)),
-                pl.BlockSpec((cols, 128), down_at(0, tail_at)),
-                pl.BlockSpec((cols, 128), down_at(1, tail_at)),
+                pl.BlockSpec(
+                    (model, 128), lambda j, order: (0, tail_at), pipeline_mode=pl.Buffered(1)
+                ),
+                pl.BlockSpec(memory_space=pl.ANY),
             ],
-            out_specs=pl.BlockSpec(
-                (2, tokens, cols), lambda j, order: (jnp.maximum(j - first, 0), 0, 0)
+            out_specs=(
+                whole((tokens, main + 128)),
+                pl.BlockSpec(
+                    (1, tokens, cols), lambda j, order: (jnp.maximum(j - tiles, 0), 0, 0)
+                ),
+                pl.BlockSpec(
+                    (1, tokens, cols), lambda j, order: (jnp.maximum(j - tiles, 0), 0, 0)
+                ),
             ),
             scratch_shapes=[
-                pltpu.VMEM((2, tokens + HALO, tile), BF16),
-                pltpu.VMEM((2, tokens + HALO, tile), BF16),
-                pltpu.VMEM((tokens, main + 128), BF16),
+                pltpu.VMEM((2, tokens + HALO, tile), F32),
+                pltpu.VMEM((2, tokens + HALO, tile), F32),
+                pltpu.VMEM((tokens + HALO, 128), F32),
+                pltpu.VMEM((sent, cols, main + 128), BF16),
+                pltpu.SemaphoreType.DMA((2 * sent,)),
             ],
         ),
-        out_shape=shape((parts, tokens, cols), BF16),
-        compiler_params=pltpu.CompilerParams(vmem_limit_bytes=56 * 2**20),
+        out_shape=(
+            shape((tokens, main + 128), BF16),
+            shape((ring - 1, tokens, cols), BF16),
+            shape((ring - 1, tokens, cols), BF16),
+        ),
+        compiler_params=pltpu.CompilerParams(vmem_limit_bytes=58 * 2**20),
         name="mixer",
-    )(order, normed, near, far, taps, *[weights] * 7)
-    down = summed_over_tp(terms.reshape(cores, ring, tokens, cols))
-    return (residual_own + down).astype(BF16)
+    )(order, normed, near, far_flags, taps, *[weights] * 4)
+
+    def last():
+        def spot(k, col):
+            return lambda j, order: (order[sent + k], col)
+
+        one = shape((1, tokens, cols), BF16)
+        swap, own = pl.pallas_call(
+            down_kernel,
+            grid_spec=pltpu.PrefetchScalarGridSpec(
+                num_scalar_prefetch=1,
+                grid=(1,),
+                in_specs=[
+                    whole((tokens, main + 128)),
+                    pl.BlockSpec((cols, main), spot(0, 2)),
+                    pl.BlockSpec((cols, main), spot(1, 2)),
+                    pl.BlockSpec((cols, 128), spot(0, tail_at)),
+                    pl.BlockSpec((cols, 128), spot(1, tail_at)),
+                ],
+                out_specs=(whole((1, tokens, cols)), whole((1, tokens, cols))),
+            ),
+            out_shape=(one, one),
+            compiler_params=pltpu.CompilerParams(vmem_limit_bytes=40 * 2**20),
+            name="down",
+        )(order, hidden, *[weights] * 4)
+        return swap[0], own[0]
+
+    down = summed_over_tp(swap, own, last)
+    return (residual_own + jnp.concatenate(down, axis=0)).astype(BF16)
 
 
 def solution(mesh):

time: 217 us -> 206 us (0.949)
  local copies, waits for them, and re-layouts: 18 us -> 11.1 us
  starting transfers between devices: 40 us -> 45.6 us
  waiting for transfers between devices: 82.5 us -> 77.2 us
    ppermute x12 -> x16, waiting for transfers between devices: 54.9 us -> 45.1 us  [shifted(): return lax.ppermute(value, 'y', [(i, (i + by) % ring) for i in range(ring)])]
    all_gather x1, waiting for transfers between devices: 14 us -> 23.9 us  [layer(): weights = lax.all_gather(packed, SP, axis=0, tiled=True)]
    pallas_call x0 -> x2, Pallas kernels: none -> 6.56 us  [the longest x1 4.07 us: last(): pl.pallas_call(down_kernel, grid_spec=pltpu.PrefetchScalarGridSpec(num_sc...]
    ppermute x6 -> x8, waiting for transfers between devices: 9.22 us -> 3.85 us  [swapped(): return lax.ppermute(value, 'c', [(0, 1), (1, 0)])]
    slice x18 -> x3, local copies, waits for them, and re-layouts: 6.27 us -> 1.93 us  [the longest x1 1.8 us: layer(): attended = summed_over_tp(swap[:3], own[:3], lambda: (swap[3], own[3]))]
    ppermute x12 -> x16, starting transfers between devices: 20.1 us -> 24.4 us  [shifted(): return lax.ppermute(value, 'y', [(i, (i + by) % ring) for i in range(ring)])]
    pallas_call x1, Pallas kernels: 30.4 us -> 26.9 us  [layer(): pl.pallas_call(mixer_kernel, grid_spec=pltpu.PrefetchScalarGridSpec(num_s...]
    pallas_call x1, Pallas kernels: 8.14 us -> 5.32 us  [layer(): pl.pallas_call(norm_kernel, grid_spec=pltpu.PrefetchScalarGridSpec(num_sc...]
  transfers between devices with their start and end apart: 24 -> 30, of which waited for: 11 -> 14; matrix products, arithmetic and copies ran while one was open for 6% -> 5% of each run, Pallas kernels for 12% -> 12%
where the time goes in v4:
time: 206 us
  waiting for transfers between devices  77.2 us (37%)
  Pallas kernels  54 us (26%)
  starting transfers between devices  45.6 us (22%)
  between operations  13.8 us (7%)
  local copies, waits for them, and re-layouts  11.1 us (5%)
  other arithmetic  4 us (2%)
    ppermute x16, waiting for transfers between devices, shifted(): return lax.ppermute(value, 'y', [(i, (i + by) % ring) for i in range(ring)])  45.1 us
    pallas_call x1, Pallas kernels, layer(): pl.pallas_call(mixer_kernel, grid_spec=pltpu.PrefetchScalarGridSpec(num_s...  26.9 us
    ppermute x16, starting transfers between devices, shifted(): return lax.ppermute(value, 'y', [(i, (i + by) % ring) for i in range(ring)])  24.4 us
    all_gather x1, waiting for transfers between devices, layer(): weights = lax.all_gather(packed, SP, axis=0, tiled=True)  23.9 us
    ppermute x4, starting transfers between devices, layer(): lax.ppermute(pay, SP, [(i, i + k) for i in range(count - k)])  15.4 us
    pallas_call x1, Pallas kernels, layer(): pl.pallas_call(mix_kernel, grid_spec=pltpu.PrefetchScalarGridSpec(num_sca...  7.98 us
    unnamed x43, local copies, waits for them, and re-layouts  6.54 us
    pallas_call x1, Pallas kernels, layer(): pl.pallas_call(norm_kernel, grid_spec=pltpu.PrefetchScalarGridSpec(num_sc...  5.32 us
  transfers between devices with their start and end apart: 30, of which 14 were waited for; matrix products, arithmetic and copies ran while one was open for 5% of the time, Pallas kernels for 12%

profile of v4, /device:TPU:0, one launch (start us, length us, event | category | flops | bytes accessed | tf_op | source)
XLA Modules:
  0.0 205.8 jit_solution(6129587072468992894)
XLA Ops:
  6.5 2.5 %pack.1 = bf16[192,3200]{1,0:T(8,128)(2,1)} custom-call(bf16[192,1056]{1,0:T(8,128)(2,1)} %gate_ref.2, bf16[192,1056]{1,0:T(8,128)(2,1)} %value_ref.1, bf16[192,1056]{1,0:T(8,128)(2,1)} %bitcast.59), custom_call_target="tpu_custom_call" | custom-call | tf_op jit(solution)/shard_map/pack/pallas_call | solution.py:425
  9.1 0.7 copy-done.14
  9.7 0.6 reshape.52.doc_ref
  10.3 0.9 copy.23.k_ref
  11.2 0.9 copy.24.v_ref
  12.1 3.6 %state.1 = (bf16[112,192]{1,0:T(8,128)(2,1)}, f32[8,768]{1,0:T(8,128)}, f32[768,8]{1,0:T(8,128)}) custom-call(bf16[768,192]{1,0:T(8,128)(2,1)} %copy.23.k_ref, bf16[768,192]{1,0:T(8,128)(2,1)} %copy.24.v_ref, f32[2,768]{1,0:T(2,128)} %in_ref.1, f32[2,768]{1,0:T(2,128)} %forget_ref.1, s32[1,768]{1,0:T(1,128)} %reshape.52.doc_ref), custom_call_target="tpu_custom_call" | custom-call | tf_op jit(solution)/shard_map/state/pallas_call | solution.py:442
  15.8 3.9 %collective-permute-start.3 = (bf16[112,192]{1,0:T(8,128)(2,1)}, bf16[112,192]{1,0:T(8,128)(2,1)S(1)}, u32[]{:S(2)}, u32[]{:S(2)}) collective-permute-start(bf16[112,192]{1,0:T(8,128)(2,1)} %get-tuple-element.21), channel_id=1, source_target_pairs={{0,32},{8,40},{16,48},{24,56},{32,64},{40,72},{48,80},{56,88},{64,... | collective-permute-start | bytes 129032 | tf_op jit(solution)/shard_map/ppermute | solution.py:455
  19.7 4.7 %collective-permute-start.2 = (bf16[112,192]{1,0:T(8,128)(2,1)}, bf16[112,192]{1,0:T(8,128)(2,1)S(1)}, u32[]{:S(2)}, u32[]{:S(2)}) collective-permute-start(bf16[112,192]{1,0:T(8,128)(2,1)} %get-tuple-element.21), channel_id=1, source_target_pairs={{0,24},{8,32},{16,40},{24,48},{32,56},{40,64},{48,72},{56,80},{64,... | collective-permute-start | bytes 129032 | tf_op jit(solution)/shard_map/ppermute | solution.py:455
  24.4 4.1 %collective-permute-start.1 = (bf16[112,192]{1,0:T(8,128)(2,1)}, bf16[112,192]{1,0:T(8,128)(2,1)S(1)}, u32[]{:S(2)}, u32[]{:S(2)}) collective-permute-start(bf16[112,192]{1,0:T(8,128)(2,1)} %get-tuple-element.21), channel_id=1, source_target_pairs={{0,16},{8,24},{16,32},{24,40},{32,48},{40,56},{48,64},{56,72},{64,... | collective-permute-start | bytes 129032 | tf_op jit(solution)/shard_map/ppermute | solution.py:455
  28.4 2.8 %collective-permute-start = (bf16[112,192]{1,0:T(8,128)(2,1)}, bf16[112,192]{1,0:T(8,128)(2,1)S(1)}, u32[]{:S(2)}, u32[]{:S(2)}) collective-permute-start(bf16[112,192]{1,0:T(8,128)(2,1)} %get-tuple-element.21), channel_id=1, source_target_pairs={{0,8},{8,16},{16,24},{24,32},{32,40},{40,48},{48,56},{56,64},{64,7... | collective-permute-start | bytes 129032 | tf_op jit(solution)/shard_map/ppermute | solution.py:455
  31.3 0.6 fusion.20.order_ref
  31.9 0.9 copy.25.q_ref
  32.8 0.9 copy.26.gate_ref
  33.7 3.6 %local.1.local_ref = f32[768,192]{1,0:T(8,128)} custom-call(bf16[768,192]{1,0:T(8,128)(2,1)} %copy.25.q_ref, bf16[768,192]{1,0:T(8,128)(2,1)} %copy.23.k_ref, bf16[768,192]{1,0:T(8,128)(2,1)} %copy.24.v_ref, f32[8,768]{1,0:T(8,128)} %get-tuple-element.19.row_ref, f32[768,8]{1,0:T(8,128)} %get-tuple-element.20.col_ref), custom_call_target="tpu_custom_call" | custom-call | tf_op jit(solution)/shard_map/local/pallas_call | solution.py:457
  38.1 8.0 %mix.1 = (bf16[4,768,384]{2,1,0:T(8,128)(2,1)}, bf16[4,768,384]{2,1,0:T(8,128)(2,1)}, f32[768,128]{1,0:T(8,128)}, f32[768,128]{1,0:T(8,128)}) custom-call(s32[8]{0:T(128)} %fusion.20.order_ref, bf16[768,192]{1,0:T(8,128)(2,1)} %copy.25.q_ref, bf16[768,192]{1,0:T(8,128)(2,1)} %copy.26.gate_ref, f32[768,192]{1,0:T(8,128)} %local.1.local_ref, ...), custom_call_target="tpu_custom_call" | custom-call | tf_op jit(solution)/shard_map/mix/pallas_call | solution.py:467
  46.0 1.8 slice.145
  47.9 1.1 slice_bitcast_fusion.4
  49.6 2.0 collective-permute-done.5
  52.1 1.6 collective-permute-start.6
  53.8 1.7 collective-permute-start.10
  55.5 1.9 collective-permute-start.8
  57.6 5.6 %collective-permute-done.6 = bf16[384,384]{1,0:T(8,128)(2,1)S(1)} collective-permute-done((bf16[384,384]{1,0:T(8,128)(2,1)S(1)}, bf16[384,384]{1,0:T(8,128)(2,1)S(1)}, u32[]{:S(2)}, u32[]{:S(2)}) %collective-permute-start.6) | collective-permute-done | bytes 294944 | tf_op jit(solution)/shard_map/ppermute | solution.py:363
  63.8 3.0 %collective-permute-start.11 = (bf16[384,384]{1,0:T(8,128)(2,1)S(1)}, bf16[384,384]{1,0:T(8,128)(2,1)S(1)}, u32[]{:S(2)}, u32[]{:S(2)}) collective-permute-start(bf16[384,384]{1,0:T(8,128)(2,1)S(1)} %fusion.9), channel_id=1, source_target_pairs={{0,6},{2,0},{4,2},{6,4},{1,7},{3,1},{5,3},{7,5},{8,14},{10,8},{12,... | collective-permute-start | bytes 884744 | tf_op jit(solution)/shard_map/ppermute | solution.py:363
  66.9 3.1 %collective-permute-done.8 = bf16[384,384]{1,0:T(8,128)(2,1)S(1)} collective-permute-done((bf16[384,384]{1,0:T(8,128)(2,1)S(1)}, bf16[384,384]{1,0:T(8,128)(2,1)S(1)}, u32[]{:S(2)}, u32[]{:S(2)}) %collective-permute-start.8) | collective-permute-done | bytes 294944 | tf_op jit(solution)/shard_map/ppermute | solution.py:363
  70.0 5.1 %collective-permute-done.7 = bf16[384,384]{1,0:T(8,128)(2,1)S(1)} collective-permute-done((bf16[384,384]{1,0:T(8,128)(2,1)S(1)}, bf16[384,384]{1,0:T(8,128)(2,1)S(1)}, u32[]{:S(2)}, u32[]{:S(2)}) %collective-permute-start.7) | collective-permute-done | bytes 294944 | tf_op jit(solution)/shard_map/ppermute | solution.py:363
  75.6 1.6 collective-permute-start.12
  77.3 1.7 collective-permute-start.13
  78.9 12.5 %collective-permute-done.12.refs_1_ = bf16[768,384]{1,0:T(8,128)(2,1)S(1)} collective-permute-done((bf16[768,384]{1,0:T(8,128)(2,1)S(1)}, bf16[768,384]{1,0:T(8,128)(2,1)S(1)}, u32[]{:S(2)}, u32[]{:S(2)}) %collective-permute-start.12) | collective-permute-done | bytes 589856 | tf_op jit(solution)/shard_map/ppermute | solution.py:363
  91.7 3.1 %collective-permute-start.15 = (bf16[384,384]{1,0:T(8,128)(2,1)S(1)}, bf16[384,384]{1,0:T(8,128)(2,1)S(1)}, u32[]{:S(2)}, u32[]{:S(2)}) collective-permute-start(bf16[384,384]{1,0:T(8,128)(2,1)S(1)} %slice.196), channel_id=1, source_target_pairs={{0,6},{2,0},{4,2},{6,4},{1,7},{3,1},{5,3},{7,5},{8,14},{10,8},{12,... | collective-permute-start | bytes 884744 | tf_op jit(solution)/shard_map/ppermute | solution.py:363
  95.4 4.8 %collective-permute-done.14 = bf16[384,384]{1,0:T(8,128)(2,1)S(1)} collective-permute-done((bf16[384,384]{1,0:T(8,128)(2,1)S(1)}, bf16[384,384]{1,0:T(8,128)(2,1)S(1)}, u32[]{:S(2)}, u32[]{:S(2)}) %collective-permute-start.14) | collective-permute-done | bytes 294944 | tf_op jit(solution)/shard_map/ppermute | solution.py:363
  100.5 1.9 collective-permute-done.19.refs_7_
  102.4 5.3 %norm.1 = (bf16[784,3072]{1,0:T(8,128)(2,1)}, bf16[16,3072]{1,0:T(8,128)(2,1)S(1)}) custom-call(s32[8]{0:T(128)S(1)} %fusion.23.order_ref, bf16[768,384]{1,0:T(8,128)(2,1)S(1)} %fusion.1.refs_0_, bf16[768,384]{1,0:T(8,128)(2,1)S(1)} %collective-permute-done.12.refs_1_, bf16[768,384]{1,0:T(8,128)(2,1)S(1)} %collective-permute-done.13.refs_2_, ...), custom_call_target="tpu_custom_call" | custom-call | tf_op jit(solution)/shard_map/norm/pallas_call | solution.py:506
  107.7 3.7 %collective-permute-start.20 = (bf16[16,3072]{1,0:T(8,128)(2,1)S(1)}, bf16[16,3072]{1,0:T(8,128)(2,1)S(1)}, u32[]{:S(2)}, u32[]{:S(2)}) collective-permute-start(bf16[16,3072]{1,0:T(8,128)(2,1)S(1)} %get-tuple-element.25), channel_id=1, source_target_pairs={{0,8},{8,16},{16,24},{24,32},{32,40},{40,48},{48,56},{56,64},{64,7... | collective-permute-start | bytes 294920 | tf_op jit(solution)/shard_map/ppermute | solution.py:521
  111.4 0.6 pad_maximum_fusion.taps_ref
  112.1 4.4 %collective-permute-done.20 = bf16[16,3072]{1,0:T(8,128)(2,1)S(1)} collective-permute-done((bf16[16,3072]{1,0:T(8,128)(2,1)S(1)}, bf16[16,3072]{1,0:T(8,128)(2,1)S(1)}, u32[]{:S(2)}, u32[]{:S(2)}) %collective-permute-start.20) | collective-permute-done | bytes 98336 | tf_op jit(solution)/shard_map/ppermute | solution.py:521
  116.5 0.6 constant_dynamic-update-slice_fusion.2.x_ref
  117.1 23.9 %all-gather.2.cloned.1.call-done.wg_ref.wv_ref.wt_ref.w_ref.wa_ref.wb_ref.ta_ref.tb_ref = bf16[3072,3200]{1,0:T(8,128)(2,1)} async-done(((bf16[192,3200]{1,0:T(8,128)(2,1)}), bf16[3072,3200]{1,0:T(8,128)(2,1)}) %all-gather.2.cloned.1.call-update) | async-done | bytes 19660816 | tf_op jit(solution)/shard_map/all_gather | solution.py:430
  141.0 26.9 %mixer.1 = (bf16[768,1152]{1,0:T(8,128)(2,1)}, bf16[3,768,384]{2,1,0:T(8,128)(2,1)}, bf16[3,768,384]{2,1,0:T(8,128)(2,1)}) custom-call(s32[8]{0:T(128)} %fusion.20.order_ref, bf16[784,3072]{1,0:T(8,128)(2,1)} %constant_dynamic-update-slice_fusion.2.x_ref, f32[768,128]{1,0:T(8,128)} %get-tuple-element.26.near_ref, f32[768,128]{1,0:T(8,128)} %get-tuple-element.27.far_ref, ...), custom_call_target="tpu_custom_call" | custom-call | tf_op jit(solution)/shard_map/mixer/pallas_call | solution.py:525
  168.2 1.5 copy-done
  169.7 4.1 %down.1 = (bf16[1,768,384]{2,1,0:T(8,128)(2,1)S(1)}, bf16[1,768,384]{2,1,0:T(8,128)(2,1)S(1)}) custom-call(s32[8]{0:T(128)S(1)} %copy-done.2, bf16[768,1152]{1,0:T(8,128)(2,1)S(1)} %copy-done, bf16[3072,3200]{1,0:T(8,128)(2,1)} %all-gather.2.cloned.1.call-done.wg_ref.wv_ref.wt_ref.w_ref.wa_ref.wb_ref.ta_ref.tb_ref, ...), custom_call_target="tpu_custom_call" | custom-call | tf_op jit(solution)/shard_map/down/pallas_call | solution.py:577
  174.8 1.5 collective-permute-start.23
  176.4 1.8 collective-permute-start.27
  178.3 1.6 collective-permute-start.25
  180.4 5.6 %collective-permute-done.23 = bf16[384,384]{1,0:T(8,128)(2,1)S(1)} collective-permute-done((bf16[384,384]{1,0:T(8,128)(2,1)S(1)}, bf16[384,384]{1,0:T(8,128)(2,1)S(1)}, u32[]{:S(2)}, u32[]{:S(2)}) %collective-permute-start.23) | collective-permute-done | bytes 294944 | tf_op jit(solution)/shard_map/ppermute | solution.py:363
  186.5 3.0 %collective-permute-start.28 = (bf16[384,384]{1,0:T(8,128)(2,1)S(1)}, bf16[384,384]{1,0:T(8,128)(2,1)S(1)}, u32[]{:S(2)}, u32[]{:S(2)}) collective-permute-start(bf16[384,384]{1,0:T(8,128)(2,1)S(1)} %fusion.3), channel_id=1, source_target_pairs={{0,6},{2,0},{4,2},{6,4},{1,7},{3,1},{5,3},{7,5},{8,14},{10,8},{12,... | collective-permute-start | bytes 884744 | tf_op jit(solution)/shard_map/ppermute | solution.py:363
  189.6 3.1 %collective-permute-done.25 = bf16[384,384]{1,0:T(8,128)(2,1)S(1)} collective-permute-done((bf16[384,384]{1,0:T(8,128)(2,1)S(1)}, bf16[384,384]{1,0:T(8,128)(2,1)S(1)}, u32[]{:S(2)}, u32[]{:S(2)}) %collective-permute-start.25) | collective-permute-done | bytes 294944 | tf_op jit(solution)/shard_map/ppermute | solution.py:363
  192.7 5.0 %collective-permute-done.24 = bf16[384,384]{1,0:T(8,128)(2,1)S(1)} collective-permute-done((bf16[384,384]{1,0:T(8,128)(2,1)S(1)}, bf16[384,384]{1,0:T(8,128)(2,1)S(1)}, u32[]{:S(2)}, u32[]{:S(2)}) %collective-permute-start.24) | collective-permute-done | bytes 294944 | tf_op jit(solution)/shard_map/ppermute | solution.py:363
  197.9 1.0 fusion
  (96 shorter events, 7.1 us)
Async XLA Ops:
  6.5 134.4 %all-gather.2.cloned.1.call-start = ((), (), s32[]{:S(2)}) async-start(), calls=%async_computation | async-start | bytes 20889600 | tf_op jit(solution)/shard_map/all_gather | solution.py:430
  9.0 0.7 copy-start.14
  9.0 1.3 copy-start.6
  9.0 2.2 %copy-start.7 = (bf16[768,192]{0,1:T(8,128)(2,1)S(1)}, bf16[768,192]{0,1:T(8,128)(2,1)}, u32[]{:S(2)}) copy-start(bf16[768,192]{0,1:T(8,128)(2,1)} %param.22) | copy-start | bytes 884740
  9.7 21.5 %copy-start.17 = (s32[8]{0:T(128)S(1)}, s32[8]{0:T(128)}, u32[]{:S(2)}) copy-start(s32[8]{0:T(128)} %constant.42.clone) | copy-start | bytes 100
  9.7 21.5 %copy-start.18 = (s32[8]{0:T(128)S(1)}, s32[8]{0:T(128)}, u32[]{:S(2)}) copy-start(s32[8]{0:T(128)} %constant.41.clone) | copy-start | bytes 100
  9.7 22.1 %copy-start.8 = (bf16[768,192]{0,1:T(8,128)(2,1)S(1)}, bf16[768,192]{0,1:T(8,128)(2,1)}, u32[]{:S(2)}) copy-start(bf16[768,192]{0,1:T(8,128)(2,1)} %param.20) | copy-start | bytes 884740
  11.2 21.6 %copy-start.9 = (bf16[768,192]{0,1:T(8,128)(2,1)S(1)}, bf16[768,192]{0,1:T(8,128)(2,1)}, u32[]{:S(2)}) copy-start(bf16[768,192]{0,1:T(8,128)(2,1)} %param.23) | copy-start | bytes 884740
  15.8 21.6 %collective-permute-start.3 = (bf16[112,192]{1,0:T(8,128)(2,1)}, bf16[112,192]{1,0:T(8,128)(2,1)S(1)}, u32[]{:S(2)}, u32[]{:S(2)}) collective-permute-start(bf16[112,192]{1,0:T(8,128)(2,1)} %get-tuple-element.21), channel_id=1, source_target_pairs={{0,32},{8,40},{16,48},{24,56},{32,64},{40,72},{48,80},{56,88},{64,... | collective-permute-start | bytes 129032 | tf_op jit(solution)/shard_map/ppermute | solution.py:455
  19.7 17.7 %collective-permute-start.2 = (bf16[112,192]{1,0:T(8,128)(2,1)}, bf16[112,192]{1,0:T(8,128)(2,1)S(1)}, u32[]{:S(2)}, u32[]{:S(2)}) collective-permute-start(bf16[112,192]{1,0:T(8,128)(2,1)} %get-tuple-element.21), channel_id=1, source_target_pairs={{0,24},{8,32},{16,40},{24,48},{32,56},{40,64},{48,72},{56,80},{64,... | collective-permute-start | bytes 129032 | tf_op jit(solution)/shard_map/ppermute | solution.py:455
  24.4 13.0 %collective-permute-start.1 = (bf16[112,192]{1,0:T(8,128)(2,1)}, bf16[112,192]{1,0:T(8,128)(2,1)S(1)}, u32[]{:S(2)}, u32[]{:S(2)}) collective-permute-start(bf16[112,192]{1,0:T(8,128)(2,1)} %get-tuple-element.21), channel_id=1, source_target_pairs={{0,16},{8,24},{16,32},{24,40},{32,48},{40,56},{48,64},{56,72},{64,... | collective-permute-start | bytes 129032 | tf_op jit(solution)/shard_map/ppermute | solution.py:455
  28.4 9.0 %collective-permute-start = (bf16[112,192]{1,0:T(8,128)(2,1)}, bf16[112,192]{1,0:T(8,128)(2,1)S(1)}, u32[]{:S(2)}, u32[]{:S(2)}) collective-permute-start(bf16[112,192]{1,0:T(8,128)(2,1)} %get-tuple-element.21), channel_id=1, source_target_pairs={{0,8},{8,16},{16,24},{24,32},{32,40},{40,48},{48,56},{56,64},{64,7... | collective-permute-start | bytes 129032 | tf_op jit(solution)/shard_map/ppermute | solution.py:455
  37.4 0.7 copy-start.12
  46.0 5.6 %copy-start.3 = (bf16[4,768,384]{2,1,0:T(8,128)(2,1)S(1)}, bf16[4,768,384]{2,1,0:T(8,128)(2,1)}, u32[]{:S(2)}) copy-start(bf16[4,768,384]{2,1,0:T(8,128)(2,1)} %get-tuple-element.22) | copy-start | bytes 7077892
  47.9 3.8 %collective-permute-start.5 = (bf16[3,768,384]{2,1,0:T(8,128)(2,1)S(1)}, bf16[3,768,384]{2,1,0:T(8,128)(2,1)S(1)}, u32[]{:S(2)}, u32[]{:S(2)}) collective-permute-start(bf16[3,768,384]{2,1,0:T(8,128)(2,1)S(1)} %slice.145), channel_id=1, source_target_pairs={{0,1},{1,0},{2,3},{3,2},{4,5},{5,4},{6,7},{7,6},{8,9},{9,8},{10,11... | collective-permute-start | bytes 5308424 | tf_op jit(solution)/shard_map/ppermute | solution.py:367
  49.1 17.7 %collective-permute-start.4 = (bf16[768,384]{1,0:T(8,128)(2,1)S(1)}, bf16[768,384]{1,0:T(8,128)(2,1)S(1)}, u32[]{:S(2)}, u32[]{:S(2)}) collective-permute-start(bf16[768,384]{1,0:T(8,128)(2,1)S(1)} %slice_bitcast_fusion.4), channel_id=1, source_target_pairs={{0,1},{1,0},{2,3},{3,2},{4,5},{5,4},{6,7},{7,6},{8,9},{9,8},{10,11... | collective-permute-start | bytes 1769480 | tf_op jit(solution)/shard_map/ppermute | solution.py:367
  52.1 11.2 %collective-permute-start.6 = (bf16[384,384]{1,0:T(8,128)(2,1)S(1)}, bf16[384,384]{1,0:T(8,128)(2,1)S(1)}, u32[]{:S(2)}, u32[]{:S(2)}) collective-permute-start(bf16[384,384]{1,0:T(8,128)(2,1)S(1)} %get-tuple-element.45), channel_id=1, source_target_pairs={{0,2},{2,4},{4,6},{6,0},{1,3},{3,5},{5,7},{7,1},{8,10},{10,12},{12... | collective-permute-start | bytes 884744 | tf_op jit(solution)/shard_map/ppermute | solution.py:363
  53.8 10.0 %collective-permute-start.10 = (bf16[384,384]{1,0:T(8,128)(2,1)S(1)}, bf16[384,384]{1,0:T(8,128)(2,1)S(1)}, u32[]{:S(2)}, u32[]{:S(2)}) collective-permute-start(bf16[384,384]{1,0:T(8,128)(2,1)S(1)} %get-tuple-element.46), channel_id=1, source_target_pairs={{0,6},{2,0},{4,2},{6,4},{1,7},{3,1},{5,3},{7,5},{8,14},{10,8},{12,... | collective-permute-start | bytes 884744 | tf_op jit(solution)/shard_map/ppermute | solution.py:363
  55.5 14.5 %collective-permute-start.8 = (bf16[384,384]{1,0:T(8,128)(2,1)S(1)}, bf16[384,384]{1,0:T(8,128)(2,1)S(1)}, u32[]{:S(2)}, u32[]{:S(2)}) collective-permute-start(bf16[384,384]{1,0:T(8,128)(2,1)S(1)} %fusion.14), channel_id=1, source_target_pairs={{0,6},{2,0},{4,2},{6,4},{1,7},{3,1},{5,3},{7,5},{8,14},{10,8},{12,... | collective-permute-start | bytes 884744 | tf_op jit(solution)/shard_map/ppermute | solution.py:363
  57.4 12.6 %collective-permute-start.9 = (bf16[384,384]{1,0:T(8,128)(2,1)S(1)}, bf16[384,384]{1,0:T(8,128)(2,1)S(1)}, u32[]{:S(2)}, u32[]{:S(2)}) collective-permute-start(bf16[384,384]{1,0:T(8,128)(2,1)S(1)} %fusion.15), channel_id=1, source_target_pairs={{0,2},{2,4},{4,6},{6,0},{1,3},{3,5},{5,7},{7,1},{8,10},{10,12},{12... | collective-permute-start | bytes 884744 | tf_op jit(solution)/shard_map/ppermute | solution.py:363
  63.3 11.8 %collective-permute-start.7 = (bf16[384,384]{1,0:T(8,128)(2,1)S(1)}, bf16[384,384]{1,0:T(8,128)(2,1)S(1)}, u32[]{:S(2)}, u32[]{:S(2)}) collective-permute-start(bf16[384,384]{1,0:T(8,128)(2,1)S(1)} %fusion.12), channel_id=1, source_target_pairs={{0,2},{2,4},{4,6},{6,0},{1,3},{3,5},{5,7},{7,1},{8,10},{10,12},{12... | collective-permute-start | bytes 884744 | tf_op jit(solution)/shard_map/ppermute | solution.py:363
  63.8 11.4 %collective-permute-start.11 = (bf16[384,384]{1,0:T(8,128)(2,1)S(1)}, bf16[384,384]{1,0:T(8,128)(2,1)S(1)}, u32[]{:S(2)}, u32[]{:S(2)}) collective-permute-start(bf16[384,384]{1,0:T(8,128)(2,1)S(1)} %fusion.9), channel_id=1, source_target_pairs={{0,6},{2,0},{4,2},{6,4},{1,7},{3,1},{5,3},{7,5},{8,14},{10,8},{12,... | collective-permute-start | bytes 884744 | tf_op jit(solution)/shard_map/ppermute | solution.py:363
  66.9 8.6 %copy-start.4 = (bf16[768,384]{1,0:T(8,128)(2,1)S(1)}, bf16[768,384]{1,0:T(8,128)(2,1)}, u32[]{:S(2)}) copy-start(bf16[768,384]{1,0:T(8,128)(2,1)} %param.19) | copy-start | bytes 1769476
  75.6 24.8 %slice-start = ((f32[3,1056]{1,0:T(4,128)}), f32[3,32]{1,0:T(4,128)S(1)}, s32[]{:S(2)}) async-start(f32[3,1056]{1,0:T(4,128)} %param.32), calls=%async_computation.1 | async-start | bytes 4096 | tf_op jit(solution)/shard_map/slice | solution.py:437
  75.6 24.9 %copy-start.15 = (s32[8]{0:T(128)S(1)}, s32[8]{0:T(128)}, u32[]{:S(2)}) copy-start(s32[8]{0:T(128)} %constant.44.clone) | copy-start | bytes 100
  75.6 24.9 %copy-start.16 = (s32[8]{0:T(128)S(1)}, s32[8]{0:T(128)}, u32[]{:S(2)}) copy-start(s32[8]{0:T(128)} %constant.43.clone) | copy-start | bytes 100
  75.6 26.8 %copy-start.1 = (f32[3072]{0:T(1024)S(1)}, f32[3072]{0:T(1024)}, u32[]{:S(2)}) copy-start(f32[3072]{0:T(1024)} %param.29) | copy-start | bytes 36868
  75.6 15.8 %collective-permute-start.12 = (bf16[768,384]{1,0:T(8,128)(2,1)S(1)}, bf16[768,384]{1,0:T(8,128)(2,1)S(1)}, u32[]{:S(2)}, u32[]{:S(2)}) collective-permute-start(bf16[768,384]{1,0:T(8,128)(2,1)S(1)} %fusion.1.refs_0_), channel_id=1, source_target_pairs={{0,2},{2,4},{4,6},{6,0},{1,3},{3,5},{5,7},{7,1},{8,10},{10,12},{12... | collective-permute-start | bytes 1769480 | tf_op jit(solution)/shard_map/ppermute | solution.py:363
  77.3 14.4 %collective-permute-start.13 = (bf16[768,384]{1,0:T(8,128)(2,1)S(1)}, bf16[768,384]{1,0:T(8,128)(2,1)S(1)}, u32[]{:S(2)}, u32[]{:S(2)}) collective-permute-start(bf16[768,384]{1,0:T(8,128)(2,1)S(1)} %fusion.1.refs_0_), channel_id=1, source_target_pairs={{0,6},{2,0},{4,2},{6,4},{1,7},{3,1},{5,3},{7,5},{8,14},{10,8},{12,... | collective-permute-start | bytes 1769480 | tf_op jit(solution)/shard_map/ppermute | solution.py:363
  91.5 8.7 %collective-permute-start.14 = (bf16[384,384]{1,0:T(8,128)(2,1)S(1)}, bf16[384,384]{1,0:T(8,128)(2,1)S(1)}, u32[]{:S(2)}, u32[]{:S(2)}) collective-permute-start(bf16[384,384]{1,0:T(8,128)(2,1)S(1)} %slice.195), channel_id=1, source_target_pairs={{0,2},{2,4},{4,6},{6,0},{1,3},{3,5},{5,7},{7,1},{8,10},{10,12},{12... | collective-permute-start | bytes 884744 | tf_op jit(solution)/shard_map/ppermute | solution.py:363
  91.7 8.5 %collective-permute-start.15 = (bf16[384,384]{1,0:T(8,128)(2,1)S(1)}, bf16[384,384]{1,0:T(8,128)(2,1)S(1)}, u32[]{:S(2)}, u32[]{:S(2)}) collective-permute-start(bf16[384,384]{1,0:T(8,128)(2,1)S(1)} %slice.196), channel_id=1, source_target_pairs={{0,6},{2,0},{4,2},{6,4},{1,7},{3,1},{5,3},{7,5},{8,14},{10,8},{12,... | collective-permute-start | bytes 884744 | tf_op jit(solution)/shard_map/ppermute | solution.py:363
  94.9 5.6 %collective-permute-start.16 = (bf16[768,384]{1,0:T(8,128)(2,1)S(1)}, bf16[768,384]{1,0:T(8,128)(2,1)S(1)}, u32[]{:S(2)}, u32[]{:S(2)}) collective-permute-start(bf16[768,384]{1,0:T(8,128)(2,1)S(1)} %fusion.1.refs_0_), channel_id=1, source_target_pairs={{0,1},{1,0},{2,3},{3,2},{4,5},{5,4},{6,7},{7,6},{8,9},{9,8},{10,11... | collective-permute-start | bytes 1769480 | tf_op jit(solution)/shard_map/ppermute | solution.py:367
  94.9 5.6 %collective-permute-start.18 = (bf16[768,384]{1,0:T(8,128)(2,1)S(1)}, bf16[768,384]{1,0:T(8,128)(2,1)S(1)}, u32[]{:S(2)}, u32[]{:S(2)}) collective-permute-start(bf16[768,384]{1,0:T(8,128)(2,1)S(1)} %collective-permute-done.13.refs_2_), channel_id=1, source_target_pairs={{0,1},{1,0},{2,3},{3,2},{4,5},{5,4},{6,7},{7,6},{8,9},{9,8},{10,11... | collective-permute-start | bytes 1769480 | tf_op jit(solution)/shard_map/ppermute | solution.py:367
  95.4 5.1 %collective-permute-start.17 = (bf16[768,384]{1,0:T(8,128)(2,1)S(1)}, bf16[768,384]{1,0:T(8,128)(2,1)S(1)}, u32[]{:S(2)}, u32[]{:S(2)}) collective-permute-start(bf16[768,384]{1,0:T(8,128)(2,1)S(1)} %collective-permute-done.12.refs_1_), channel_id=1, source_target_pairs={{0,1},{1,0},{2,3},{3,2},{4,5},{5,4},{6,7},{7,6},{8,9},{9,8},{10,11... | collective-permute-start | bytes 1769480 | tf_op jit(solution)/shard_map/ppermute | solution.py:367
  100.3 2.1 %collective-permute-start.19 = (bf16[768,384]{1,0:T(8,128)(2,1)S(1)}, bf16[768,384]{1,0:T(8,128)(2,1)S(1)}, u32[]{:S(2)}, u32[]{:S(2)}) collective-permute-start(bf16[768,384]{1,0:T(8,128)(2,1)S(1)} %constant_dynamic-update-slice_fusion.refs_3_), channel_id=1, source_target_pairs={{0,1},{1,0},{2,3},{3,2},{4,5},{5,4},{6,7},{7,6},{8,9},{9,8},{10,11... | collective-permute-start | bytes 1769480 | tf_op jit(solution)/shard_map/ppermute | solution.py:367
  102.4 9.0 %slice-start.1 = ((f32[3,1056]{1,0:T(4,128)}), f32[3,1024]{1,0:T(4,128)S(1)}, s32[]{:S(2)}) async-start(f32[3,1056]{1,0:T(4,128)} %param.32), calls=%async_computation.2 | async-start | bytes 32768 | tf_op jit(solution)/shard_map/slice | solution.py:436
  107.7 8.7 %collective-permute-start.20 = (bf16[16,3072]{1,0:T(8,128)(2,1)S(1)}, bf16[16,3072]{1,0:T(8,128)(2,1)S(1)}, u32[]{:S(2)}, u32[]{:S(2)}) collective-permute-start(bf16[16,3072]{1,0:T(8,128)(2,1)S(1)} %get-tuple-element.25), channel_id=1, source_target_pairs={{0,8},{8,16},{16,24},{24,32},{32,40},{40,48},{48,56},{56,64},{64,7... | collective-permute-start | bytes 294920 | tf_op jit(solution)/shard_map/ppermute | solution.py:521
  141.0 27.2 %copy-start.2 = (s32[8]{0:T(128)S(1)}, s32[8]{0:T(128)}, u32[]{:S(2)}) copy-start(s32[8]{0:T(128)} %fusion.20.order_ref) | copy-start | bytes 100
  167.9 6.4 %collective-permute-start.22 = (bf16[3,768,384]{2,1,0:T(8,128)(2,1)}, bf16[3,768,384]{2,1,0:T(8,128)(2,1)S(1)}, u32[]{:S(2)}, u32[]{:S(2)}) collective-permute-start(bf16[3,768,384]{2,1,0:T(8,128)(2,1)} %get-tuple-element.32), channel_id=1, source_target_pairs={{0,1},{1,0},{2,3},{3,2},{4,5},{5,4},{6,7},{7,6},{8,9},{9,8},{10,11... | collective-permute-start | bytes 5308424 | tf_op jit(solution)/shard_map/ppermute | solution.py:367
  168.2 1.5 copy-start
  169.7 4.6 %copy-start.5 = (bf16[3,768,384]{2,1,0:T(8,128)(2,1)S(1)}, bf16[3,768,384]{2,1,0:T(8,128)(2,1)}, u32[]{:S(2)}) copy-start(bf16[3,768,384]{2,1,0:T(8,128)(2,1)} %get-tuple-element.31) | copy-start | bytes 5308420
  173.8 15.7 %collective-permute-start.21 = (bf16[768,384]{1,0:T(8,128)(2,1)S(1)}, bf16[768,384]{1,0:T(8,128)(2,1)S(1)}, u32[]{:S(2)}, u32[]{:S(2)}) collective-permute-start(bf16[768,384]{1,0:T(8,128)(2,1)S(1)} %bitcast.58), channel_id=1, source_target_pairs={{0,1},{1,0},{2,3},{3,2},{4,5},{5,4},{6,7},{7,6},{8,9},{9,8},{10,11... | collective-permute-start | bytes 1769480 | tf_op jit(solution)/shard_map/ppermute | solution.py:367
  174.8 11.2 %collective-permute-start.23 = (bf16[384,384]{1,0:T(8,128)(2,1)S(1)}, bf16[384,384]{1,0:T(8,128)(2,1)S(1)}, u32[]{:S(2)}, u32[]{:S(2)}) collective-permute-start(bf16[384,384]{1,0:T(8,128)(2,1)S(1)} %get-tuple-element.43), channel_id=1, source_target_pairs={{0,2},{2,4},{4,6},{6,0},{1,3},{3,5},{5,7},{7,1},{8,10},{10,12},{12... | collective-permute-start | bytes 884744 | tf_op jit(solution)/shard_map/ppermute | solution.py:363
  176.4 10.0 %collective-permute-start.27 = (bf16[384,384]{1,0:T(8,128)(2,1)S(1)}, bf16[384,384]{1,0:T(8,128)(2,1)S(1)}, u32[]{:S(2)}, u32[]{:S(2)}) collective-permute-start(bf16[384,384]{1,0:T(8,128)(2,1)S(1)} %get-tuple-element.44), channel_id=1, source_target_pairs={{0,6},{2,0},{4,2},{6,4},{1,7},{3,1},{5,3},{7,5},{8,14},{10,8},{12,... | collective-permute-start | bytes 884744 | tf_op jit(solution)/shard_map/ppermute | solution.py:363
  178.3 14.4 %collective-permute-start.25 = (bf16[384,384]{1,0:T(8,128)(2,1)S(1)}, bf16[384,384]{1,0:T(8,128)(2,1)S(1)}, u32[]{:S(2)}, u32[]{:S(2)}) collective-permute-start(bf16[384,384]{1,0:T(8,128)(2,1)S(1)} %fusion.16), channel_id=1, source_target_pairs={{0,6},{2,0},{4,2},{6,4},{1,7},{3,1},{5,3},{7,5},{8,14},{10,8},{12,... | collective-permute-start | bytes 884744 | tf_op jit(solution)/shard_map/ppermute | solution.py:363
  179.9 12.8 %collective-permute-start.26 = (bf16[384,384]{1,0:T(8,128)(2,1)S(1)}, bf16[384,384]{1,0:T(8,128)(2,1)S(1)}, u32[]{:S(2)}, u32[]{:S(2)}) collective-permute-start(bf16[384,384]{1,0:T(8,128)(2,1)S(1)} %fusion.17), channel_id=1, source_target_pairs={{0,2},{2,4},{4,6},{6,0},{1,3},{3,5},{5,7},{7,1},{8,10},{10,12},{12... | collective-permute-start | bytes 884744 | tf_op jit(solution)/shard_map/ppermute | solution.py:363
  186.0 11.6 %collective-permute-start.24 = (bf16[384,384]{1,0:T(8,128)(2,1)S(1)}, bf16[384,384]{1,0:T(8,128)(2,1)S(1)}, u32[]{:S(2)}, u32[]{:S(2)}) collective-permute-start(bf16[384,384]{1,0:T(8,128)(2,1)S(1)} %fusion.6), channel_id=1, source_target_pairs={{0,2},{2,4},{4,6},{6,0},{1,3},{3,5},{5,7},{7,1},{8,10},{10,12},{12... | collective-permute-start | bytes 884744 | tf_op jit(solution)/shard_map/ppermute | solution.py:363
  186.5 11.3 %collective-permute-start.28 = (bf16[384,384]{1,0:T(8,128)(2,1)S(1)}, bf16[384,384]{1,0:T(8,128)(2,1)S(1)}, u32[]{:S(2)}, u32[]{:S(2)}) collective-permute-start(bf16[384,384]{1,0:T(8,128)(2,1)S(1)} %fusion.3), channel_id=1, source_target_pairs={{0,6},{2,0},{4,2},{6,4},{1,7},{3,1},{5,3},{7,5},{8,14},{10,8},{12,... | collective-permute-start | bytes 884744 | tf_op jit(solution)/shard_map/ppermute | solution.py:363
  (3 other events, 1.9 us)
Sparse Core Ops, SparseCore 0:
  9.5 131.4 all-gather.1
